TPU v7x, 256 devices: a whole 4x4x8 slice. The times are simulated.
256 devices in a mesh: sp: 32 (over z, y), fs: 4 (over x), tp: 2 (over core).
Axes of the slice: x: 4, y: 4, z: 8, core: 2. Of those that a mesh axis runs over, the one named last changes fastest.
Arguments:
- hidden_in: bfloat16 [4, 8192, 2048], P('fs', 'sp', 'tp'), may hold values from -6 to 6
- sb_query_w: bfloat16 [2048, 1024], P('fs', 'tp'), may hold values from -0.21875 to 0.21875
- sb_key_w: bfloat16 [2048, 1024], P('fs', 'tp'), may hold values from -0.21875 to 0.21875
- sb_value_w: bfloat16 [2048, 1024], P('fs', 'tp'), may hold values from -0.125 to 0.125
- sb_offset: float32 [16], P('tp'), may hold values from -16 to -6
- delta_query_w: bfloat16 [2048, 1024], P('fs', 'tp'), may hold values from -0.125 to 0.125
- delta_key_w: bfloat16 [2048, 1024], P('fs', 'tp'), may hold values from -0.125 to 0.125
- delta_value_w: bfloat16 [2048, 1024], P('fs', 'tp'), may hold values from -0.125 to 0.125
- decay_w: bfloat16 [2048, 8], P(None, 'tp'), may hold values from -0.125 to 0.125
- write_w: bfloat16 [2048, 8], P(None, 'tp'), may hold values from -0.125 to 0.125
- write_bias: float32 [8], P('tp'), may hold values from -7 to 1.5
- decay_log_scale: float32 [8], P('tp'), may hold values from -14 to -3
- decay_shift: float32 [4, 8, 8192], P('fs', 'tp', 'sp'), may hold values from -3 to 0
- head_gain: float32 [128], replicated, may hold values from 0.1 to 1.9
- sb_out_w: bfloat16 [1024, 2048], P('tp'), may hold values from -0.125 to 0.125
- delta_out_w: bfloat16 [1024, 2048], P('tp'), may hold values from -0.125 to 0.125
Outputs:
- mixed_out: bfloat16 [4, 8192, 2048], P('fs', ('sp', 'tp'))
All inputs are finite; a program needn't handle non-finite values.
Results may differ from a plain program's by a relative error of at most 0.015.
Values may be sent and summed in bfloat16 or wider, within the bound.
A program may use at most 128 MiB of HBM per device.

v0:
```python
import jax
import jax.numpy as jnp
from jax import lax
from jax.sharding import Mesh
from jax.sharding import PartitionSpec as P

SB_DIM = 64
GDN_DIM = 128
BLOCK = 64
SP = ("sp_0", "sp_1")
SP_TP = ("sp_0", "sp_1", "tp")


NORM_EPS = 1e-06


def joined_along(tiles, dim):
    tiles = jnp.moveaxis(tiles, 0, dim)
    shape = tiles.shape
    return tiles.reshape(*shape[:dim], shape[dim] * shape[dim + 1], *shape[dim + 2 :])


def sent_to_all(value, axis):
    devices = lax.axis_size(axis)
    return lax.all_to_all(
        jnp.broadcast_to(value[None], (devices, *value.shape)), axis, 0, 0, tiled=True
    )


def gathered_copies(value, axis, dim):
    return joined_along(sent_to_all(value, axis), dim)


def in_one_piece(arrays, axis, dim, along):
    widths = [a.shape[along] for a in arrays]
    both = jnp.concatenate(arrays, axis=along)
    result = lax.all_gather(both, axis, axis=dim, tiled=True)
    return tuple(jnp.split(result, [sum(widths[:k]) for k in range(1, len(widths))], axis=along))


def neutral_like(value, identity):
    return jax.tree.map(
        lambda part, zero: jnp.zeros_like(part) + jnp.asarray(zero, part.dtype), value, identity
    )


def entering(value, axes, combine, identity):
    before = start = neutral_like(value, identity)
    so_far = value
    for axis in reversed(axes):
        devices, index = (lax.axis_size(axis), lax.axis_index(axis))
        pieces = jax.tree.map(
            lambda part, kind: lax.all_gather(part.astype(kind), axis),
            so_far,
            (jnp.bfloat16, jnp.bfloat16),
        )
        inside, so_far = (start, start)
        for k in range(devices):
            passed = k < index
            so_far = combine(
                so_far, jax.tree.map(lambda part, own: part[k].astype(own.dtype), pieces, value)
            )
            inside = jax.tree.map(lambda new, old: jnp.where(passed, new, old), so_far, inside)
        before = combine(inside, before)
    return before


def split_up(value, dim, devices):
    before, after = (value.shape[:dim], value.shape[dim + 1 :])
    return jnp.moveaxis(value.reshape(*before, devices, -1, *after), dim, 0)


def sent_and_summed(value, axis, dim):
    tiles = split_up(value, dim, lax.axis_size(axis))
    arrived = lax.all_to_all(tiles, axis, split_axis=0, concat_axis=0, tiled=True)
    return arrived.astype(jnp.float32).sum(axis=0)


def unit_lower_inverse(strict_part):
    order_size = strict_part.shape[-1]
    powered = strict_part
    inverse = jnp.eye(order_size, dtype=strict_part.dtype) - strict_part
    for repeat_number in range(max(1, (order_size - 1).bit_length()) - 1):
        powered = jnp.einsum("...ij,...jk->...ik", powered, powered)
        inverse = inverse + jnp.einsum("...ij,...jk->...ik", inverse, powered)
    return inverse


def to_blocks(row_data, block_span):
    blocks_count = row_data.shape[0] // block_span
    shaped = row_data.reshape((blocks_count, block_span) + row_data.shape[1:])
    return jnp.swapaxes(shaped, 1, 2)


def from_blocks(blocked):
    swapped = jnp.swapaxes(blocked, 1, 2)
    return swapped.reshape((-1,) + swapped.shape[2:])


def unit_rows(vectors):
    return vectors * lax.rsqrt(jnp.sum(vectors * vectors, axis=-1, keepdims=True) + NORM_EPS)


def delta_inputs(
    query_proj,
    key_proj,
    value_proj,
    decay_pre,
    write_pre,
    write_bias,
    decay_log_scale,
    shift_rows,
    head_count,
    head_size,
):
    query_act = jax.nn.silu(query_proj.astype(jnp.float32)).reshape(-1, head_count, head_size)
    key_act = jax.nn.silu(key_proj.astype(jnp.float32)).reshape(-1, head_count, head_size)
    value_rows = jax.nn.silu(value_proj.astype(jnp.float32)).reshape(-1, head_count, head_size)
    queries = unit_rows(query_act) * head_size ** (-0.5)
    key_rows = unit_rows(key_act)
    log_decay = -jnp.exp(decay_log_scale) * jax.nn.softplus(decay_pre) + shift_rows
    strength = jax.nn.sigmoid(write_pre + write_bias)
    return (queries, key_rows, value_rows, log_decay, strength)


def delta_prepare(queries, key_rows, value_rows, log_decay, strength):
    block_span = queries.shape[2]
    cumulative = jnp.cumsum(log_decay, axis=-1)
    row_place = lax.broadcasted_iota(jnp.int32, (block_span, block_span), 0)
    col_place = lax.broadcasted_iota(jnp.int32, (block_span, block_span), 1)
    inclusive = col_place <= row_place
    strictly = col_place < row_place
    spread = cumulative[..., :, None] - cumulative[..., None, :]
    decay_table = jnp.where(inclusive, jnp.exp(jnp.where(inclusive, spread, 0.0)), 0.0)
    keys_beta = key_rows * strength[..., None]
    lower_part = jnp.where(
        strictly, jnp.einsum("nhik,nhjk->nhij", keys_beta, key_rows) * decay_table, 0.0
    )
    inverse = unit_lower_inverse(lower_part)
    growth = jnp.exp(cumulative)
    state_updates = jnp.einsum("nhij,nhjv->nhiv", inverse, value_rows * strength[..., None])
    erase_term = jnp.einsum("nhij,nhjk->nhik", inverse, keys_beta * growth[..., None])
    inside_block = jnp.einsum("nhik,nhjk->nhij", queries, key_rows) * decay_table
    boosted_query = queries * growth[..., None]
    damped_keys = key_rows * jnp.exp(cumulative[..., -1:] - cumulative)[..., None]
    decay_per_block = jnp.exp(cumulative[..., -1])
    return (state_updates, erase_term, inside_block, boosted_query, damped_keys, decay_per_block)


def delta_step(memory_state, inputs):
    state_updates, erase_term, inside_block, boosted_query, damped_keys, decay_per_block = inputs
    fixed_values = state_updates - jnp.einsum("mzq,mqc->mzc", erase_term, memory_state)
    produced_rows = jnp.einsum("mzq,mqc->mzc", boosted_query, memory_state) + jnp.einsum(
        "efq,eqn->efn", inside_block, fixed_values
    )
    memory_state = memory_state * decay_per_block[:, None, None] + jnp.einsum(
        "wam,waz->wmz", damped_keys, fixed_values
    )
    return (memory_state, produced_rows)


def transition_step(carried, inputs):
    memory_state, transfer = carried
    state_updates, erase_term, inside_block, boosted_query, damped_keys, decay_per_block = inputs
    fixed_values = state_updates - jnp.einsum("mzq,mqc->mzc", erase_term, memory_state)
    coupling = jnp.einsum("hik,hil->hkl", damped_keys, erase_term)
    memory_state = memory_state * decay_per_block[:, None, None] + jnp.einsum(
        "wam,waz->wmz", damped_keys, fixed_values
    )
    transfer = transfer * decay_per_block[:, None, None] - jnp.einsum(
        "hkl,hlm->hkm", coupling, transfer
    )
    return ((memory_state, transfer), None)


def compose(prior_blocks, following_blocks):
    joined_map = jnp.einsum("hkl,hlm->hkm", following_blocks[0], prior_blocks[0])
    joined_state = (
        jnp.einsum("djo,dog->djg", following_blocks[0], prior_blocks[1]) + following_blocks[1]
    )
    return (joined_map, joined_state)


def stick_block(queries, key_rows, value_rows, query_place, key_place, offsets):
    scale_factor = queries.shape[-1] ** (-0.5)
    scores = (
        jnp.einsum("qhd,khd->hqk", queries, key_rows, preferred_element_type=jnp.float32)
        * scale_factor
        + offsets[:, None, None]
    )
    visible = key_place[None, :] < query_place[:, None]
    skipped = jnp.where(visible, jax.nn.log_sigmoid(-scores), 0.0)
    beyond = lax.cumsum(skipped, axis=2, reverse=True) - skipped
    weights = jnp.where(visible, jnp.exp(jax.nn.log_sigmoid(scores) + beyond), 0.0).astype(
        jnp.bfloat16
    )
    partial_value = jnp.einsum(
        "hqk,khd->qhd", weights, value_rows, preferred_element_type=jnp.float32
    )
    return (partial_value, jnp.sum(skipped, axis=2).T)


def stick_combine(partials, totals):
    beyond = jnp.cumsum(totals[::-1], axis=0)[::-1] - totals
    return jnp.sum(partials * jnp.exp(beyond)[..., None], axis=0)


def on_device(
    hidden_in,
    sb_query_w,
    sb_key_w,
    sb_value_w,
    sb_offset,
    delta_query_w,
    delta_key_w,
    delta_value_w,
    decay_w,
    write_w,
    write_bias,
    decay_log_scale,
    decay_shift,
    head_gain,
    sb_out_w,
    delta_out_w,
):
    token_rows = hidden_in.shape[1]
    local_in = hidden_in.reshape(token_rows, hidden_in.shape[2])
    gathered = (
        lax.all_gather(sb_query_w, "fs", axis=0, tiled=True),
        lax.all_gather(sb_key_w, "fs", axis=0, tiled=True),
        lax.all_gather(sb_value_w, "fs", axis=0, tiled=True),
        lax.all_gather(delta_query_w, "fs", axis=0, tiled=True),
        lax.all_gather(delta_key_w, "fs", axis=0, tiled=True),
        lax.all_gather(delta_value_w, "fs", axis=0, tiled=True),
    )
    in_weights = tuple(gathered) + (decay_w, write_w)
    portion = gathered_copies(local_in, "tp", 1)
    projected = tuple(
        (jnp.dot(portion, weight, preferred_element_type=jnp.float32) for weight in in_weights)
    )
    sb_heads = sb_offset.shape[0]
    delta_heads = decay_log_scale.shape[0]
    sb_query = projected[0].astype(jnp.bfloat16).reshape(token_rows, sb_heads, SB_DIM)
    sb_keys = projected[1].astype(jnp.bfloat16)
    sb_values = projected[2].astype(jnp.bfloat16)
    shift_rows = decay_shift.reshape(delta_heads, token_rows).T
    queries, key_rows, value_rows, log_decay, strength = delta_inputs(
        projected[3].astype(jnp.bfloat16),
        projected[4].astype(jnp.bfloat16),
        projected[5].astype(jnp.bfloat16),
        projected[6],
        projected[7],
        write_bias,
        decay_log_scale,
        shift_rows,
        delta_heads,
        GDN_DIM,
    )
    prepared = delta_prepare(
        to_blocks(queries, BLOCK),
        to_blocks(key_rows, BLOCK),
        to_blocks(value_rows, BLOCK),
        to_blocks(log_decay, BLOCK),
        to_blocks(strength, BLOCK),
    )
    identity_map = jnp.broadcast_to(
        jnp.eye(GDN_DIM, dtype=jnp.float32), (delta_heads, GDN_DIM, GDN_DIM)
    )
    empty_state = jnp.zeros((delta_heads, GDN_DIM, GDN_DIM), jnp.float32)
    (local_end, local_map), unused_out = lax.scan(
        transition_step, (empty_state, identity_map), prepared
    )
    own_first = lax.axis_index(SP) * token_rows
    query_place = own_first + lax.iota(jnp.int32, token_rows)
    sp_count = lax.axis_size(SP)
    slot_out = jnp.zeros((sp_count, token_rows, sb_heads, SB_DIM), jnp.float32)
    slot_total = jnp.zeros((sp_count, token_rows, sb_heads), jnp.float32)

    def absorb(slot_arrays, address_portion, value_part, shard_first):

        def active(current):
            partial_value, totals = stick_block(
                sb_query,
                address_portion.reshape(token_rows, sb_heads, SB_DIM),
                value_part.reshape(token_rows, sb_heads, SB_DIM),
                query_place,
                shard_first + lax.iota(jnp.int32, token_rows),
                sb_offset,
            )
            slot_index = shard_first // token_rows
            return (
                lax.dynamic_update_index_in_dim(current[0], partial_value, slot_index, 0),
                lax.dynamic_update_index_in_dim(current[1], totals, slot_index, 0),
            )

        def inactive(current):
            return current

        usable = jnp.logical_and(shard_first >= 0, shard_first <= own_first)
        return lax.cond(usable, active, inactive, slot_arrays)

    key_block, value_block = in_one_piece((sb_keys, sb_values), SP, 0, 1)

    def per_shard(shard_number, current):
        row_begin = shard_number * token_rows
        return absorb(
            current,
            lax.dynamic_slice_in_dim(key_block, row_begin, token_rows, 0),
            lax.dynamic_slice_in_dim(value_block, row_begin, token_rows, 0),
            row_begin,
        )

    slot_arrays = lax.fori_loop(
        0, key_block.shape[0] // token_rows, per_shard, (slot_out, slot_total)
    )
    unused_map, incoming = entering(
        (local_map, local_end), SP, compose, (identity_map, empty_state)
    )
    sb_mixed = (
        stick_combine(slot_arrays[0], slot_arrays[1])
        .astype(jnp.bfloat16)
        .reshape(token_rows, sb_heads * SB_DIM)
    )
    unused_end, produced_rows = lax.scan(delta_step, incoming, prepared)
    produced_rows = from_blocks(produced_rows)
    normed = (
        produced_rows
        * lax.rsqrt(jnp.mean(produced_rows * produced_rows, axis=-1, keepdims=True) + NORM_EPS)
        * head_gain
    )
    delta_mixed = normed.astype(jnp.bfloat16).reshape(token_rows, delta_heads * GDN_DIM)
    result = sent_and_summed(
        (
            jnp.dot(sb_mixed, sb_out_w, preferred_element_type=jnp.float32)
            + jnp.dot(delta_mixed, delta_out_w, preferred_element_type=jnp.float32)
        ).astype(jnp.bfloat16),
        "tp",
        0,
    )
    return result.astype(jnp.bfloat16).reshape(1, result.shape[0], result.shape[1])


def solution(mesh):
    finer = Mesh(
        mesh.devices.reshape(8, 4, mesh.shape["fs"], mesh.shape["tp"]), ("sp_0", "sp_1", "fs", "tp")
    )
    return jax.shard_map(
        on_device,
        mesh=finer,
        in_specs=(
            P("fs", SP, "tp"),
            P("fs", "tp"),
            P("fs", "tp"),
            P("fs", "tp"),
            P("tp"),
            P("fs", "tp"),
            P("fs", "tp"),
            P("fs", "tp"),
            P(None, "tp"),
            P(None, "tp"),
            P("tp"),
            P("tp"),
            P("fs", "tp", SP),
            P(),
            P("tp", None),
            P("tp", None),
        ),
        out_specs=P("fs", SP_TP, None),
        check_vma=False,
    )
```

profile of v0, /device:TPU:249, one launch (start us, length us, event | category | flops | bytes accessed | tf_op | source)
XLA Modules:
  0.0 923.9 jit_solution(8913548011204064963)
XLA Ops:
  11.3 5.2 all-to-all-start
  22.8 19.7 %all-gather.22.cloned.1.call-done = bf16[2048,512]{1,0:T(8,128)(2,1)} async-done(((bf16[512,512]{1,0:T(8,128)(2,1)}), bf16[2048,512]{1,0:T(8,128)(2,1)}) %all-gather.22.cloned.1.call-update) | async-done | bytes 2097168 | tf_op jit(solution)/shard_map/all_gather | solution.py:233
  47.9 29.9 %all-gather.24.cloned.1.call-done = bf16[2048,512]{1,0:T(8,128)(2,1)} async-done(((bf16[512,512]{1,0:T(8,128)(2,1)}), bf16[2048,512]{1,0:T(8,128)(2,1)}) %all-gather.24.cloned.1.call-update) | async-done | bytes 2097168 | tf_op jit(solution)/shard_map/all_gather | solution.py:234
  93.1 10.3 %while.43 = (s32[]{:T(128)}, f32[4,128,128]{2,1,0:T(8,128)S(1)}, f32[4,128,128]{2,1,0:T(8,128)S(1)}, f32[4,4]{1,0:T(4,128)S(1)}, bf16[4,4,64,128]{3,2,1,0:T(8,12...) while((s32[]{:T(128)}, f32[4,128,128]{2,1,0:T(8,128)S(1)}, ...), condition=%wide.region_12.13_spmd.clone, body=%wide.region_11.12_spmd.clone.sunk | while | flops 42401792 | bytes 3019410 | solution.py:270
  103.4 10.7 %all-gather = bf16[16,128,128]{2,1,0:T(8,128)(2,1)S(1)} all-gather(bf16[4,128,128]{2,1,0:T(8,128)(2,1)S(1)} %convert_element_type.181), channel_id=2, replica_groups=mesh['sp_0'=8,'sp_1'=4,'fs'=4,'tp'=2] {'sp_1'}, dimensions={0}, use_global_device_ids=true | all-gather | bytes 655360 | tf_op jit(solution)/shard_map/all_gather | solution.py:53
  116.3 11.1 %all-gather.2 = bf16[16,128,128]{2,1,0:T(8,128)(2,1)S(1)} all-gather(bf16[4,128,128]{2,1,0:T(8,128)(2,1)S(1)} %convert_element_type.183), channel_id=4, replica_groups=mesh['sp_0'=8,'sp_1'=4,'fs'=4,'tp'=2] {'sp_1'}, dimensions={0}, use_global_device_ids=true | all-gather | bytes 655360 | tf_op jit(solution)/shard_map/all_gather | solution.py:53
  133.6 14.4 %all-gather.14.cloned.1.call-done = bf16[2048,512]{1,0:T(8,128)(2,1)} async-done(((bf16[512,512]{1,0:T(8,128)(2,1)}), bf16[2048,512]{1,0:T(8,128)(2,1)}) %all-gather.14.cloned.1.call-update) | async-done | bytes 2097168 | tf_op jit(solution)/shard_map/all_gather | solution.py:230
  151.6 31.4 %all-gather.26.cloned.1.call-done = bf16[2048,512]{1,0:T(8,128)(2,1)} async-done(((bf16[512,512]{1,0:T(8,128)(2,1)}), bf16[2048,512]{1,0:T(8,128)(2,1)}) %all-gather.26.cloned.1.call-update) | async-done | bytes 2097168 | tf_op jit(solution)/shard_map/all_gather | solution.py:232
  187.3 30.9 %all-gather.20.cloned.1.call-done = bf16[2048,512]{1,0:T(8,128)(2,1)} async-done(((bf16[512,512]{1,0:T(8,128)(2,1)}), bf16[2048,512]{1,0:T(8,128)(2,1)}) %all-gather.20.cloned.1.call-update) | async-done | bytes 2097168 | tf_op jit(solution)/shard_map/all_gather | solution.py:229
  225.1 26.8 %all-gather.28.cloned.1.call-done = bf16[32,128,128]{2,1,0:T(8,128)(2,1)} async-done(((bf16[4,128,128]{2,1,0:T(8,128)(2,1)}), bf16[32,128,128]{2,1,0:T(8,128)(2,1)}) %all-gather.28.cloned.1.call-update) | async-done | bytes 1048592 | tf_op jit(solution)/shard_map/all_gather | solution.py:53
  252.0 38.6 %all-gather.30.cloned.1.call-done = bf16[32,128,128]{2,1,0:T(8,128)(2,1)} async-done(((bf16[4,128,128]{2,1,0:T(8,128)(2,1)}), bf16[32,128,128]{2,1,0:T(8,128)(2,1)}) %all-gather.30.cloned.1.call-update) | async-done | bytes 1048592 | tf_op jit(solution)/shard_map/all_gather | solution.py:53
  298.6 13.8 %while.42 = (s32[]{:T(128)}, f32[4,128,128]{2,1,0:T(8,128)S(1)}, f32[4,4,64,128]{3,2,1,0:T(8,128)S(1)}, f32[4,4]{1,0:T(4,128)S(1)}, bf16[4,4,64,128]{3,2,1,0:T(8...) while((s32[]{:T(128)}, f32[4,128,128]{2,1,0:T(8,128)S(1)}, ...), condition=%wide.region_15.16_spmd, body=%wide.region_14.15_spmd.sunk | while | flops 29589504 | bytes 2034329 | solution.py:324
  314.5 118.9 %all-gather.18.cloned.1.call-done = bf16[8192,1024]{1,0:T(8,128)(2,1)} async-done(((bf16[256,1024]{1,0:T(8,128)(2,1)}), bf16[8192,1024]{1,0:T(8,128)(2,1)}) %all-gather.18.cloned.1.call-update) | async-done | bytes 16777232 | tf_op jit(solution)/shard_map/all_gather | solution.py:37
  433.5 11.3 %fusion.145 = (bf16[8192,512]{1,0:T(8,128)(2,1)}, bf16[8192,512]{1,0:T(8,128)(2,1)}) fusion(bf16[8192,1024]{1,0:T(8,128)(2,1)} %all-gather.18.cloned.1.call-done), kind=kLoop, calls=%fused_computation.198 | loop fusion | bytes 33554432 | tf_op jit(solution)/shard_map/split | solution.py:38
  444.8 11.5 %copy.85 = bf16[8192,512]{0,1:T(8,128)(2,1)} copy(bf16[8192,512]{1,0:T(8,128)(2,1)} %get-tuple-element.527) | data formatting | bytes 16777216
  456.3 11.3 %copy.84 = bf16[8192,512]{0,1:T(8,128)(2,1)} copy(bf16[8192,512]{1,0:T(8,128)(2,1)} %get-tuple-element.528) | data formatting | bytes 16777216
  467.7 7.9 broadcast_in_dim.96
  475.5 420.3 %while.44 = (s32[]{:T(128)}, f32[32,256,8,64]{1,3,2,0:T(8,128)}, f32[32,256,8]{1,2,0:T(8,128)S(1)}, s32[]{:T(128)}, bf16[8192,512]{0,1:T(8,128)(2,1)}, /*index=5...) while((s32[]{:T(128)}, f32[32,256,8,64]{1,3,2,0:T(8,128)}, ...), condition=%wide.region_6.7_spmd.clone.clone, body=%wide.region_0.6_spmd.clone.clone.sunk | while | flops 218698256 | bytes 25745960 | solution.py:313
  475.5 13.2 %conditional.4 = ((f32[32,256,8,64]{1,3,2,0:T(8,128)}, f32[32,256,8]{1,2,0:T(8,128)S(1)})) conditional(s32[]{:T(128)} %convert_element_type.285, (f32[32,256,8,64]{1,3,2,0:T(8,128)}, f32[32,256,8]{1,2,0:T(8,128)S(1)}) %tuple.97, (s32[]{:T(128)}, s32[]{:T(128)}, bf16[8192,512]{0,1:T(8,128)(2,1)}, bf16[256,8,64]{0,2,1:T(8,128)(2,1)S(1)}, ...), branch_computations={%region_1.1_spmd, %region_2.0_spmd} | conditional | flops 218698256 | bytes 25744700 | solution.py:300
  478.6 5.1 fusion.13
  488.7 13.1 %conditional.4 = ((f32[32,256,8,64]{1,3,2,0:T(8,128)}, f32[32,256,8]{1,2,0:T(8,128)S(1)})) conditional(s32[]{:T(128)} %convert_element_type.285, (f32[32,256,8,64]{1,3,2,0:T(8,128)}, f32[32,256,8]{1,2,0:T(8,128)S(1)}) %tuple.97, (s32[]{:T(128)}, s32[]{:T(128)}, bf16[8192,512]{0,1:T(8,128)(2,1)}, bf16[256,8,64]{0,2,1:T(8,128)(2,1)S(1)}, ...), branch_computations={%region_1.1_spmd, %region_2.0_spmd} | conditional | flops 218698256 | bytes 25744700 | solution.py:300
  501.9 13.1 %conditional.4 = ((f32[32,256,8,64]{1,3,2,0:T(8,128)}, f32[32,256,8]{1,2,0:T(8,128)S(1)})) conditional(s32[]{:T(128)} %convert_element_type.285, (f32[32,256,8,64]{1,3,2,0:T(8,128)}, f32[32,256,8]{1,2,0:T(8,128)S(1)}) %tuple.97, (s32[]{:T(128)}, s32[]{:T(128)}, bf16[8192,512]{0,1:T(8,128)(2,1)}, bf16[256,8,64]{0,2,1:T(8,128)(2,1)S(1)}, ...), branch_computations={%region_1.1_spmd, %region_2.0_spmd} | conditional | flops 218698256 | bytes 25744700 | solution.py:300
  504.8 5.1 fusion.13
  515.0 13.1 %conditional.4 = ((f32[32,256,8,64]{1,3,2,0:T(8,128)}, f32[32,256,8]{1,2,0:T(8,128)S(1)})) conditional(s32[]{:T(128)} %convert_element_type.285, (f32[32,256,8,64]{1,3,2,0:T(8,128)}, f32[32,256,8]{1,2,0:T(8,128)S(1)}) %tuple.97, (s32[]{:T(128)}, s32[]{:T(128)}, bf16[8192,512]{0,1:T(8,128)(2,1)}, bf16[256,8,64]{0,2,1:T(8,128)(2,1)S(1)}, ...), branch_computations={%region_1.1_spmd, %region_2.0_spmd} | conditional | flops 218698256 | bytes 25744700 | solution.py:300
  518.0 5.1 fusion.13
  528.1 13.1 %conditional.4 = ((f32[32,256,8,64]{1,3,2,0:T(8,128)}, f32[32,256,8]{1,2,0:T(8,128)S(1)})) conditional(s32[]{:T(128)} %convert_element_type.285, (f32[32,256,8,64]{1,3,2,0:T(8,128)}, f32[32,256,8]{1,2,0:T(8,128)S(1)}) %tuple.97, (s32[]{:T(128)}, s32[]{:T(128)}, bf16[8192,512]{0,1:T(8,128)(2,1)}, bf16[256,8,64]{0,2,1:T(8,128)(2,1)S(1)}, ...), branch_computations={%region_1.1_spmd, %region_2.0_spmd} | conditional | flops 218698256 | bytes 25744700 | solution.py:300
  531.1 5.1 fusion.13
  541.2 13.1 %conditional.4 = ((f32[32,256,8,64]{1,3,2,0:T(8,128)}, f32[32,256,8]{1,2,0:T(8,128)S(1)})) conditional(s32[]{:T(128)} %convert_element_type.285, (f32[32,256,8,64]{1,3,2,0:T(8,128)}, f32[32,256,8]{1,2,0:T(8,128)S(1)}) %tuple.97, (s32[]{:T(128)}, s32[]{:T(128)}, bf16[8192,512]{0,1:T(8,128)(2,1)}, bf16[256,8,64]{0,2,1:T(8,128)(2,1)S(1)}, ...), branch_computations={%region_1.1_spmd, %region_2.0_spmd} | conditional | flops 218698256 | bytes 25744700 | solution.py:300
  544.2 5.1 fusion.13
  554.4 13.1 %conditional.4 = ((f32[32,256,8,64]{1,3,2,0:T(8,128)}, f32[32,256,8]{1,2,0:T(8,128)S(1)})) conditional(s32[]{:T(128)} %convert_element_type.285, (f32[32,256,8,64]{1,3,2,0:T(8,128)}, f32[32,256,8]{1,2,0:T(8,128)S(1)}) %tuple.97, (s32[]{:T(128)}, s32[]{:T(128)}, bf16[8192,512]{0,1:T(8,128)(2,1)}, bf16[256,8,64]{0,2,1:T(8,128)(2,1)S(1)}, ...), branch_computations={%region_1.1_spmd, %region_2.0_spmd} | conditional | flops 218698256 | bytes 25744700 | solution.py:300
  557.3 5.1 fusion.13
  567.5 13.1 %conditional.4 = ((f32[32,256,8,64]{1,3,2,0:T(8,128)}, f32[32,256,8]{1,2,0:T(8,128)S(1)})) conditional(s32[]{:T(128)} %convert_element_type.285, (f32[32,256,8,64]{1,3,2,0:T(8,128)}, f32[32,256,8]{1,2,0:T(8,128)S(1)}) %tuple.97, (s32[]{:T(128)}, s32[]{:T(128)}, bf16[8192,512]{0,1:T(8,128)(2,1)}, bf16[256,8,64]{0,2,1:T(8,128)(2,1)S(1)}, ...), branch_computations={%region_1.1_spmd, %region_2.0_spmd} | conditional | flops 218698256 | bytes 25744700 | solution.py:300
  570.5 5.1 fusion.13
  580.6 13.1 %conditional.4 = ((f32[32,256,8,64]{1,3,2,0:T(8,128)}, f32[32,256,8]{1,2,0:T(8,128)S(1)})) conditional(s32[]{:T(128)} %convert_element_type.285, (f32[32,256,8,64]{1,3,2,0:T(8,128)}, f32[32,256,8]{1,2,0:T(8,128)S(1)}) %tuple.97, (s32[]{:T(128)}, s32[]{:T(128)}, bf16[8192,512]{0,1:T(8,128)(2,1)}, bf16[256,8,64]{0,2,1:T(8,128)(2,1)S(1)}, ...), branch_computations={%region_1.1_spmd, %region_2.0_spmd} | conditional | flops 218698256 | bytes 25744700 | solution.py:300
  583.6 5.1 fusion.13
  593.7 13.1 %conditional.4 = ((f32[32,256,8,64]{1,3,2,0:T(8,128)}, f32[32,256,8]{1,2,0:T(8,128)S(1)})) conditional(s32[]{:T(128)} %convert_element_type.285, (f32[32,256,8,64]{1,3,2,0:T(8,128)}, f32[32,256,8]{1,2,0:T(8,128)S(1)}) %tuple.97, (s32[]{:T(128)}, s32[]{:T(128)}, bf16[8192,512]{0,1:T(8,128)(2,1)}, bf16[256,8,64]{0,2,1:T(8,128)(2,1)S(1)}, ...), branch_computations={%region_1.1_spmd, %region_2.0_spmd} | conditional | flops 218698256 | bytes 25744700 | solution.py:300
  596.7 5.1 fusion.13
  606.9 13.1 %conditional.4 = ((f32[32,256,8,64]{1,3,2,0:T(8,128)}, f32[32,256,8]{1,2,0:T(8,128)S(1)})) conditional(s32[]{:T(128)} %convert_element_type.285, (f32[32,256,8,64]{1,3,2,0:T(8,128)}, f32[32,256,8]{1,2,0:T(8,128)S(1)}) %tuple.97, (s32[]{:T(128)}, s32[]{:T(128)}, bf16[8192,512]{0,1:T(8,128)(2,1)}, bf16[256,8,64]{0,2,1:T(8,128)(2,1)S(1)}, ...), branch_computations={%region_1.1_spmd, %region_2.0_spmd} | conditional | flops 218698256 | bytes 25744700 | solution.py:300
  609.8 5.1 fusion.13
  620.0 13.1 %conditional.4 = ((f32[32,256,8,64]{1,3,2,0:T(8,128)}, f32[32,256,8]{1,2,0:T(8,128)S(1)})) conditional(s32[]{:T(128)} %convert_element_type.285, (f32[32,256,8,64]{1,3,2,0:T(8,128)}, f32[32,256,8]{1,2,0:T(8,128)S(1)}) %tuple.97, (s32[]{:T(128)}, s32[]{:T(128)}, bf16[8192,512]{0,1:T(8,128)(2,1)}, bf16[256,8,64]{0,2,1:T(8,128)(2,1)S(1)}, ...), branch_computations={%region_1.1_spmd, %region_2.0_spmd} | conditional | flops 218698256 | bytes 25744700 | solution.py:300
  623.0 5.1 fusion.13
  633.1 13.1 %conditional.4 = ((f32[32,256,8,64]{1,3,2,0:T(8,128)}, f32[32,256,8]{1,2,0:T(8,128)S(1)})) conditional(s32[]{:T(128)} %convert_element_type.285, (f32[32,256,8,64]{1,3,2,0:T(8,128)}, f32[32,256,8]{1,2,0:T(8,128)S(1)}) %tuple.97, (s32[]{:T(128)}, s32[]{:T(128)}, bf16[8192,512]{0,1:T(8,128)(2,1)}, bf16[256,8,64]{0,2,1:T(8,128)(2,1)S(1)}, ...), branch_computations={%region_1.1_spmd, %region_2.0_spmd} | conditional | flops 218698256 | bytes 25744700 | solution.py:300
  636.1 5.1 fusion.13
  646.3 13.1 %conditional.4 = ((f32[32,256,8,64]{1,3,2,0:T(8,128)}, f32[32,256,8]{1,2,0:T(8,128)S(1)})) conditional(s32[]{:T(128)} %convert_element_type.285, (f32[32,256,8,64]{1,3,2,0:T(8,128)}, f32[32,256,8]{1,2,0:T(8,128)S(1)}) %tuple.97, (s32[]{:T(128)}, s32[]{:T(128)}, bf16[8192,512]{0,1:T(8,128)(2,1)}, bf16[256,8,64]{0,2,1:T(8,128)(2,1)S(1)}, ...), branch_computations={%region_1.1_spmd, %region_2.0_spmd} | conditional | flops 218698256 | bytes 25744700 | solution.py:300
  659.4 13.1 %conditional.4 = ((f32[32,256,8,64]{1,3,2,0:T(8,128)}, f32[32,256,8]{1,2,0:T(8,128)S(1)})) conditional(s32[]{:T(128)} %convert_element_type.285, (f32[32,256,8,64]{1,3,2,0:T(8,128)}, f32[32,256,8]{1,2,0:T(8,128)S(1)}) %tuple.97, (s32[]{:T(128)}, s32[]{:T(128)}, bf16[8192,512]{0,1:T(8,128)(2,1)}, bf16[256,8,64]{0,2,1:T(8,128)(2,1)S(1)}, ...), branch_computations={%region_1.1_spmd, %region_2.0_spmd} | conditional | flops 218698256 | bytes 25744700 | solution.py:300
  672.5 13.2 %conditional.4 = ((f32[32,256,8,64]{1,3,2,0:T(8,128)}, f32[32,256,8]{1,2,0:T(8,128)S(1)})) conditional(s32[]{:T(128)} %convert_element_type.285, (f32[32,256,8,64]{1,3,2,0:T(8,128)}, f32[32,256,8]{1,2,0:T(8,128)S(1)}) %tuple.97, (s32[]{:T(128)}, s32[]{:T(128)}, bf16[8192,512]{0,1:T(8,128)(2,1)}, bf16[256,8,64]{0,2,1:T(8,128)(2,1)S(1)}, ...), branch_computations={%region_1.1_spmd, %region_2.0_spmd} | conditional | flops 218698256 | bytes 25744700 | solution.py:300
  685.7 13.2 %conditional.4 = ((f32[32,256,8,64]{1,3,2,0:T(8,128)}, f32[32,256,8]{1,2,0:T(8,128)S(1)})) conditional(s32[]{:T(128)} %convert_element_type.285, (f32[32,256,8,64]{1,3,2,0:T(8,128)}, f32[32,256,8]{1,2,0:T(8,128)S(1)}) %tuple.97, (s32[]{:T(128)}, s32[]{:T(128)}, bf16[8192,512]{0,1:T(8,128)(2,1)}, bf16[256,8,64]{0,2,1:T(8,128)(2,1)S(1)}, ...), branch_computations={%region_1.1_spmd, %region_2.0_spmd} | conditional | flops 218698256 | bytes 25744700 | solution.py:300
  698.9 13.1 %conditional.4 = ((f32[32,256,8,64]{1,3,2,0:T(8,128)}, f32[32,256,8]{1,2,0:T(8,128)S(1)})) conditional(s32[]{:T(128)} %convert_element_type.285, (f32[32,256,8,64]{1,3,2,0:T(8,128)}, f32[32,256,8]{1,2,0:T(8,128)S(1)}) %tuple.97, (s32[]{:T(128)}, s32[]{:T(128)}, bf16[8192,512]{0,1:T(8,128)(2,1)}, bf16[256,8,64]{0,2,1:T(8,128)(2,1)S(1)}, ...), branch_computations={%region_1.1_spmd, %region_2.0_spmd} | conditional | flops 218698256 | bytes 25744700 | solution.py:300
  712.0 13.1 %conditional.4 = ((f32[32,256,8,64]{1,3,2,0:T(8,128)}, f32[32,256,8]{1,2,0:T(8,128)S(1)})) conditional(s32[]{:T(128)} %convert_element_type.285, (f32[32,256,8,64]{1,3,2,0:T(8,128)}, f32[32,256,8]{1,2,0:T(8,128)S(1)}) %tuple.97, (s32[]{:T(128)}, s32[]{:T(128)}, bf16[8192,512]{0,1:T(8,128)(2,1)}, bf16[256,8,64]{0,2,1:T(8,128)(2,1)S(1)}, ...), branch_computations={%region_1.1_spmd, %region_2.0_spmd} | conditional | flops 218698256 | bytes 25744700 | solution.py:300
  725.1 13.1 %conditional.4 = ((f32[32,256,8,64]{1,3,2,0:T(8,128)}, f32[32,256,8]{1,2,0:T(8,128)S(1)})) conditional(s32[]{:T(128)} %convert_element_type.285, (f32[32,256,8,64]{1,3,2,0:T(8,128)}, f32[32,256,8]{1,2,0:T(8,128)S(1)}) %tuple.97, (s32[]{:T(128)}, s32[]{:T(128)}, bf16[8192,512]{0,1:T(8,128)(2,1)}, bf16[256,8,64]{0,2,1:T(8,128)(2,1)S(1)}, ...), branch_computations={%region_1.1_spmd, %region_2.0_spmd} | conditional | flops 218698256 | bytes 25744700 | solution.py:300
  738.2 13.1 %conditional.4 = ((f32[32,256,8,64]{1,3,2,0:T(8,128)}, f32[32,256,8]{1,2,0:T(8,128)S(1)})) conditional(s32[]{:T(128)} %convert_element_type.285, (f32[32,256,8,64]{1,3,2,0:T(8,128)}, f32[32,256,8]{1,2,0:T(8,128)S(1)}) %tuple.97, (s32[]{:T(128)}, s32[]{:T(128)}, bf16[8192,512]{0,1:T(8,128)(2,1)}, bf16[256,8,64]{0,2,1:T(8,128)(2,1)S(1)}, ...), branch_computations={%region_1.1_spmd, %region_2.0_spmd} | conditional | flops 218698256 | bytes 25744700 | solution.py:300
  751.4 13.1 %conditional.4 = ((f32[32,256,8,64]{1,3,2,0:T(8,128)}, f32[32,256,8]{1,2,0:T(8,128)S(1)})) conditional(s32[]{:T(128)} %convert_element_type.285, (f32[32,256,8,64]{1,3,2,0:T(8,128)}, f32[32,256,8]{1,2,0:T(8,128)S(1)}) %tuple.97, (s32[]{:T(128)}, s32[]{:T(128)}, bf16[8192,512]{0,1:T(8,128)(2,1)}, bf16[256,8,64]{0,2,1:T(8,128)(2,1)S(1)}, ...), branch_computations={%region_1.1_spmd, %region_2.0_spmd} | conditional | flops 218698256 | bytes 25744700 | solution.py:300
  764.5 13.1 %conditional.4 = ((f32[32,256,8,64]{1,3,2,0:T(8,128)}, f32[32,256,8]{1,2,0:T(8,128)S(1)})) conditional(s32[]{:T(128)} %convert_element_type.285, (f32[32,256,8,64]{1,3,2,0:T(8,128)}, f32[32,256,8]{1,2,0:T(8,128)S(1)}) %tuple.97, (s32[]{:T(128)}, s32[]{:T(128)}, bf16[8192,512]{0,1:T(8,128)(2,1)}, bf16[256,8,64]{0,2,1:T(8,128)(2,1)S(1)}, ...), branch_computations={%region_1.1_spmd, %region_2.0_spmd} | conditional | flops 218698256 | bytes 25744700 | solution.py:300
  777.6 13.2 %conditional.4 = ((f32[32,256,8,64]{1,3,2,0:T(8,128)}, f32[32,256,8]{1,2,0:T(8,128)S(1)})) conditional(s32[]{:T(128)} %convert_element_type.285, (f32[32,256,8,64]{1,3,2,0:T(8,128)}, f32[32,256,8]{1,2,0:T(8,128)S(1)}) %tuple.97, (s32[]{:T(128)}, s32[]{:T(128)}, bf16[8192,512]{0,1:T(8,128)(2,1)}, bf16[256,8,64]{0,2,1:T(8,128)(2,1)S(1)}, ...), branch_computations={%region_1.1_spmd, %region_2.0_spmd} | conditional | flops 218698256 | bytes 25744700 | solution.py:300
  790.8 13.2 %conditional.4 = ((f32[32,256,8,64]{1,3,2,0:T(8,128)}, f32[32,256,8]{1,2,0:T(8,128)S(1)})) conditional(s32[]{:T(128)} %convert_element_type.285, (f32[32,256,8,64]{1,3,2,0:T(8,128)}, f32[32,256,8]{1,2,0:T(8,128)S(1)}) %tuple.97, (s32[]{:T(128)}, s32[]{:T(128)}, bf16[8192,512]{0,1:T(8,128)(2,1)}, bf16[256,8,64]{0,2,1:T(8,128)(2,1)S(1)}, ...), branch_computations={%region_1.1_spmd, %region_2.0_spmd} | conditional | flops 218698256 | bytes 25744700 | solution.py:300
  803.9 13.1 %conditional.4 = ((f32[32,256,8,64]{1,3,2,0:T(8,128)}, f32[32,256,8]{1,2,0:T(8,128)S(1)})) conditional(s32[]{:T(128)} %convert_element_type.285, (f32[32,256,8,64]{1,3,2,0:T(8,128)}, f32[32,256,8]{1,2,0:T(8,128)S(1)}) %tuple.97, (s32[]{:T(128)}, s32[]{:T(128)}, bf16[8192,512]{0,1:T(8,128)(2,1)}, bf16[256,8,64]{0,2,1:T(8,128)(2,1)S(1)}, ...), branch_computations={%region_1.1_spmd, %region_2.0_spmd} | conditional | flops 218698256 | bytes 25744700 | solution.py:300
  817.0 13.1 %conditional.4 = ((f32[32,256,8,64]{1,3,2,0:T(8,128)}, f32[32,256,8]{1,2,0:T(8,128)S(1)})) conditional(s32[]{:T(128)} %convert_element_type.285, (f32[32,256,8,64]{1,3,2,0:T(8,128)}, f32[32,256,8]{1,2,0:T(8,128)S(1)}) %tuple.97, (s32[]{:T(128)}, s32[]{:T(128)}, bf16[8192,512]{0,1:T(8,128)(2,1)}, bf16[256,8,64]{0,2,1:T(8,128)(2,1)S(1)}, ...), branch_computations={%region_1.1_spmd, %region_2.0_spmd} | conditional | flops 218698256 | bytes 25744700 | solution.py:300
  830.2 13.2 %conditional.4 = ((f32[32,256,8,64]{1,3,2,0:T(8,128)}, f32[32,256,8]{1,2,0:T(8,128)S(1)})) conditional(s32[]{:T(128)} %convert_element_type.285, (f32[32,256,8,64]{1,3,2,0:T(8,128)}, f32[32,256,8]{1,2,0:T(8,128)S(1)}) %tuple.97, (s32[]{:T(128)}, s32[]{:T(128)}, bf16[8192,512]{0,1:T(8,128)(2,1)}, bf16[256,8,64]{0,2,1:T(8,128)(2,1)S(1)}, ...), branch_computations={%region_1.1_spmd, %region_2.0_spmd} | conditional | flops 218698256 | bytes 25744700 | solution.py:300
  843.3 13.2 %conditional.4 = ((f32[32,256,8,64]{1,3,2,0:T(8,128)}, f32[32,256,8]{1,2,0:T(8,128)S(1)})) conditional(s32[]{:T(128)} %convert_element_type.285, (f32[32,256,8,64]{1,3,2,0:T(8,128)}, f32[32,256,8]{1,2,0:T(8,128)S(1)}) %tuple.97, (s32[]{:T(128)}, s32[]{:T(128)}, bf16[8192,512]{0,1:T(8,128)(2,1)}, bf16[256,8,64]{0,2,1:T(8,128)(2,1)S(1)}, ...), branch_computations={%region_1.1_spmd, %region_2.0_spmd} | conditional | flops 218698256 | bytes 25744700 | solution.py:300
  856.5 13.1 %conditional.4 = ((f32[32,256,8,64]{1,3,2,0:T(8,128)}, f32[32,256,8]{1,2,0:T(8,128)S(1)})) conditional(s32[]{:T(128)} %convert_element_type.285, (f32[32,256,8,64]{1,3,2,0:T(8,128)}, f32[32,256,8]{1,2,0:T(8,128)S(1)}) %tuple.97, (s32[]{:T(128)}, s32[]{:T(128)}, bf16[8192,512]{0,1:T(8,128)(2,1)}, bf16[256,8,64]{0,2,1:T(8,128)(2,1)S(1)}, ...), branch_computations={%region_1.1_spmd, %region_2.0_spmd} | conditional | flops 218698256 | bytes 25744700 | solution.py:300
  869.6 13.1 %conditional.4 = ((f32[32,256,8,64]{1,3,2,0:T(8,128)}, f32[32,256,8]{1,2,0:T(8,128)S(1)})) conditional(s32[]{:T(128)} %convert_element_type.285, (f32[32,256,8,64]{1,3,2,0:T(8,128)}, f32[32,256,8]{1,2,0:T(8,128)S(1)}) %tuple.97, (s32[]{:T(128)}, s32[]{:T(128)}, bf16[8192,512]{0,1:T(8,128)(2,1)}, bf16[256,8,64]{0,2,1:T(8,128)(2,1)S(1)}, ...), branch_computations={%region_1.1_spmd, %region_2.0_spmd} | conditional | flops 218698256 | bytes 25744700 | solution.py:300
  882.7 13.1 %conditional.4 = ((f32[32,256,8,64]{1,3,2,0:T(8,128)}, f32[32,256,8]{1,2,0:T(8,128)S(1)})) conditional(s32[]{:T(128)} %convert_element_type.285, (f32[32,256,8,64]{1,3,2,0:T(8,128)}, f32[32,256,8]{1,2,0:T(8,128)S(1)}) %tuple.97, (s32[]{:T(128)}, s32[]{:T(128)}, bf16[8192,512]{0,1:T(8,128)(2,1)}, bf16[256,8,64]{0,2,1:T(8,128)(2,1)S(1)}, ...), branch_computations={%region_1.1_spmd, %region_2.0_spmd} | conditional | flops 218698256 | bytes 25744700 | solution.py:300
  900.1 8.1 multiply_reduce_fusion
  910.6 5.7 all_to_all.10
  (597 shorter events, 453.3 us)
Async XLA Ops:
  6.5 901.7 %copy-start = (bf16[512,2048]{1,0:T(8,128)(2,1)S(1)}, bf16[512,2048]{1,0:T(8,128)(2,1)}, u32[]{:S(2)}) copy-start(bf16[512,2048]{1,0:T(8,128)(2,1)} %param.38) | copy-start | bytes 6291460
  6.5 3.4 copy-start.14
  6.5 35.9 %all-gather.22.cloned.1.call-start = ((), (), s32[]{:S(2)}) async-start(), calls=%async_computation.6 | async-start | bytes 2621440 | tf_op jit(solution)/shard_map/all_gather | solution.py:233
  7.3 70.5 %all-gather.24.cloned.1.call-start = ((), (), s32[]{:S(2)}) async-start(), calls=%async_computation.7 | async-start | bytes 2621440 | tf_op jit(solution)/shard_map/all_gather | solution.py:234
  8.0 123.0 %all-gather.16.cloned.1.call-start = ((), (), s32[]{:S(2)}) async-start(), calls=%async_computation.3 | async-start | bytes 2621440 | tf_op jit(solution)/shard_map/all_gather | solution.py:231
  8.7 139.3 %all-gather.14.cloned.1.call-start = ((), (), s32[]{:S(2)}) async-start(), calls=%async_computation.2 | async-start | bytes 2621440 | tf_op jit(solution)/shard_map/all_gather | solution.py:230
  9.3 173.8 %all-gather.26.cloned.1.call-start = ((), (), s32[]{:S(2)}) async-start(), calls=%async_computation.8 | async-start | bytes 2621440 | tf_op jit(solution)/shard_map/all_gather | solution.py:232
  10.1 7.1 copy-start.22
  10.1 8.2 copy-start.16
  10.2 8.2 copy-start.19
  11.3 9.9 %copy-start.17 = (bf16[2048,4]{0,1:T(4,128)(2,1)S(1)}, bf16[2048,4]{0,1:T(4,128)(2,1)}, u32[]{:S(2)}) copy-start(bf16[2048,4]{0,1:T(4,128)(2,1)} %param.33) | copy-start | bytes 49156
  11.3 9.9 %copy-start.20 = (f32[4]{0:T(128)S(1)}, f32[4]{0:T(128)}, u32[]{:S(2)}) copy-start(f32[4]{0:T(128)} %param.34) | copy-start | bytes 52
  11.3 7.1 all-to-all-start
  16.5 201.7 %all-gather.20.cloned.1.call-start = ((), (), s32[]{:S(2)}) async-start(), calls=%async_computation.5 | async-start | bytes 2621440 | tf_op jit(solution)/shard_map/all_gather | solution.py:229
  17.1 234.9 %all-gather.28.cloned.1.call-start = ((), (), s32[]{:S(2)}) async-start(), calls=%async_computation.9 | async-start | bytes 1179648 | tf_op jit(solution)/shard_map/all_gather | solution.py:53
  82.7 8.1 copy-start.2
  114.3 2.0 copy-start.8
  114.5 1.8 copy-start.9
  114.7 0.7 copy-start.10
  116.2 174.4 %all-gather.30.cloned.1.call-start = ((), (), s32[]{:S(2)}) async-start(), calls=%async_computation.10 | async-start | bytes 1179648 | tf_op jit(solution)/shard_map/all_gather | solution.py:53
  127.5 0.7 copy-start.7
  128.4 0.7 copy-start.11
  129.2 0.7 copy-start.12
  130.7 302.7 %all-gather.18.cloned.1.call-start = ((), (), s32[]{:S(2)}) async-start(), calls=%async_computation.4 | async-start | bytes 17301504 | tf_op jit(solution)/shard_map/all_gather | solution.py:37
  133.6 18.0 %copy-start.21 = (f32[128]{0:T(128)S(1)}, f32[128]{0:T(128)}, u32[]{:S(2)}) copy-start(f32[128]{0:T(128)} %param.37) | copy-start | bytes 1540
  220.8 3.1 copy-start.3
  252.0 42.2 %copy-start.1 = (bf16[32,128,128]{2,1,0:T(8,128)(2,1)S(1)}, bf16[32,128,128]{2,1,0:T(8,128)(2,1)}, u32[]{:S(2)}) copy-start(bf16[32,128,128]{2,1,0:T(8,128)(2,1)} %all-gather.28.cloned.1.call-done) | copy-start | bytes 3145732
  290.6 3.5 copy-start.13
  295.8 2.7 copy-start.5
  312.3 0.8 copy-start.6
  467.6 7.9 copy-start.15
  467.6 7.9 copy-start.18
  908.2 1.6 copy-start.4
Sparse Core Ops, SparseCore 0:
  9.1 33.2 all-gather.21
  44.3 33.4 all-gather.23
  79.6 33.3 all-gather.15
  114.7 33.3 all-gather.13
  149.7 33.3 all-gather.25
  184.8 33.3 all-gather.19
  219.9 31.9 all-gather.27
  253.8 36.7 all-gather.29
  293.2 140.2 all-gather.17
where the time goes:
time: 927 us; the launch traced here: 924 us
  waiting for transfers between devices  316 us (34%)
  other arithmetic  287 us (31%)
  matrix products  160 us (17%)
  local copies, waits for them, and re-layouts  112 us (12%)
  blocking collectives  27.4 us (3%)
  between operations  13.9 us (1%)
    another operation x64, other arithmetic  164 us
    all_gather x1, waiting for transfers between devices, in_one_piece(): result = lax.all_gather(both, axis, axis=dim, tiled=True)  119 us
    convert_element_type x32, other arithmetic, stick_block(): jnp.where(visible, jnp.exp(jax.nn.log_sigmoid(scores) + beyond), 0.0)  97.4 us
    all_gather x2, waiting for transfers between devices, entering(): lax.all_gather(part.astype(kind), axis)  65.5 us
    dot_general x32, matrix products, stick_block(): jnp.einsum('qhd,khd->hqk', queries, key_rows, preferred_element_type=jnp....  56.7 us
    dot_general x32, matrix products, stick_block(): jnp.einsum('hqk,khd->qhd', weights, value_rows, preferred_element_type=jn...  35.6 us
    dynamic_slice x32, local copies, waits for them, and re-layouts, per_shard(): lax.dynamic_slice_in_dim(value_block, row_begin, token_rows, 0)  34.4 us
    all_gather x1, waiting for transfers between devices, on_device(): lax.all_gather(delta_query_w, 'fs', axis=0, tiled=True)  31.4 us
  transfers between devices with their start and end apart: 10, of which 9 were waited for; matrix products, arithmetic and copies ran while one was open for 9% of the time, Pallas kernels for 0%

commit v1 on v0

--- a/solution.py
+++ b/solution.py
@@ -2,6 +2,8 @@
 import jax.numpy as jnp
 from jax import lax
 from jax.sharding import Mesh
+from jax.experimental import pallas as pl
+from jax.experimental.pallas import tpu as pltpu
 from jax.sharding import PartitionSpec as P
 
 SB_DIM = 64
@@ -181,28 +183,103 @@
     return (joined_map, joined_state)
 
 
-def stick_block(queries, key_rows, value_rows, query_place, key_place, offsets):
-    scale_factor = queries.shape[-1] ** (-0.5)
-    scores = (
-        jnp.einsum("qhd,khd->hqk", queries, key_rows, preferred_element_type=jnp.float32)
-        * scale_factor
-        + offsets[:, None, None]
-    )
-    visible = key_place[None, :] < query_place[:, None]
-    skipped = jnp.where(visible, jax.nn.log_sigmoid(-scores), 0.0)
-    beyond = lax.cumsum(skipped, axis=2, reverse=True) - skipped
-    weights = jnp.where(visible, jnp.exp(jax.nn.log_sigmoid(scores) + beyond), 0.0).astype(
-        jnp.bfloat16
-    )
-    partial_value = jnp.einsum(
-        "hqk,khd->qhd", weights, value_rows, preferred_element_type=jnp.float32
-    )
-    return (partial_value, jnp.sum(skipped, axis=2).T)
-
-
-def stick_combine(partials, totals):
-    beyond = jnp.cumsum(totals[::-1], axis=0)[::-1] - totals
-    return jnp.sum(partials * jnp.exp(beyond)[..., None], axis=0)
+def stick_kernel(offset_ref, query_ref, kv_ref, out_ref, later_ref, rows_ref, acc_ref, beyond_ref):
+    place = lax.axis_index("sp_1")
+    tile = query_ref.shape[2]
+    size = query_ref.shape[1]
+    groups = kv_ref.shape[2] // tile
+    row_at = lax.broadcasted_iota(jnp.int32, (tile, tile), 0)
+    col_at = lax.broadcasted_iota(jnp.int32, (tile, tile), 1)
+    later_ref[...] = jnp.where(row_at > col_at, 1.0, 0.0).astype(jnp.bfloat16)
+    offset = offset_ref[0]
+
+    def key_row(row, blocks, diagonal):
+        queries = rows_ref[...]
+        beyond = None if diagonal else beyond_ref[...]
+        weights = []
+        for k in range(blocks - 1, -1, -1):
+            scores = (
+                jnp.dot(
+                    queries,
+                    kv_ref[row, 0:size, k * tile : (k + 1) * tile],
+                    preferred_element_type=jnp.float32,
+                )
+                + offset
+            )
+            above = jnp.maximum(scores, 0.0)
+            below = scores - above
+            small = jnp.exp(below - above)
+            log_term = jnp.where(small < 2.0**-12, small, jnp.log(1.0 + small))
+            passed = above + log_term
+            exponent = below - log_term
+            if diagonal and k == blocks - 1:
+                visible = col_at < row_at
+                passed = jnp.where(visible, passed, 0.0)
+                exponent = jnp.where(visible, exponent, -jnp.inf)
+            after = jnp.dot(
+                passed.astype(jnp.bfloat16), later_ref[...], preferred_element_type=jnp.float32
+            )
+            exponent = exponent - after
+            if beyond is not None:
+                exponent = exponent - beyond
+            total = after[:, :1] + passed[:, :1]
+            beyond = total if beyond is None else beyond + total
+            weights.append(jnp.exp(exponent).astype(jnp.bfloat16))
+        partial = lax.dot_general(
+            jnp.concatenate(weights[::-1], axis=1),
+            kv_ref[row, size : 2 * size, 0 : blocks * tile],
+            (((1,), (1,)), ((), ())),
+            preferred_element_type=jnp.float32,
+        )
+        beyond_ref[...] = beyond
+        if diagonal:
+            acc_ref[...] = partial
+        else:
+            acc_ref[...] += partial
+
+    def per_query(query_row, unused):
+        rows_ref[...] = (
+            (query_ref[query_row].astype(jnp.float32) * size ** (-0.5)).T.astype(jnp.bfloat16)
+        )
+        for k in range(groups):
+
+            @pl.when(place == k)
+            def _():
+                key_row(query_row, k + 1, True)
+
+        def earlier(step, carried):
+            key_row(query_row - 1 - step, groups, False)
+            return carried
+
+        lax.fori_loop(0, query_row, earlier, 0)
+        out_ref[query_row] = acc_ref[...].T.astype(jnp.bfloat16)
+        return unused
+
+    lax.fori_loop(0, query_ref.shape[0], per_query, 0)
+
+
+def stick_attention(offset, queries, keys_values):
+    rows, size, tile = queries.shape
+    return pl.pallas_call(
+        stick_kernel,
+        out_shape=jax.ShapeDtypeStruct((rows, size, tile), jnp.bfloat16),
+        in_specs=[
+            pl.BlockSpec(memory_space=pltpu.SMEM),
+            pl.BlockSpec(memory_space=pltpu.VMEM),
+            pl.BlockSpec(memory_space=pltpu.VMEM),
+        ],
+        out_specs=pl.BlockSpec(memory_space=pltpu.VMEM),
+        scratch_shapes=[
+            pltpu.VMEM((tile, tile), jnp.bfloat16),
+            pltpu.VMEM((tile, size), jnp.bfloat16),
+            pltpu.VMEM((tile, size), jnp.float32),
+            pltpu.VMEM((tile, 1), jnp.float32),
+        ],
+        name="stick",
+        cost_estimate=pl.CostEstimate(
+            flops=40_000_000_000, bytes_accessed=3_000_000, transcendentals=27_000_000
+        ),
+    )(offset, queries, keys_values)
 
 
 def on_device(
@@ -223,38 +300,59 @@
     sb_out_w,
     delta_out_w,
 ):
-    token_rows = hidden_in.shape[1]
-    local_in = hidden_in.reshape(token_rows, hidden_in.shape[2])
-    gathered = (
-        lax.all_gather(sb_query_w, "fs", axis=0, tiled=True),
-        lax.all_gather(sb_key_w, "fs", axis=0, tiled=True),
-        lax.all_gather(sb_value_w, "fs", axis=0, tiled=True),
-        lax.all_gather(delta_query_w, "fs", axis=0, tiled=True),
-        lax.all_gather(delta_key_w, "fs", axis=0, tiled=True),
-        lax.all_gather(delta_value_w, "fs", axis=0, tiled=True),
-    )
-    in_weights = tuple(gathered) + (decay_w, write_w)
-    portion = gathered_copies(local_in, "tp", 1)
-    projected = tuple(
-        (jnp.dot(portion, weight, preferred_element_type=jnp.float32) for weight in in_weights)
-    )
-    sb_heads = sb_offset.shape[0]
-    delta_heads = decay_log_scale.shape[0]
-    sb_query = projected[0].astype(jnp.bfloat16).reshape(token_rows, sb_heads, SB_DIM)
-    sb_keys = projected[1].astype(jnp.bfloat16)
-    sb_values = projected[2].astype(jnp.bfloat16)
-    shift_rows = decay_shift.reshape(delta_heads, token_rows).T
+    tokens, part = hidden_in.shape[1], hidden_in.shape[2]
+    fs_count = lax.axis_size("fs")
+    sp_count = lax.axis_size(SP)
+    z_count = lax.axis_size("sp_0")
+    mine = lax.axis_index("fs")
+    wide = lax.all_gather(hidden_in.reshape(tokens, part), ("fs", "tp"), axis=0, tiled=False)
+    wide = wide.reshape(fs_count, -1, tokens, part)
+    rows = sb_query_w.shape[0]
+    slab = rows // sp_count
+    first = lax.axis_index(SP) * slab
+    weights = (sb_query_w, sb_key_w, sb_value_w, delta_query_w, delta_key_w, delta_value_w)
+    pieces = jnp.stack([lax.dynamic_slice_in_dim(w, first, slab, 0) for w in weights], axis=1)
+    pieces = pieces.reshape(slab, len(weights), fs_count, -1).transpose(2, 0, 1, 3)
+    pieces = lax.all_to_all(pieces, "fs", 0, 0, tiled=True)
+    pieces = pieces.reshape(fs_count, slab, -1)
+    columns = lax.all_gather(pieces, SP, axis=0, tiled=False)
+    columns = columns.transpose(1, 0, 2, 3).reshape(wide.shape[1], part, -1)
+    gates_w = jnp.concatenate(
+        [lax.dynamic_slice_in_dim(w, mine, 1, 1) for w in (decay_w, write_w)], axis=1
+    ).reshape(wide.shape[1], part, 2)
+    projected = jnp.einsum(
+        "ftnc,tcm->fnm", wide, columns, preferred_element_type=jnp.float32
+    ).astype(jnp.bfloat16)
+    gates = jnp.einsum("ftnc,tcm->mnf", wide, gates_w, preferred_element_type=jnp.float32)
+    width = projected.shape[2] // 2
+    head_pair = sb_offset.shape[0] // fs_count
+    units = (
+        projected[:, :, :width]
+        .reshape(fs_count, tokens, 3, head_pair, SB_DIM)
+        .transpose(0, 3, 2, 4, 1)
+        .reshape(z_count, 3 * SB_DIM, tokens)
+    )
+    arrived = lax.all_to_all(units, "sp_0", 0, 0, tiled=True)
+    keys_values = lax.all_gather(arrived[:, SB_DIM:], "sp_1", axis=2, tiled=True)
+    offset = lax.dynamic_slice_in_dim(
+        sb_offset, head_pair * mine + lax.rem(lax.axis_index("sp_0"), head_pair), 1, 0
+    )
+    sb_out = stick_attention(offset, arrived[:, :SB_DIM], keys_values)
+    dq, dk, dv = (
+        projected[:, :, width + k * GDN_DIM : width + (k + 1) * GDN_DIM]
+        .transpose(1, 0, 2)
+        .reshape(tokens, fs_count * GDN_DIM)
+        for k in range(3)
+    )
+    shift_rows = lax.all_to_all(
+        decay_shift.reshape(decay_log_scale.shape[0], tokens), "fs", 0, 0, tiled=True
+    ).T
+    own_bias = jnp.broadcast_to(lax.dynamic_slice_in_dim(write_bias, mine, 1, 0), (fs_count,))
+    own_scale = jnp.broadcast_to(
+        lax.dynamic_slice_in_dim(decay_log_scale, mine, 1, 0), (fs_count,)
+    )
     queries, key_rows, value_rows, log_decay, strength = delta_inputs(
-        projected[3].astype(jnp.bfloat16),
-        projected[4].astype(jnp.bfloat16),
-        projected[5].astype(jnp.bfloat16),
-        projected[6],
-        projected[7],
-        write_bias,
-        decay_log_scale,
-        shift_rows,
-        delta_heads,
-        GDN_DIM,
+        dq, dk, dv, gates[0], gates[1], own_bias, own_scale, shift_rows, fs_count, GDN_DIM
     )
     prepared = delta_prepare(
         to_blocks(queries, BLOCK),
@@ -264,62 +362,14 @@
         to_blocks(strength, BLOCK),
     )
     identity_map = jnp.broadcast_to(
-        jnp.eye(GDN_DIM, dtype=jnp.float32), (delta_heads, GDN_DIM, GDN_DIM)
-    )
-    empty_state = jnp.zeros((delta_heads, GDN_DIM, GDN_DIM), jnp.float32)
+        jnp.eye(GDN_DIM, dtype=jnp.float32), (fs_count, GDN_DIM, GDN_DIM)
+    )
+    empty_state = jnp.zeros((fs_count, GDN_DIM, GDN_DIM), jnp.float32)
     (local_end, local_map), unused_out = lax.scan(
         transition_step, (empty_state, identity_map), prepared
     )
-    own_first = lax.axis_index(SP) * token_rows
-    query_place = own_first + lax.iota(jnp.int32, token_rows)
-    sp_count = lax.axis_size(SP)
-    slot_out = jnp.zeros((sp_count, token_rows, sb_heads, SB_DIM), jnp.float32)
-    slot_total = jnp.zeros((sp_count, token_rows, sb_heads), jnp.float32)
-
-    def absorb(slot_arrays, address_portion, value_part, shard_first):
-
-        def active(current):
-            partial_value, totals = stick_block(
-                sb_query,
-                address_portion.reshape(token_rows, sb_heads, SB_DIM),
-                value_part.reshape(token_rows, sb_heads, SB_DIM),
-                query_place,
-                shard_first + lax.iota(jnp.int32, token_rows),
-                sb_offset,
-            )
-            slot_index = shard_first // token_rows
-            return (
-                lax.dynamic_update_index_in_dim(current[0], partial_value, slot_index, 0),
-                lax.dynamic_update_index_in_dim(current[1], totals, slot_index, 0),
-            )
-
-        def inactive(current):
-            return current
-
-        usable = jnp.logical_and(shard_first >= 0, shard_first <= own_first)
-        return lax.cond(usable, active, inactive, slot_arrays)
-
-    key_block, value_block = in_one_piece((sb_keys, sb_values), SP, 0, 1)
-
-    def per_shard(shard_number, current):
-        row_begin = shard_number * token_rows
-        return absorb(
-            current,
-            lax.dynamic_slice_in_dim(key_block, row_begin, token_rows, 0),
-            lax.dynamic_slice_in_dim(value_block, row_begin, token_rows, 0),
-            row_begin,
-        )
-
-    slot_arrays = lax.fori_loop(
-        0, key_block.shape[0] // token_rows, per_shard, (slot_out, slot_total)
-    )
     unused_map, incoming = entering(
         (local_map, local_end), SP, compose, (identity_map, empty_state)
-    )
-    sb_mixed = (
-        stick_combine(slot_arrays[0], slot_arrays[1])
-        .astype(jnp.bfloat16)
-        .reshape(token_rows, sb_heads * SB_DIM)
     )
     unused_end, produced_rows = lax.scan(delta_step, incoming, prepared)
     produced_rows = from_blocks(produced_rows)
@@ -328,11 +378,24 @@
         * lax.rsqrt(jnp.mean(produced_rows * produced_rows, axis=-1, keepdims=True) + NORM_EPS)
         * head_gain
     )
-    delta_mixed = normed.astype(jnp.bfloat16).reshape(token_rows, delta_heads * GDN_DIM)
+    delta_mixed = lax.all_to_all(
+        normed.astype(jnp.bfloat16).transpose(1, 0, 2), "fs", 0, 0, tiled=True
+    )
+    sb_back = lax.all_to_all(sb_out, "sp_0", 0, 0, tiled=True)
+    sb_mixed = lax.all_to_all(
+        sb_back.reshape(fs_count, head_pair * SB_DIM, tokens), "fs", 0, 0, tiled=True
+    ).reshape(-1, tokens)
     result = sent_and_summed(
         (
-            jnp.dot(sb_mixed, sb_out_w, preferred_element_type=jnp.float32)
-            + jnp.dot(delta_mixed, delta_out_w, preferred_element_type=jnp.float32)
+            lax.dot_general(
+                sb_mixed, sb_out_w, (((0,), (0,)), ((), ())), preferred_element_type=jnp.float32
+            )
+            + jnp.einsum(
+                "xnd,xdm->nm",
+                delta_mixed,
+                delta_out_w.reshape(fs_count, GDN_DIM, -1),
+                preferred_element_type=jnp.float32,
+            )
         ).astype(jnp.bfloat16),
         "tp",
         0,

time: 927 us -> 397 us (0.43)
  other arithmetic: 287 us -> 9.66 us
  waiting for transfers between devices: 316 us -> 179 us
  matrix products: 160 us -> 53.1 us
  local copies, waits for them, and re-layouts: 112 us -> 20.3 us
  Pallas kernels: 0 us -> 43.3 us
  blocking collectives: 27.4 us -> 51.6 us
  starting transfers between devices: 5.68 us -> 17.7 us
    another operation x97 -> x0, other arithmetic: 172 us -> none
    all_gather x7 -> x3, waiting for transfers between devices: 245 us -> 116 us  [the longest x1 65.7 us: on_device(): columns = lax.all_gather(pieces, SP, axis=0, tiled=False)]
    dot_general x74 -> x4, matrix products: 115 us -> 12.9 us  [the longest x1 6.71 us: on_device(): jnp.einsum('ftnc,tcm->fnm', wide, columns, preferred_element_type=jnp.flo...]
    convert_element_type x32 -> x2, other arithmetic: 97.4 us -> 1.86 us  [the longest x1 0.95 us: delta_inputs(): value_proj.astype(jnp.float32)]
    pallas_call x0 -> x1, Pallas kernels: none -> 43.3 us  [stick_attention(): pl.pallas_call(stick_kernel, out_shape=jax.ShapeDtypeStruct((rows, size,...]
    dynamic_slice x32 -> x7, local copies, waits for them, and re-layouts: 34.4 us -> 4.24 us  [the longest x3 2.37 us: on_device(): lax.dynamic_slice_in_dim(w, first, slab, 0)]
    unnamed x48 -> x51, local copies, waits for them, and re-layouts: 26.5 us -> 1.89 us
    another operation x65 -> x8, local copies, waits for them, and re-layouts: 22.7 us -> 0.87 us  [the longest x1 0.77 us: on_device(): columns = lax.all_gather(pieces, SP, axis=0, tiled=False)]
  transfers between devices with their start and end apart: 10 -> 9, of which waited for: 9 -> 7; matrix products, arithmetic and copies ran while one was open for 9% -> 14% of each run, Pallas kernels for 0% -> 11%
where the time goes in v1:
time: 397 us; the launch traced here: 390 us
  waiting for transfers between devices  179 us (45%)
  matrix products  53.1 us (13%)
  blocking collectives  51.6 us (13%)
  Pallas kernels  43.3 us (11%)
  local copies, waits for them, and re-layouts  20.3 us (5%)
  starting transfers between devices  17.7 us (4%)
  between operations  14.4 us (4%)
  other arithmetic  9.66 us (2%)
    all_gather x1, waiting for transfers between devices, on_device(): columns = lax.all_gather(pieces, SP, axis=0, tiled=False)  65.7 us
    all_gather x2, waiting for transfers between devices, entering(): lax.all_gather(part.astype(kind), axis)  48.5 us
    pallas_call x1, Pallas kernels, stick_attention(): pl.pallas_call(stick_kernel, out_shape=jax.ShapeDtypeStruct((rows, size,...  43.3 us
    all_gather x1, waiting for transfers between devices, on_device(): lax.all_gather(hidden_in.reshape(tokens, part), ('fs', 'tp'), axis=0, til...  36.5 us
    all_gather x2, blocking collectives, entering(): lax.all_gather(part.astype(kind), axis)  20.4 us
    all_gather x1, waiting for transfers between devices, on_device(): lax.all_gather(arrived[:, SB_DIM:], 'sp_1', axis=2, tiled=True)  13.6 us
    all_to_all x1, blocking collectives, on_device(): sb_back = lax.all_to_all(sb_out, 'sp_0', 0, 0, tiled=True)  12.2 us
    all_to_all x1, waiting for transfers between devices, on_device(): arrived = lax.all_to_all(units, 'sp_0', 0, 0, tiled=True)  11 us
  transfers between devices with their start and end apart: 9, of which 7 were waited for; matrix products, arithmetic and copies ran while one was open for 14% of the time, Pallas kernels for 11%

profile of v1, /device:TPU:249, one launch (start us, length us, event | category | flops | bytes accessed | tf_op | source)
XLA Modules:
  0.0 389.9 jit_solution(4907941745325716044)
XLA Ops:
  6.6 0.9 constant_dynamic-slice_fusion.8
  9.2 8.5 %all_to_all.42 = bf16[4,16,6,128]{3,1,2,0:T(8,128)(2,1)S(1)} all-to-all(bf16[4,16,6,128]{3,1,2,0:T(8,128)(2,1)S(1)} %copy.48), channel_id=1, replica_groups=mesh['sp_0'=8,'sp_1'=4,'fs'=4,'tp'=2] {'fs'}, dimensions={0} | all-to-all | bytes 196608 | tf_op jit(solution)/shard_map/all_to_all | solution.py:316
  19.9 3.2 all-to-all-start.4
  25.2 65.7 %all-gather.10.cloned.1.call-done = bf16[32,4,16,768]{3,2,1,0:T(8,128)(2,1)} async-done(((bf16[1,4,16,768]{3,2,1,0:T(8,128)(2,1)}), bf16[32,4,16,768]{3,2,1,0:T(8,128)(2,1)}) %all-gather.10.cloned.1.call-update) | async-done | bytes 3145744 | tf_op jit(solution)/shard_map/all_gather | solution.py:318
  90.9 3.9 %copy.50 = bf16[4,32,16,768]{3,2,1,0:T(8,128)(2,1)} copy(bf16[4,32,16,768]{3,2,0,1:T(8,128)(2,1)} %bitcast.274) | data formatting | bytes 6291456 | tf_op jit(solution)/shard_map/transpose | solution.py:319
  94.9 36.5 %all-gather.12.cloned.1.call-done = bf16[8,256,1024]{2,1,0:T(8,128)(2,1)} async-done(((bf16[1,256,1024]{2,1,0:T(8,128)(2,1)}), bf16[8,256,1024]{2,1,0:T(8,128)(2,1)}) %all-gather.12.cloned.1.call-update) | async-done | bytes 4194320 | tf_op jit(solution)/shard_map/all_gather | solution.py:308
  131.4 6.7 %fusion.48 = bf16[4,256,768]{2,1,0:T(8,128)(2,1)S(1)} fusion(bf16[2,1024,768,1]{2,1,0,3:T(8,128)(2,1)} %bitcast.275, bf16[4,2,256,1024]{3,2,1,0:T(8,128)(2,1)} %bitcast.271), kind=kOutput, calls=%fused_computation.46 | convolution fusion | flops 3222011904 | bytes 8912896 | tf_op jit(solution)/shard_map/ftnc,tcm->fnm/dot_general | solution.py:323
  138.5 1.0 slice_convert_fusion
  139.4 1.2 convolution_bitcast_fusion.1
  141.4 0.9 reduce_window_sum.11
  142.7 2.2 multiply_multiply_fusion.2
  146.7 1.0 convolution_add_fusion.5
  147.8 1.6 convolution_add_fusion.4
  149.9 2.2 fusion.64
  152.3 6.7 %while.26 = (s32[]{:T(128)}, f32[4,128,128]{2,1,0:T(8,128)S(1)}, f32[4,128,128]{2,1,0:T(8,128)S(1)}, f32[4,4]{1,0:T(4,128)S(1)}, bf16[4,4,64,128]{3,2,1,0:T(8,12...) while((s32[]{:T(128)}, f32[4,128,128]{2,1,0:T(8,128)S(1)}, ...), condition=%wide.region_3.4_spmd.clone, body=%wide.region_2.3_spmd.clone.sunk | while | flops 42401792 | bytes 3019402 | solution.py:368
  152.4 1.2 convolution_add_fusion.25
  154.1 1.2 convolution_add_fusion.25
  155.7 1.2 convolution_add_fusion.25
  157.4 1.2 convolution_add_fusion.25
  159.1 9.9 %all-gather = bf16[16,128,128]{2,1,0:T(8,128)(2,1)S(1)} all-gather(bf16[4,128,128]{2,1,0:T(8,128)(2,1)S(1)} %convert_element_type.161), channel_id=2, replica_groups=mesh['sp_0'=8,'sp_1'=4,'fs'=4,'tp'=2] {'sp_1'}, dimensions={0}, use_global_device_ids=true | all-gather | bytes 655360 | tf_op jit(solution)/shard_map/all_gather | solution.py:55
  169.0 10.5 %all-gather.2 = bf16[16,128,128]{2,1,0:T(8,128)(2,1)S(1)} all-gather(bf16[4,128,128]{2,1,0:T(8,128)(2,1)S(1)} %convert_element_type.163), channel_id=4, replica_groups=mesh['sp_0'=8,'sp_1'=4,'fs'=4,'tp'=2] {'sp_1'}, dimensions={0}, use_global_device_ids=true | all-gather | bytes 655360 | tf_op jit(solution)/shard_map/all_gather | solution.py:55
  180.7 0.8 convolution_add_fusion.16
  183.3 0.8 fusion.144
  184.2 1.1 slice-done
  185.3 1.2 copy.51
  186.5 2.2 copy.52
  188.7 6.4 %all-to-all-start.1 = ((bf16[8,192,256]{2,1,0:T(8,128)(2,1)}), bf16[8,192,256]{2,1,0:T(8,128)(2,1)}, u32[]{:S(2)}, u32[]{:S(2)}) async-start(bf16[8,192,256]{2,1,0:T(8,128)(2,1)} %bitcast.276), calls=%async_computation.1 | async-start | bytes 1572864 | tf_op jit(solution)/shard_map/all_to_all | solution.py:335
  195.6 1.9 bitcast_multiply_fusion.1
  197.6 2.0 convolution_multiply_fusion
  199.6 11.0 %all-to-all-done.1 = bf16[8,192,256]{2,1,0:T(8,128)(2,1)} async-done(((bf16[8,192,256]{2,1,0:T(8,128)(2,1)}), bf16[8,192,256]{2,1,0:T(8,128)(2,1)}, u32[]{:S(2)}, u32[]{:S(2)}) %all-to-all-start.1) | async-done | bytes 786464 | tf_op jit(solution)/shard_map/all_to_all | solution.py:335
  210.6 1.9 slice.159
  212.5 1.7 slice.158.query_ref
  214.2 12.6 %all-gather.18.cloned.1.call-done = bf16[32,128,128]{2,1,0:T(8,128)(2,1)} async-done(((bf16[4,128,128]{2,1,0:T(8,128)(2,1)}), bf16[32,128,128]{2,1,0:T(8,128)(2,1)}) %all-gather.18.cloned.1.call-update) | async-done | bytes 1048592 | tf_op jit(solution)/shard_map/all_gather | solution.py:55
  226.8 35.9 %all-gather.16.cloned.1.call-done = bf16[32,128,128]{2,1,0:T(8,128)(2,1)} async-done(((bf16[4,128,128]{2,1,0:T(8,128)(2,1)}), bf16[32,128,128]{2,1,0:T(8,128)(2,1)}) %all-gather.16.cloned.1.call-update) | async-done | bytes 1048592 | tf_op jit(solution)/shard_map/all_gather | solution.py:55
  262.7 1.3 convolution_add_fusion.20
  264.0 1.1 convolution_add_fusion.15
  265.1 1.1 convolution_add_fusion.14
  267.1 0.9 fusion.55
  268.0 2.0 fusion.52
  269.9 1.4 convolution_add_fusion.21
  271.3 13.6 %while.25 = (s32[]{:T(128)}, f32[4,128,128]{2,1,0:T(8,128)S(1)}, f32[4,4,64,128]{3,2,1,0:T(8,128)S(1)}, f32[4,4]{1,0:T(4,128)S(1)}, bf16[4,4,64,128]{3,2,1,0:T(8...) while((s32[]{:T(128)}, f32[4,128,128]{2,1,0:T(8,128)S(1)}, ...), condition=%wide.region_6.7_spmd, body=%wide.region_5.6_spmd.sunk | while | flops 29589504 | bytes 2034829 | solution.py:374
  271.3 1.1 convolution_subtract_fusion.5
  272.4 1.0 fusion.236
  273.4 1.0 fusion.237
  274.7 1.1 convolution_subtract_fusion.5
  275.8 1.0 fusion.236
  276.8 1.0 fusion.237
  278.1 1.1 convolution_subtract_fusion.5
  279.2 1.0 fusion.236
  280.2 1.0 fusion.237
  281.5 1.1 convolution_subtract_fusion.5
  282.6 1.0 fusion.236
  283.6 1.0 fusion.237
  285.3 0.9 fusion.59
  286.2 4.0 %all-to-all-start.5 = ((bf16[4,256,128]{2,1,0:T(8,128)(2,1)}), bf16[4,256,128]{2,1,0:T(8,128)(2,1)S(1)}, u32[]{:S(2)}, u32[]{:S(2)}) async-start(bf16[4,256,128]{2,1,0:T(8,128)(2,1)} %bitcast.43), calls=%async_computation.5 | async-start | bytes 524288 | tf_op jit(solution)/shard_map/all_to_all | solution.py:381
  290.2 13.6 %all-gather.14.cloned.1.call-done.kv_ref = bf16[8,128,1024]{2,1,0:T(8,128)(2,1)} async-done(((bf16[8,128,256]{2,1,0:T(8,128)(2,1)}), bf16[8,128,1024]{2,1,0:T(8,128)(2,1)}) %all-gather.14.cloned.1.call-update) | async-done | bytes 2097168 | tf_op jit(solution)/shard_map/all_gather | solution.py:336
  303.8 43.3 %stick.1 = bf16[8,64,256]{2,1,0:T(8,128)(2,1)} custom-call(f32[1]{0:T(128)} %dynamic_slice.68.offset_ref, bf16[8,64,256]{2,1,0:T(8,128)(2,1)} %slice.158.query_ref, bf16[8,128,1024]{2,1,0:T(8,128)(2,1)} %all-gather.14.cloned.1.call-done.kv_ref), custom_call_target="tpu_custom_call" | custom-call | flops 40000000000 | bytes 3000000 | tf_op jit(solution)/shard_map/stick/pallas_call | solution.py:263
  347.1 12.2 %all_to_all.43 = bf16[8,64,256]{2,1,0:T(8,128)(2,1)} all-to-all(bf16[8,64,256]{2,1,0:T(8,128)(2,1)} %stick.1), channel_id=1, replica_groups=mesh['sp_0'=8,'sp_1'=4,'fs'=4,'tp'=2] {'sp_0'}, dimensions={0} | all-to-all | bytes 524288 | tf_op jit(solution)/shard_map/all_to_all | solution.py:384
  359.3 4.0 %all-to-all-start.3 = ((bf16[4,128,256]{2,1,0:T(8,128)(2,1)}), bf16[4,128,256]{2,1,0:T(8,128)(2,1)S(1)}, u32[]{:S(2)}, u32[]{:S(2)}) async-start(bf16[4,128,256]{2,1,0:T(8,128)(2,1)} %bitcast.18), calls=%async_computation.3 | async-start | bytes 524288 | tf_op jit(solution)/shard_map/all_to_all | solution.py:385
  363.3 2.1 convolution_bitcast_fusion
  365.3 3.4 all-to-all-done.3
  368.8 3.0 fusion.47
  371.7 10.5 %all_to_all.44 = bf16[2,128,2048]{2,1,0:T(8,128)(2,1)S(1)} all-to-all(bf16[2,128,2048]{2,1,0:T(8,128)(2,1)S(1)} %bitcast.273), channel_id=1, replica_groups=mesh['sp_0'=8,'sp_1'=4,'fs'=4,'tp'=2] {'tp'}, dimensions={0} | all-to-all | bytes 2097152 | tf_op jit(solution)/shard_map/all_to_all | solution.py:77
  382.3 1.1 reduce_sum.42
  (151 shorter events, 16.8 us)
Async XLA Ops:
  6.5 356.7 %copy-start = (bf16[512,2048]{1,0:T(8,128)(2,1)S(1)}, bf16[512,2048]{1,0:T(8,128)(2,1)}, u32[]{:S(2)}) copy-start(bf16[512,2048]{1,0:T(8,128)(2,1)} %param.35) | copy-start | bytes 6291460
  6.5 12.7 %copy-start.16 = (f32[1,4,256]{2,1,0:T(4,128)S(1)}, f32[1,4,256]{2,1,0:T(4,128)}, u32[]{:S(2)}) copy-start(f32[1,4,256]{2,1,0:T(4,128)} %param.32) | copy-start | bytes 12292
  6.5 16.6 %copy-start.20 = (f32[4]{0:T(128)S(1)}, f32[4]{0:T(128)}, u32[]{:S(2)}) copy-start(f32[4]{0:T(128)} %param.30) | copy-start | bytes 52
  6.5 17.2 %copy-start.21 = (f32[4]{0:T(128)S(1)}, f32[4]{0:T(128)}, u32[]{:S(2)}) copy-start(f32[4]{0:T(128)} %param.31) | copy-start | bytes 52
  6.5 18.6 %copy-start.18 = (bf16[2048,4]{0,1:T(4,128)(2,1)S(1)}, bf16[2048,4]{0,1:T(4,128)(2,1)}, u32[]{:S(2)}) copy-start(bf16[2048,4]{0,1:T(4,128)(2,1)} %param.28) | copy-start | bytes 49156
  6.5 18.6 %copy-start.17 = (bf16[2048,4]{0,1:T(4,128)(2,1)S(1)}, bf16[2048,4]{0,1:T(4,128)(2,1)}, u32[]{:S(2)}) copy-start(bf16[2048,4]{0,1:T(4,128)(2,1)} %param.29) | copy-start | bytes 49156
  6.6 84.4 %all-gather.10.cloned.1.call-start = ((), (), s32[]{:S(2)}) async-start(), calls=%async_computation.7 | async-start | bytes 3244032 | tf_op jit(solution)/shard_map/all_gather | solution.py:318
  18.5 112.8 %all-gather.12.cloned.1.call-start = ((), (), s32[]{:S(2)}) async-start(), calls=%async_computation.8 | async-start | bytes 4718592 | tf_op jit(solution)/shard_map/all_gather | solution.py:308
  19.9 121.4 %all-to-all-start.4 = ((f32[4,1,256]{2,1,0:T(1,128)}), f32[4,1,256]{2,1,0:T(1,128)S(1)}, u32[]{:S(2)}, u32[]{:S(2)}) async-start(f32[4,1,256]{2,1,0:T(1,128)} %all_to_all.30), calls=%async_computation.4 | async-start | bytes 8192 | tf_op jit(solution)/shard_map/all_to_all | solution.py:347
  23.1 203.7 %all-gather.18.cloned.1.call-start = ((), (), s32[]{:S(2)}) async-start(), calls=%async_computation.11 | async-start | bytes 1179648 | tf_op jit(solution)/shard_map/all_gather | solution.py:55
  131.4 8.1 %copy-start.4 = (bf16[8,256,1024]{2,1,0:T(8,128)(2,1)S(1)}, bf16[8,256,1024]{2,1,0:T(8,128)(2,1)}, u32[]{:S(2)}) copy-start(bf16[8,256,1024]{2,1,0:T(8,128)(2,1)} %all-gather.12.cloned.1.call-done) | copy-start | bytes 12582916
  138.1 2.5 copy-start.5
  144.8 7.2 %copy-start.2 = (f32[256,4,128]{2,0,1:T(8,128)}, f32[256,4,128]{2,0,1:T(8,128)S(1)}, u32[]{:S(2)}) copy-start(f32[256,4,128]{2,0,1:T(8,128)S(1)} %get-tuple-element.152) | copy-start | bytes 1572868
  179.7 2.5 copy-start.7
  179.9 2.3 copy-start.8
  180.1 0.7 copy-start.9
  181.6 81.1 %all-gather.16.cloned.1.call-start = ((), (), s32[]{:S(2)}) async-start(), calls=%async_computation.10 | async-start | bytes 1179648 | tf_op jit(solution)/shard_map/all_gather | solution.py:55
  181.8 0.7 copy-start.10
  182.0 0.7 copy-start.12
  182.7 0.6 copy-start.14
  184.2 1.1 slice-start
  185.3 9.7 %copy-start.22 = (f32[8]{0:T(128)S(1)}, f32[8]{0:T(128)}, u32[]{:S(2)}) copy-start(f32[8]{0:T(128)} %param.24) | copy-start | bytes 100
  186.5 11.1 %copy-start.3 = (f32[256,4,128]{2,0,1:T(8,128)S(1)}, f32[256,4,128]{2,0,1:T(8,128)}, u32[]{:S(2)}) copy-start(f32[256,4,128]{2,0,1:T(8,128)} %copy-done.2) | copy-start | bytes 1572868
  188.7 21.9 %all-to-all-start.1 = ((bf16[8,192,256]{2,1,0:T(8,128)(2,1)}), bf16[8,192,256]{2,1,0:T(8,128)(2,1)}, u32[]{:S(2)}, u32[]{:S(2)}) async-start(bf16[8,192,256]{2,1,0:T(8,128)(2,1)} %bitcast.276), calls=%async_computation.1 | async-start | bytes 1572864 | tf_op jit(solution)/shard_map/all_to_all | solution.py:335
  195.0 108.8 %all-gather.14.cloned.1.call-start = ((), (), s32[]{:S(2)}) async-start(), calls=%async_computation.9 | async-start | bytes 2621440 | tf_op jit(solution)/shard_map/all_gather | solution.py:336
  262.7 3.6 copy-start.1
  262.7 3.6 copy-start.15
  266.5 1.5 copy-start.11
  266.5 1.5 copy-start.13
  267.0 4.3 %copy-start.6 = (f32[4,4,64,128]{3,2,1,0:T(8,128)S(1)}, f32[4,4,64,128]{3,2,1,0:T(8,128)}, u32[]{:S(2)}) copy-start(f32[4,4,64,128]{3,2,1,0:T(8,128)} %custom-call.2) | copy-start | bytes 1572868
  271.3 14.0 %copy-start.19 = (f32[128]{0:T(128)S(1)}, f32[128]{0:T(128)}, u32[]{:S(2)}) copy-start(f32[128]{0:T(128)} %param.33) | copy-start | bytes 1540
  286.2 60.9 %all-to-all-start.5 = ((bf16[4,256,128]{2,1,0:T(8,128)(2,1)}), bf16[4,256,128]{2,1,0:T(8,128)(2,1)S(1)}, u32[]{:S(2)}, u32[]{:S(2)}) async-start(bf16[4,256,128]{2,1,0:T(8,128)(2,1)} %bitcast.43), calls=%async_computation.5 | async-start | bytes 524288 | tf_op jit(solution)/shard_map/all_to_all | solution.py:381
  359.3 9.5 %all-to-all-start.3 = ((bf16[4,128,256]{2,1,0:T(8,128)(2,1)}), bf16[4,128,256]{2,1,0:T(8,128)(2,1)S(1)}, u32[]{:S(2)}, u32[]{:S(2)}) async-start(bf16[4,128,256]{2,1,0:T(8,128)(2,1)} %bitcast.18), calls=%async_computation.3 | async-start | bytes 524288 | tf_op jit(solution)/shard_map/all_to_all | solution.py:385
Sparse Core Ops, SparseCore 0:
  18.6 72.2 all-gather.9
  92.8 38.5 all-gather.11
  181.7 45.0 all-gather.17
  228.4 34.2 all-gather.15
  264.3 39.4 all-gather.13

commit v2 on v1

--- a/solution.py
+++ b/solution.py
@@ -281,6 +281,280 @@
         ),
     )(offset, queries, keys_values)
 
+class Links:
+    def __init__(self, send, recv):
+        self.send, self.recv, self.count, self.sent, self.open = send, recv, 0, 0, []
+
+    def number(self, n=1):
+        self.count += n
+        return self.count - n
+
+    def copy(self, src, dst, k, axis, to):
+        return pltpu.make_async_remote_copy(
+            src_ref=src,
+            dst_ref=dst,
+            send_sem=self.send.at[self.sent],
+            recv_sem=self.recv.at[k],
+            device_id={axis: to},
+            device_id_type=pl.DeviceIdType.MESH,
+        )
+
+    def start(self, src, dst, k, axis, to):
+        made = self.copy(src, dst, k, axis, to)
+        made.start()
+        self.sent += 1
+        self.open.append(made)
+
+    def arrived(self, dst, k, axis):
+        self.copy(dst, dst, k, axis, lax.axis_index(axis)).wait_recv()
+
+    def drain(self):
+        for made in self.open:
+            made.wait_send()
+        self.open = []
+
+
+def greet(peers):
+    barrier = pltpu.get_barrier_semaphore()
+    for axis, to in peers:
+        pl.semaphore_signal(
+            barrier, inc=1, device_id={axis: to}, device_id_type=pl.DeviceIdType.MESH
+        )
+    pl.semaphore_wait(barrier, len(peers))
+
+
+def project_kernel(
+    hidden_ref, gates_ref, q0, k0, v0, q1, k1, v1,
+    query_ref, kv_ref, delta_ref, pre_ref,
+    acts, sb_w, delta_w, units, send, recv, local,
+):
+    z, y, x, t = (lax.axis_index(a) for a in ("sp_0", "sp_1", "fs", "tp"))
+    nz, ny, nx = (lax.axis_size(a) for a in ("sp_0", "sp_1", "fs"))
+    links = Links(send, recv)
+    tokens = hidden_ref.shape[0]
+    half = tokens // 2
+    lanes = q0.shape[1] // nx
+    z_rows, y_rows = q0.shape[0] // nz, q0.shape[0] // ny
+
+    def at(axis, size, by):
+        return lax.rem(lax.axis_index(axis) + by + size, size)
+
+    greet(
+        [("fs", at("fs", nx, d)) for d in range(1, nx)]
+        + [("sp_0", at("sp_0", nz, d)) for d in range(1, nz)]
+        + [("sp_1", at("sp_1", ny, d)) for d in (1, -1)]
+        + [("tp", 1 - t)]
+    )
+    sets = ((q0, k0, v0), sb_w, z * z_rows, z_rows), ((q1, k1, v1), delta_w, y * y_rows, y_rows)
+    width = 3 * lanes
+    first = {}
+    for d in (2, 1, 3):
+        to = at("fs", nx, d)
+        for s, (mats, held, row, size) in enumerate(sets):
+            first[d, s] = links.number()
+            for m, w in enumerate(mats):
+                links.start(
+                    w.at[pl.ds(row, size), pl.ds(to * lanes, lanes)],
+                    held.at[x, pl.ds(row, size), m * lanes : (m + 1) * lanes],
+                    first[d, s], "fs", to,
+                )
+    own = []
+    for s, (mats, held, row, size) in enumerate(sets):
+        for m, w in enumerate(mats):
+            own.append(
+                pltpu.make_async_copy(
+                    w.at[pl.ds(row, size), pl.ds(x * lanes, lanes)],
+                    held.at[x, pl.ds(row, size), m * lanes : (m + 1) * lanes],
+                    local.at[3 * s + m],
+                )
+            )
+            own[-1].start()
+    right, left, other = at("fs", nx, 1), at("fs", nx, -1), 1 - t
+    act = links.number(8)
+    links.start(hidden_ref, acts.at[x, t], act, "fs", right)
+    links.start(hidden_ref, acts.at[x, t], act + 1, "fs", left)
+    links.start(hidden_ref, acts.at[x, t], act + 4, "tp", other)
+    keep = pltpu.make_async_copy(hidden_ref, acts.at[x, t], local.at[6])
+    keep.start()
+    for made in own:
+        made.wait()
+    for d in (1, 3, 2):
+        source = at("fs", nx, -d)
+        for s, (mats, held, row, size) in enumerate(sets):
+            links.arrived(held.at[source, pl.ds(row, size), 0:width], first[d, s], "fs")
+
+    def sb_piece(by, low=0, count=nx):
+        return sb_w.at[low : low + count, pl.ds(at("sp_0", nz, by) * z_rows, z_rows), :]
+
+    def delta_piece(by, low=0, count=nx):
+        rows = pl.ds(at("sp_1", ny, by) * y_rows, y_rows)
+        return delta_w.at[low : low + count, rows, 0:width]
+
+    z_right, z_left = at("sp_0", nz, 1), at("sp_0", nz, -1)
+    y_right, y_left = at("sp_1", ny, 1), at("sp_1", ny, -1)
+    steps = nz // 2
+    zr, zl = links.number(steps), links.number(steps)
+    yr, yl = links.number(2), links.number(2)
+    links.start(sb_piece(0), sb_piece(0), zr, "sp_0", z_right)
+    links.start(sb_piece(0), sb_piece(0), zl, "sp_0", z_left)
+    links.start(delta_piece(0), delta_piece(0), yr, "sp_1", y_right)
+    links.start(delta_piece(0), delta_piece(0), yl, "sp_1", y_left)
+
+    def z_step(s):
+        if s < steps:
+            low, count = (0, nx) if s < steps - 1 else (0, nx // 2)
+            links.arrived(sb_piece(-s), zr + s - 1, "sp_0")
+            links.start(sb_piece(-s, low, count), sb_piece(-s, low, count), zr + s, "sp_0", z_right)
+            low, count = (0, nx) if s < steps - 1 else (nx // 2, nx // 2)
+            links.arrived(sb_piece(s), zl + s - 1, "sp_0")
+            links.start(sb_piece(s, low, count), sb_piece(s, low, count), zl + s, "sp_0", z_left)
+        else:
+            links.arrived(sb_piece(steps, 0, nx // 2), zr + s - 1, "sp_0")
+            links.arrived(sb_piece(steps, nx // 2, nx // 2), zl + s - 1, "sp_0")
+
+    z_step(1)
+    links.arrived(delta_piece(-1), yr, "sp_1")
+    links.start(delta_piece(-1, 0, 2), delta_piece(-1, 0, 2), yr + 1, "sp_1", y_right)
+    links.arrived(delta_piece(1), yl, "sp_1")
+    links.start(delta_piece(1, 2, 2), delta_piece(1, 2, 2), yl + 1, "sp_1", y_left)
+    z_step(2)
+    before, after, far = at("fs", nx, -1), at("fs", nx, 1), at("fs", nx, 2)
+    links.arrived(acts.at[before, t], act, "fs")
+    links.start(acts.at[before, t, 0:half], acts.at[before, t, 0:half], act + 2, "fs", right)
+    links.start(acts.at[before, t], acts.at[before, t], act + 5, "tp", other)
+    links.arrived(acts.at[after, t], act + 1, "fs")
+    links.start(
+        acts.at[after, t, half:tokens], acts.at[after, t, half:tokens], act + 3, "fs", left
+    )
+    links.start(acts.at[after, t], acts.at[after, t], act + 6, "tp", other)
+    z_step(3)
+    delta_w[:, :, width : width + lanes] = gates_ref[...]
+    z_step(4)
+    links.arrived(delta_piece(2, 0, 2), yr + 1, "sp_1")
+    links.arrived(delta_piece(2, 2, 2), yl + 1, "sp_1")
+    links.arrived(acts.at[far, t, 0:half], act + 2, "fs")
+    links.arrived(acts.at[far, t, half:tokens], act + 3, "fs")
+    links.start(acts.at[far, t], acts.at[far, t], act + 7, "tp", other)
+    keep.wait()
+    for k, c in enumerate((x, before, after, far)):
+        links.arrived(acts.at[c, other], act + 4 + k, "tp")
+
+    size = lanes // 2
+    zq, zk = links.number(nz), links.number(nz)
+
+    def product(c, held, cols):
+        return sum(
+            jnp.dot(
+                acts[c, p],
+                held[2 * p : 2 * p + 2, :, cols].reshape(acts.shape[3], -1),
+                preferred_element_type=jnp.float32,
+            )
+            for p in range(2)
+        )
+
+    def sb_sequence(c, carried):
+        for m in range(3):
+            block = product(c, sb_w, slice(m * lanes, (m + 1) * lanes)).T.astype(jnp.bfloat16)
+            units[2 * c, m * size : (m + 1) * size, :] = block[0:size]
+            units[2 * c + 1, m * size : (m + 1) * size, :] = block[size:lanes]
+        return carried
+
+    lax.fori_loop(0, nx, sb_sequence, 0)
+
+    def delta_sequence(c, carried):
+        out = product(c, delta_w, slice(0, width + lanes))
+        delta_ref[c] = out[:, 0:width].astype(jnp.bfloat16)
+        pre_ref[c] = out[:, width : width + lanes]
+        return carried
+
+    delta_sequence(0, 0)
+
+    here = pl.ds(pl.multiple_of(y * tokens, tokens), tokens)
+    for d in (4, 3, 5, 2, 6, 1, 7):
+        to = at("sp_0", nz, d)
+        links.start(units.at[to, 0:size], query_ref.at[z], zq + d, "sp_0", to)
+        links.start(units.at[to, size : 3 * size], kv_ref.at[z, :, here], zk + d, "sp_0", to)
+    mine = (
+        pltpu.make_async_copy(units.at[z, 0:size], query_ref.at[z], local.at[7]),
+        pltpu.make_async_copy(units.at[z, size : 3 * size], kv_ref.at[z, :, here], local.at[8]),
+    )
+    for made in mine:
+        made.start()
+    lax.fori_loop(1, nx, delta_sequence, 0)
+    for made in mine:
+        made.wait()
+    kv_r, kv_l = links.number(nz), links.number(nz)
+    kv_rr, kv_ll = links.number(nz), links.number(nz)
+    order = (0, 1, 7, 2, 6, 3, 5, 4)
+
+    def kv_piece(row, by, low=0, count=2 * size):
+        cols = pl.ds(pl.multiple_of(at("sp_1", ny, by) * tokens, tokens), tokens)
+        return kv_ref.at[row, low : low + count, cols]
+
+    def forward(d):
+        row = at("sp_0", nz, -d)
+        links.arrived(kv_piece(row, -1), kv_r + d, "sp_1")
+        links.start(
+            kv_piece(row, -1, 0, size), kv_piece(row, -1, 0, size), kv_rr + d, "sp_1", y_right
+        )
+        links.arrived(kv_piece(row, 1), kv_l + d, "sp_1")
+        links.start(
+            kv_piece(row, 1, size, size), kv_piece(row, 1, size, size), kv_ll + d, "sp_1", y_left
+        )
+
+    for i, d in enumerate(order):
+        row = at("sp_0", nz, -d)
+        if d:
+            links.arrived(kv_ref.at[row, :, here], zk + d, "sp_0")
+        links.start(kv_piece(row, 0), kv_piece(row, 0), kv_r + d, "sp_1", y_right)
+        links.start(kv_piece(row, 0), kv_piece(row, 0), kv_l + d, "sp_1", y_left)
+        if i >= 2:
+            forward(order[i - 2])
+    for d in order[-2:]:
+        forward(d)
+    for d in order:
+        row = at("sp_0", nz, -d)
+        if d:
+            links.arrived(query_ref.at[row], zq + d, "sp_0")
+        links.arrived(kv_piece(row, 2, 0, size), kv_rr + d, "sp_1")
+        links.arrived(kv_piece(row, 2, size, size), kv_ll + d, "sp_1")
+    links.drain()
+
+
+def project_and_share(hidden, gates, sb_weights, delta_weights):
+    nz, ny, nx = (lax.axis_size(a) for a in ("sp_0", "sp_1", "fs"))
+    tokens, part = hidden.shape
+    rows, lanes = sb_weights[0].shape[0], sb_weights[0].shape[1] // nx
+    size = lanes // 2
+    vmem = pl.BlockSpec(memory_space=pltpu.VMEM)
+    anywhere = pl.BlockSpec(memory_space=pl.ANY)
+    copies = 96
+    return pl.pallas_call(
+        project_kernel,
+        out_shape=(
+            jax.ShapeDtypeStruct((nz, size, tokens), jnp.bfloat16),
+            jax.ShapeDtypeStruct((nz, 2 * size, ny * tokens), jnp.bfloat16),
+            jax.ShapeDtypeStruct((nx, tokens, 3 * lanes), jnp.bfloat16),
+            jax.ShapeDtypeStruct((nx, tokens, lanes), jnp.float32),
+        ),
+        in_specs=[vmem, vmem] + [anywhere] * 6,
+        out_specs=(vmem,) * 4,
+        scratch_shapes=[
+            pltpu.VMEM((nx, 2, tokens, part), jnp.bfloat16),
+            pltpu.VMEM((nx, rows, 3 * lanes), jnp.bfloat16),
+            pltpu.VMEM((nx, rows, 4 * lanes), jnp.bfloat16),
+            pltpu.VMEM((nz, 3 * size, tokens), jnp.bfloat16),
+            pltpu.SemaphoreType.DMA((copies,)),
+            pltpu.SemaphoreType.DMA((copies,)),
+            pltpu.SemaphoreType.DMA((9,)),
+        ],
+        compiler_params=pltpu.CompilerParams(collective_id=0, has_side_effects=True),
+        name="project",
+        cost_estimate=pl.CostEstimate(
+            flops=60_000_000_000, bytes_accessed=10_000_000, transcendentals=0
+        ),
+    )(hidden, gates, *sb_weights, *delta_weights)
+
 
 def on_device(
     hidden_in,
@@ -302,44 +576,25 @@
 ):
     tokens, part = hidden_in.shape[1], hidden_in.shape[2]
     fs_count = lax.axis_size("fs")
-    sp_count = lax.axis_size(SP)
-    z_count = lax.axis_size("sp_0")
     mine = lax.axis_index("fs")
-    wide = lax.all_gather(hidden_in.reshape(tokens, part), ("fs", "tp"), axis=0, tiled=False)
-    wide = wide.reshape(fs_count, -1, tokens, part)
-    rows = sb_query_w.shape[0]
-    slab = rows // sp_count
-    first = lax.axis_index(SP) * slab
-    weights = (sb_query_w, sb_key_w, sb_value_w, delta_query_w, delta_key_w, delta_value_w)
-    pieces = jnp.stack([lax.dynamic_slice_in_dim(w, first, slab, 0) for w in weights], axis=1)
-    pieces = pieces.reshape(slab, len(weights), fs_count, -1).transpose(2, 0, 1, 3)
-    pieces = lax.all_to_all(pieces, "fs", 0, 0, tiled=True)
-    pieces = pieces.reshape(fs_count, slab, -1)
-    columns = lax.all_gather(pieces, SP, axis=0, tiled=False)
-    columns = columns.transpose(1, 0, 2, 3).reshape(wide.shape[1], part, -1)
     gates_w = jnp.concatenate(
         [lax.dynamic_slice_in_dim(w, mine, 1, 1) for w in (decay_w, write_w)], axis=1
-    ).reshape(wide.shape[1], part, 2)
-    projected = jnp.einsum(
-        "ftnc,tcm->fnm", wide, columns, preferred_element_type=jnp.float32
-    ).astype(jnp.bfloat16)
-    gates = jnp.einsum("ftnc,tcm->mnf", wide, gates_w, preferred_element_type=jnp.float32)
-    width = projected.shape[2] // 2
+    )
+    lanes = sb_query_w.shape[1] // fs_count
+    gates_w = jnp.pad(gates_w, ((0, 0), (0, lanes - 2))).reshape(fs_count, -1, lanes)
     head_pair = sb_offset.shape[0] // fs_count
-    units = (
-        projected[:, :, :width]
-        .reshape(fs_count, tokens, 3, head_pair, SB_DIM)
-        .transpose(0, 3, 2, 4, 1)
-        .reshape(z_count, 3 * SB_DIM, tokens)
-    )
-    arrived = lax.all_to_all(units, "sp_0", 0, 0, tiled=True)
-    keys_values = lax.all_gather(arrived[:, SB_DIM:], "sp_1", axis=2, tiled=True)
+    unit_queries, keys_values, delta_proj, gates = project_and_share(
+        hidden_in.reshape(tokens, part),
+        gates_w,
+        (sb_query_w, sb_key_w, sb_value_w),
+        (delta_query_w, delta_key_w, delta_value_w),
+    )
     offset = lax.dynamic_slice_in_dim(
         sb_offset, head_pair * mine + lax.rem(lax.axis_index("sp_0"), head_pair), 1, 0
     )
-    sb_out = stick_attention(offset, arrived[:, :SB_DIM], keys_values)
+    sb_out = stick_attention(offset, unit_queries, keys_values)
     dq, dk, dv = (
-        projected[:, :, width + k * GDN_DIM : width + (k + 1) * GDN_DIM]
+        delta_proj[:, :, k * GDN_DIM : (k + 1) * GDN_DIM]
         .transpose(1, 0, 2)
         .reshape(tokens, fs_count * GDN_DIM)
         for k in range(3)
@@ -352,7 +607,7 @@
         lax.dynamic_slice_in_dim(decay_log_scale, mine, 1, 0), (fs_count,)
     )
     queries, key_rows, value_rows, log_decay, strength = delta_inputs(
-        dq, dk, dv, gates[0], gates[1], own_bias, own_scale, shift_rows, fs_count, GDN_DIM
+        dq, dk, dv, gates[:, :, 0].T, gates[:, :, 1].T, own_bias, own_scale, shift_rows, fs_count, GDN_DIM
     )
     prepared = delta_prepare(
         to_blocks(queries, BLOCK),

time: 397 us -> 283 us (0.71)
  the two profiles are of different devices: /device:TPU:249 before, /device:TPU:1 now
where the time goes in v2:
time: 283 us; the launch traced here: 282 us
  Pallas kernels  123 us (43%)
  matrix products  44.1 us (16%)
  blocking collectives  42.5 us (15%)
  waiting for transfers between devices  23 us (8%)
  between operations  14.6 us (5%)
  starting transfers between devices  13.6 us (5%)
  other arithmetic  10.6 us (4%)
  local copies, waits for them, and re-layouts  9.98 us (4%)
    pallas_call x1, Pallas kernels, project_and_share(): pl.pallas_call(project_kernel, out_shape=(jax.ShapeDtypeStruct((nz, size,...  85.8 us
    pallas_call x1, Pallas kernels, stick_attention(): pl.pallas_call(stick_kernel, out_shape=jax.ShapeDtypeStruct((rows, size,...  37.6 us
    all_gather x2, blocking collectives, entering(): lax.all_gather(part.astype(kind), axis)  20.8 us
    all_gather x2, waiting for transfers between devices, entering(): lax.all_gather(part.astype(kind), axis)  19.5 us
    all_to_all x1, blocking collectives, sent_and_summed(): lax.all_to_all(tiles, axis, split_axis=0, concat_axis=0, tiled=True)  12.1 us
    all_to_all x1, blocking collectives, on_device(): lax.all_to_all(normed.astype(jnp.bfloat16).transpose(1, 0, 2), 'fs', 0, 0...  9.66 us
    dot_general x14, matrix products, compose(): jnp.einsum('djo,dog->djg', following_blocks[0], prior_blocks[1])  7.99 us
  transfers between devices with their start and end apart: 5, of which 2 were waited for; matrix products, arithmetic and copies ran while one was open for 13% of the time, Pallas kernels for 44%

profile of v2, /device:TPU:1, one launch (start us, length us, event | category | flops | bytes accessed | tf_op | source)
XLA Modules:
  0.0 282.1 jit_solution(6073513856611401963)
XLA Ops:
  6.5 1.4 all_to_all.22
  8.0 4.8 %all-to-all-start.2 = ((f32[4,1,256]{2,1,0:T(1,128)}), f32[4,1,256]{2,1,0:T(1,128)S(1)}, u32[]{:S(2)}, u32[]{:S(2)}) async-start(f32[4,1,256]{2,1,0:T(1,128)} %all_to_all.22), calls=%async_computation.2 | async-start | bytes 8192 | tf_op jit(solution)/shard_map/all_to_all | solution.py:602
  12.8 0.8 constant_dynamic-slice_fusion.2
  13.9 0.9 pad.4.clone
  14.8 85.8 %project.1 = (bf16[8,64,256]{2,1,0:T(8,128)(2,1)}, bf16[8,128,1024]{2,1,0:T(8,128)(2,1)}, bf16[4,256,384]{2,1,0:T(8,128)(2,1)}, f32[4,256,128]{2,1,0:T(8,128)}) custom-call(bf16[256,1024]{1,0:T(8,128)(2,1)} %bitcast.256, bf16[4,512,128]{2,1,0:T(8,128)(2,1)} %bitcast.252, bf16[512,512]{1,0:T(8,128)(2,1)} %q0.1, bf16[512,512]{1,0:T(8,128)(2,1)} %k0.1, ...), custom_call_target="tpu_custom_call" | custom-call | flops 60000002048 | bytes 10000000 | tf_op jit(solution)/shard_map/project/pallas_call | solution.py:532
  100.6 1.5 multiply_reduce_fusion.1
  102.1 1.8 slice_convert_fusion
  103.9 0.6 dynamic_slice.54
  104.5 2.4 fusion.77
  106.9 1.1 multiply_multiply_fusion.2
  108.0 0.7 dynamic_slice.53
  109.6 0.9 reduce_window_sum.11
  112.9 1.0 convolution_add_fusion.5
  114.0 2.3 convolution_add_fusion.4
  116.2 1.5 fusion.56
  117.7 2.3 fusion.63
  120.0 6.7 %while.26 = (s32[]{:T(128)}, f32[4,128,128]{2,1,0:T(8,128)S(1)}, f32[4,128,128]{2,1,0:T(8,128)S(1)}, f32[4,4]{1,0:T(4,128)S(1)}, bf16[4,4,64,128]{3,2,1,0:T(8,12...) while((s32[]{:T(128)}, f32[4,128,128]{2,1,0:T(8,128)S(1)}, ...), condition=%wide.region_3.4_spmd.clone, body=%wide.region_2.3_spmd.clone.sunk | while | flops 42401792 | bytes 3019410 | solution.py:623
  120.1 0.4 convolution_subtract_fusion.6
  120.4 1.2 convolution_add_fusion.25
  121.8 0.4 convolution_subtract_fusion.6
  122.1 1.2 convolution_add_fusion.25
  123.8 1.2 convolution_add_fusion.25
  125.5 1.2 convolution_add_fusion.25
  126.8 9.9 %all-gather = bf16[16,128,128]{2,1,0:T(8,128)(2,1)S(1)} all-gather(bf16[4,128,128]{2,1,0:T(8,128)(2,1)S(1)} %convert_element_type.155), channel_id=2, replica_groups=mesh['sp_0'=8,'sp_1'=4,'fs'=4,'tp'=2] {'sp_1'}, dimensions={0}, use_global_device_ids=true | all-gather | bytes 655360 | tf_op jit(solution)/shard_map/all_gather | solution.py:55
  136.9 0.7 copy-done.9
  137.7 0.6 copy-done.10
  138.6 0.7 copy-done.11
  139.2 0.8 fusion.139
  140.1 0.6 dynamic_slice.50.offset_ref
  140.8 10.9 %all-gather.2 = bf16[16,128,128]{2,1,0:T(8,128)(2,1)S(1)} all-gather(bf16[4,128,128]{2,1,0:T(8,128)(2,1)S(1)} %convert_element_type.157), channel_id=4, replica_groups=mesh['sp_0'=8,'sp_1'=4,'fs'=4,'tp'=2] {'sp_1'}, dimensions={0}, use_global_device_ids=true | all-gather | bytes 655360 | tf_op jit(solution)/shard_map/all_gather | solution.py:55
  151.9 0.6 copy-done.8
  152.7 0.6 copy-done.12
  153.6 0.6 copy-done.13
  154.2 0.8 convolution_add_fusion.16
  155.1 37.6 %stick.1 = bf16[8,64,256]{2,1,0:T(8,128)(2,1)} custom-call(f32[1]{0:T(128)} %dynamic_slice.50.offset_ref, bf16[8,64,256]{2,1,0:T(8,128)(2,1)} %get-tuple-element.94.query_ref, bf16[8,128,1024]{2,1,0:T(8,128)(2,1)} %get-tuple-element.95.kv_ref), custom_call_target="tpu_custom_call" | custom-call | flops 40000000000 | bytes 3000000 | tf_op jit(solution)/shard_map/stick/pallas_call | solution.py:263
  192.7 5.3 %all-to-all-start = ((bf16[8,64,256]{2,1,0:T(8,128)(2,1)}), bf16[8,64,256]{2,1,0:T(8,128)(2,1)}, u32[]{:S(2)}, u32[]{:S(2)}) async-start(bf16[8,64,256]{2,1,0:T(8,128)(2,1)} %stick.1), calls=%async_computation | async-start | bytes 524288 | tf_op jit(solution)/shard_map/all_to_all | solution.py:639
  198.0 0.9 bitcast_multiply_fusion.1
  198.9 1.0 convolution_multiply_fusion
  199.9 19.5 %all-gather.9.cloned.1.call-done = bf16[32,128,128]{2,1,0:T(8,128)(2,1)} async-done(((bf16[4,128,128]{2,1,0:T(8,128)(2,1)}), bf16[32,128,128]{2,1,0:T(8,128)(2,1)}) %all-gather.9.cloned.1.call-update) | async-done | bytes 1048592 | tf_op jit(solution)/shard_map/all_gather | solution.py:55
  219.4 1.2 convolution_add_fusion.20
  220.6 1.1 convolution_add_fusion.15
  221.8 1.1 convolution_add_fusion.14
  223.7 0.9 fusion.54
  224.6 1.3 fusion.51
  226.1 13.8 %while.25 = (s32[]{:T(128)}, f32[4,128,128]{2,1,0:T(8,128)S(1)}, f32[4,4,64,128]{3,2,1,0:T(8,128)S(1)}, f32[4,4]{1,0:T(4,128)S(1)}, bf16[4,4,64,128]{3,2,1,0:T(8...) while((s32[]{:T(128)}, f32[4,128,128]{2,1,0:T(8,128)S(1)}, ...), condition=%wide.region_6.7_spmd, body=%wide.region_5.6_spmd.sunk | while | flops 29589504 | bytes 2034329 | solution.py:629
  226.2 1.1 convolution_subtract_fusion.5
  227.3 1.0 fusion.227
  228.3 1.0 fusion.228
  229.6 1.1 convolution_subtract_fusion.5
  230.7 1.0 fusion.227
  231.7 1.0 fusion.228
  233.1 1.1 convolution_subtract_fusion.5
  234.2 1.0 fusion.227
  235.2 1.0 fusion.228
  236.5 1.1 convolution_subtract_fusion.5
  237.6 1.0 fusion.227
  238.6 1.0 fusion.228
  240.5 9.7 %all_to_all.32 = bf16[4,256,128]{2,1,0:T(8,128)(2,1)S(1)} all-to-all(bf16[4,256,128]{2,1,0:T(8,128)(2,1)S(1)} %bitcast.249), channel_id=1, replica_groups=mesh['sp_0'=8,'sp_1'=4,'fs'=4,'tp'=2] {'fs'}, dimensions={0} | all-to-all | bytes 524288 | tf_op jit(solution)/shard_map/all_to_all | solution.py:636
  250.2 3.4 %all-to-all-start.1 = ((bf16[4,128,256]{2,1,0:T(8,128)(2,1)}), bf16[4,128,256]{2,1,0:T(8,128)(2,1)S(1)}, u32[]{:S(2)}, u32[]{:S(2)}) async-start(bf16[4,128,256]{2,1,0:T(8,128)(2,1)} %bitcast.9), calls=%async_computation.1 | async-start | bytes 524288 | tf_op jit(solution)/shard_map/all_to_all | solution.py:640
  253.6 2.0 convolution_bitcast_fusion
  255.6 3.4 %all-to-all-done.1 = bf16[4,128,256]{2,1,0:T(8,128)(2,1)S(1)} async-done(((bf16[4,128,256]{2,1,0:T(8,128)(2,1)}), bf16[4,128,256]{2,1,0:T(8,128)(2,1)S(1)}, u32[]{:S(2)}, u32[]{:S(2)}) %all-to-all-start.1) | async-done | bytes 262176 | tf_op jit(solution)/shard_map/all_to_all | solution.py:640
  259.1 3.0 %fusion.47 = bf16[256,2048]{1,0:T(8,128)(2,1)S(1)} fusion(f32[256,2048]{1,0:T(8,128)} %convolution_bitcast_fusion, bf16[512,256]{1,0:T(8,128)(2,1)S(1)} %bitcast.250, bf16[512,2048]{1,0:T(8,128)(2,1)} %param.34), kind=kOutput, calls=%fused_computation.44 | convolution fusion | flops 537919488 | bytes 5505024 | tf_op jit(solution)/shard_map/dot_general | solution.py:645
  262.0 12.1 %all_to_all.33 = bf16[2,128,2048]{2,1,0:T(8,128)(2,1)S(1)} all-to-all(bf16[2,128,2048]{2,1,0:T(8,128)(2,1)S(1)} %bitcast.245), channel_id=1, replica_groups=mesh['sp_0'=8,'sp_1'=4,'fs'=4,'tp'=2] {'tp'}, dimensions={0} | all-to-all | bytes 2097152 | tf_op jit(solution)/shard_map/all_to_all | solution.py:77
  274.1 1.1 reduce_sum.42
  (107 shorter events, 7.8 us)
Async XLA Ops:
  6.5 247.1 %copy-start = (bf16[512,2048]{1,0:T(8,128)(2,1)S(1)}, bf16[512,2048]{1,0:T(8,128)(2,1)}, u32[]{:S(2)}) copy-start(bf16[512,2048]{1,0:T(8,128)(2,1)} %param.35) | copy-start | bytes 6291460
  8.0 101.5 %all-to-all-start.2 = ((f32[4,1,256]{2,1,0:T(1,128)}), f32[4,1,256]{2,1,0:T(1,128)S(1)}, u32[]{:S(2)}, u32[]{:S(2)}) async-start(f32[4,1,256]{2,1,0:T(1,128)} %all_to_all.22), calls=%async_computation.2 | async-start | bytes 8192 | tf_op jit(solution)/shard_map/all_to_all | solution.py:602
  12.8 187.1 %all-gather.7.cloned.1.call-start = ((), (), s32[]{:S(2)}) async-start(), calls=%async_computation.5 | async-start | bytes 1179648 | tf_op jit(solution)/shard_map/all_gather | solution.py:55
  14.8 89.0 %copy-start.16 = (f32[4]{0:T(128)S(1)}, f32[4]{0:T(128)}, u32[]{:S(2)}) copy-start(f32[4]{0:T(128)} %param.30) | copy-start | bytes 52
  100.6 6.3 %copy-start.5 = (bf16[4,256,384]{2,1,0:T(8,128)(2,1)S(1)}, bf16[4,256,384]{2,1,0:T(8,128)(2,1)}, u32[]{:S(2)}) copy-start(bf16[4,256,384]{2,1,0:T(8,128)(2,1)} %get-tuple-element.97) | copy-start | bytes 2359300
  100.6 7.4 %copy-start.17 = (f32[4]{0:T(128)S(1)}, f32[4]{0:T(128)}, u32[]{:S(2)}) copy-start(f32[4]{0:T(128)} %param.31) | copy-start | bytes 52
  108.0 8.3 %copy-start.3 = (f32[256,4,128]{2,0,1:T(8,128)}, f32[256,4,128]{2,0,1:T(8,128)S(1)}, u32[]{:S(2)}) copy-start(f32[256,4,128]{2,0,1:T(8,128)S(1)} %get-tuple-element.162) | copy-start | bytes 1572868
  126.7 25.0 %copy-start.2 = (bf16[4,4,64,128]{3,2,1,0:T(8,128)(2,1)}, bf16[4,4,64,128]{3,2,1,0:T(8,128)(2,1)S(1)}, u32[]{:S(2)}) copy-start(bf16[4,4,64,128]{3,2,1,0:T(8,128)(2,1)S(1)} %get-tuple-element.328) | copy-start | bytes 786436
  126.7 13.4 %copy-start.18 = (f32[8]{0:T(128)S(1)}, f32[8]{0:T(128)}, u32[]{:S(2)}) copy-start(f32[8]{0:T(128)} %param.24) | copy-start | bytes 100
  136.9 0.7 copy-start.9
  137.7 0.7 copy-start.10
  138.5 0.7 copy-start.11
  140.1 79.3 %all-gather.9.cloned.1.call-start = ((), (), s32[]{:S(2)}) async-start(), calls=%async_computation.6 | async-start | bytes 1179648 | tf_op jit(solution)/shard_map/all_gather | solution.py:55
  151.9 0.7 copy-start.8
  152.7 0.7 copy-start.12
  153.6 0.7 copy-start.13
  155.1 42.9 %copy-start.6 = (f32[256,4,128]{2,0,1:T(8,128)S(1)}, f32[256,4,128]{2,0,1:T(8,128)}, u32[]{:S(2)}) copy-start(f32[256,4,128]{2,0,1:T(8,128)} %get-tuple-element.161) | copy-start | bytes 1572868
  155.1 43.8 %copy-start.4 = (f32[256,4,128]{2,0,1:T(8,128)S(1)}, f32[256,4,128]{2,0,1:T(8,128)}, u32[]{:S(2)}) copy-start(f32[256,4,128]{2,0,1:T(8,128)} %copy-done.3) | copy-start | bytes 1572868
  192.7 47.8 %all-to-all-start = ((bf16[8,64,256]{2,1,0:T(8,128)(2,1)}), bf16[8,64,256]{2,1,0:T(8,128)(2,1)}, u32[]{:S(2)}, u32[]{:S(2)}) async-start(bf16[8,64,256]{2,1,0:T(8,128)(2,1)} %stick.1), calls=%async_computation | async-start | bytes 524288 | tf_op jit(solution)/shard_map/all_to_all | solution.py:639
  199.9 23.0 %copy-start.1 = (bf16[32,128,128]{2,1,0:T(8,128)(2,1)S(1)}, bf16[32,128,128]{2,1,0:T(8,128)(2,1)}, u32[]{:S(2)}) copy-start(bf16[32,128,128]{2,1,0:T(8,128)(2,1)} %all-gather.7.cloned.1.call-done) | copy-start | bytes 3145732
  219.4 3.5 %copy-start.14 = (bf16[32,128,128]{2,1,0:T(8,128)(2,1)S(1)}, bf16[32,128,128]{2,1,0:T(8,128)(2,1)}, u32[]{:S(2)}) copy-start(bf16[32,128,128]{2,1,0:T(8,128)(2,1)} %all-gather.9.cloned.1.call-done) | copy-start | bytes 3145732
  224.6 1.5 copy-start.7
  226.1 14.2 %copy-start.15 = (f32[128]{0:T(128)S(1)}, f32[128]{0:T(128)}, u32[]{:S(2)}) copy-start(f32[128]{0:T(128)} %param.33) | copy-start | bytes 1540
  250.2 8.9 %all-to-all-start.1 = ((bf16[4,128,256]{2,1,0:T(8,128)(2,1)}), bf16[4,128,256]{2,1,0:T(8,128)(2,1)S(1)}, u32[]{:S(2)}, u32[]{:S(2)}) async-start(bf16[4,128,256]{2,1,0:T(8,128)(2,1)} %bitcast.9), calls=%async_computation.1 | async-start | bytes 524288 | tf_op jit(solution)/shard_map/all_to_all | solution.py:640
Sparse Core Ops, SparseCore 0:
  140.2 38.4 all-gather.6
  180.5 38.8 all-gather.8

commit v3 on v2

v3 whole, which is shorter than its diff:
```python
import jax
import jax.numpy as jnp
from jax import lax
from jax.experimental import pallas as pl
from jax.experimental.pallas import tpu as pltpu
from jax.sharding import Mesh
from jax.sharding import PartitionSpec as P

SB_DIM = 64
GDN_DIM = 128
BLOCK = 64
SP = ("sp_0", "sp_1")
SP_TP = ("sp_0", "sp_1", "tp")
NORM_EPS = 1e-06


def unit_rows(vectors):
    return vectors * lax.rsqrt(jnp.sum(vectors * vectors, axis=-1, keepdims=True) + NORM_EPS)


class Links:
    def __init__(self, send, recv, me):
        self.me = me
        self.send, self.recv, self.count, self.sent, self.open = send, recv, 0, 0, []

    def number(self, n=1):
        self.count += n
        return self.count - n

    def copy(self, src, dst, k, axis, to):
        return pltpu.make_async_remote_copy(
            src_ref=src,
            dst_ref=dst,
            send_sem=self.send.at[self.sent],
            recv_sem=self.recv.at[k],
            device_id={axis: to},
            device_id_type=pl.DeviceIdType.MESH,
        )

    def start(self, src, dst, k, axis, to, like=None):
        made = self.copy(src, dst, k, axis, to)
        made.start()
        self.open.append((made, self.sent, like, axis))
        self.sent += 1

    def arrived(self, dst, k, axis):
        self.copy(dst, dst, k, axis, self.me[axis]).wait_recv()

    def drain(self):
        for made, sent, like, axis in self.open:
            if like is not None:
                self.sent = sent
                made = self.copy(like(), like(), 0, axis, self.me[axis])
            made.wait_send()
        self.open = []


def greet(peers):
    barrier = pltpu.get_barrier_semaphore()
    for axis, to in peers:
        pl.semaphore_signal(
            barrier, inc=1, device_id={axis: to}, device_id_type=pl.DeviceIdType.MESH
        )
    pl.semaphore_wait(barrier, len(peers))


def project_kernel(
    hidden_ref, gates_ref, shift_in, q0, k0, v0, q1, k1, v1,
    query_ref, kv_ref, delta_ref, pre_ref, shift_ref,
    acts, sb_w, delta_w, units, send, recv, local,
):
    z, y, x, t = (lax.axis_index(a) for a in ("sp_0", "sp_1", "fs", "tp"))
    nz, ny, nx = (lax.axis_size(a) for a in ("sp_0", "sp_1", "fs"))
    me = {"sp_0": z, "sp_1": y, "fs": x, "tp": t}
    links = Links(send, recv, me)
    tokens = hidden_ref.shape[0]
    half = tokens // 2
    lanes = q0.shape[1] // nx
    z_rows, y_rows = q0.shape[0] // nz, q0.shape[0] // ny

    def at(axis, size, by):
        return lax.rem(me[axis] + by + size, size)

    greet(
        [("fs", at("fs", nx, d)) for d in range(1, nx)]
        + [("sp_0", at("sp_0", nz, d)) for d in range(1, nz)]
        + [("sp_1", at("sp_1", ny, d)) for d in (1, -1)]
        + [("tp", 1 - t)]
    )
    sets = ((q0, k0, v0), sb_w, z * z_rows, z_rows), ((q1, k1, v1), delta_w, y * y_rows, y_rows)
    width = 3 * lanes
    first = {}
    for d in (2, 1, 3):
        to = at("fs", nx, d)
        for s, (mats, held, row, size) in enumerate(sets):
            first[d, s] = links.number()
            for m, w in enumerate(mats):
                links.start(
                    w.at[pl.ds(row, size), pl.ds(to * lanes, lanes)],
                    held.at[x, pl.ds(row, size), m * lanes : (m + 1) * lanes],
                    first[d, s], "fs", to,
                )
    own = []
    for s, (mats, held, row, size) in enumerate(sets):
        for m, w in enumerate(mats):
            own.append(
                pltpu.make_async_copy(
                    w.at[pl.ds(row, size), pl.ds(x * lanes, lanes)],
                    held.at[x, pl.ds(row, size), m * lanes : (m + 1) * lanes],
                    local.at[3 * s + m],
                )
            )
            own[-1].start()
    shifts = links.number(nx)
    for d in range(1, nx):
        links.start(shift_in.at[at("fs", nx, d)], shift_ref.at[x], shifts + d, "fs", at("fs", nx, d))
    own.append(pltpu.make_async_copy(shift_in.at[x], shift_ref.at[x], local.at[9]))
    own[-1].start()
    right, left, other = at("fs", nx, 1), at("fs", nx, -1), 1 - t
    act = links.number(8)
    links.start(hidden_ref, acts.at[x, t], act, "fs", right)
    links.start(hidden_ref, acts.at[x, t], act + 1, "fs", left)
    links.start(hidden_ref, acts.at[x, t], act + 4, "tp", other)
    keep = pltpu.make_async_copy(hidden_ref, acts.at[x, t], local.at[6])
    keep.start()
    for made in own:
        made.wait()
    for d in (1, 3, 2):
        source = at("fs", nx, -d)
        for s, (mats, held, row, size) in enumerate(sets):
            links.arrived(held.at[source, pl.ds(row, size), 0:width], first[d, s], "fs")

    def sb_piece(by, low=0, count=nx):
        return sb_w.at[low : low + count, pl.ds(at("sp_0", nz, by) * z_rows, z_rows), :]

    def delta_piece(by, low=0, count=nx):
        rows = pl.ds(at("sp_1", ny, by) * y_rows, y_rows)
        return delta_w.at[low : low + count, rows, 0:width]

    z_right, z_left = at("sp_0", nz, 1), at("sp_0", nz, -1)
    y_right, y_left = at("sp_1", ny, 1), at("sp_1", ny, -1)
    steps = nz // 2
    zr, zl = links.number(steps), links.number(steps)
    yr, yl = links.number(2), links.number(2)
    links.start(sb_piece(0), sb_piece(0), zr, "sp_0", z_right)
    links.start(sb_piece(0), sb_piece(0), zl, "sp_0", z_left)
    links.start(delta_piece(0), delta_piece(0), yr, "sp_1", y_right)
    links.start(delta_piece(0), delta_piece(0), yl, "sp_1", y_left)

    def z_step(s):
        if s < steps:
            low, count = (0, nx) if s < steps - 1 else (0, nx // 2)
            links.arrived(sb_piece(-s), zr + s - 1, "sp_0")
            links.start(sb_piece(-s, low, count), sb_piece(-s, low, count), zr + s, "sp_0", z_right)
            low, count = (0, nx) if s < steps - 1 else (nx // 2, nx // 2)
            links.arrived(sb_piece(s), zl + s - 1, "sp_0")
            links.start(sb_piece(s, low, count), sb_piece(s, low, count), zl + s, "sp_0", z_left)
        else:
            links.arrived(sb_piece(steps, 0, nx // 2), zr + s - 1, "sp_0")
            links.arrived(sb_piece(steps, nx // 2, nx // 2), zl + s - 1, "sp_0")

    z_step(1)
    links.arrived(delta_piece(-1), yr, "sp_1")
    links.start(delta_piece(-1, 0, 2), delta_piece(-1, 0, 2), yr + 1, "sp_1", y_right)
    links.arrived(delta_piece(1), yl, "sp_1")
    links.start(delta_piece(1, 2, 2), delta_piece(1, 2, 2), yl + 1, "sp_1", y_left)
    z_step(2)
    before, after, far = at("fs", nx, -1), at("fs", nx, 1), at("fs", nx, 2)
    links.arrived(acts.at[before, t], act, "fs")
    links.start(acts.at[before, t, 0:half], acts.at[before, t, 0:half], act + 2, "fs", right)
    links.start(acts.at[before, t], acts.at[before, t], act + 5, "tp", other)
    links.arrived(acts.at[after, t], act + 1, "fs")
    links.start(
        acts.at[after, t, half:tokens], acts.at[after, t, half:tokens], act + 3, "fs", left
    )
    links.start(acts.at[after, t], acts.at[after, t], act + 6, "tp", other)
    z_step(3)
    delta_w[:, :, width : width + lanes] = gates_ref[...]
    z_step(4)
    links.arrived(delta_piece(2, 0, 2), yr + 1, "sp_1")
    links.arrived(delta_piece(2, 2, 2), yl + 1, "sp_1")
    links.arrived(acts.at[far, t, 0:half], act + 2, "fs")
    links.arrived(acts.at[far, t, half:tokens], act + 3, "fs")
    links.start(acts.at[far, t], acts.at[far, t], act + 7, "tp", other)
    keep.wait()
    for k, c in enumerate((x, before, after, far)):
        links.arrived(acts.at[c, other], act + 4 + k, "tp")

    size = lanes // 2
    zq, zk = links.number(nz), links.number(nz)

    def product(c, held, cols):
        return sum(
            jnp.dot(
                acts[c, p],
                held[2 * p : 2 * p + 2, :, cols].reshape(acts.shape[3], -1),
                preferred_element_type=jnp.float32,
            )
            for p in range(2)
        )

    def sb_sequence(c, carried):
        for m in range(3):
            block = product(c, sb_w, slice(m * lanes, (m + 1) * lanes)).T.astype(jnp.bfloat16)
            units[2 * c, m * size : (m + 1) * size, :] = block[0:size]
            units[2 * c + 1, m * size : (m + 1) * size, :] = block[size:lanes]
        return carried

    lax.fori_loop(0, nx, sb_sequence, 0)

    def delta_sequence(c, carried):
        out = product(c, delta_w, slice(0, width + lanes))
        delta_ref[c] = out[:, 0:width].astype(jnp.bfloat16)
        pre_ref[c] = out[:, width : width + lanes].T[0:8]
        return carried

    delta_sequence(0, 0)

    here = pl.ds(pl.multiple_of(y * tokens, tokens), tokens)
    for d in (4, 3, 5, 2, 6, 1, 7):
        to = at("sp_0", nz, d)
        links.start(units.at[to, 0:size], query_ref.at[z], zq + d, "sp_0", to)
        links.start(units.at[to, size : 3 * size], kv_ref.at[z, :, here], zk + d, "sp_0", to)
    mine = (
        pltpu.make_async_copy(units.at[z, 0:size], query_ref.at[z], local.at[7]),
        pltpu.make_async_copy(units.at[z, size : 3 * size], kv_ref.at[z, :, here], local.at[8]),
    )
    for made in mine:
        made.start()
    lax.fori_loop(1, nx, delta_sequence, 0)
    for made in mine:
        made.wait()
    kv_r, kv_l = links.number(nz), links.number(nz)
    kv_rr, kv_ll = links.number(nz), links.number(nz)
    order = (0, 1, 7, 2, 6, 3, 5, 4)

    def kv_piece(row, by, low=0, count=2 * size):
        cols = pl.ds(pl.multiple_of(at("sp_1", ny, by) * tokens, tokens), tokens)
        return kv_ref.at[row, low : low + count, cols]

    def forward(d):
        row = at("sp_0", nz, -d)
        links.arrived(kv_piece(row, -1), kv_r + d, "sp_1")
        links.start(
            kv_piece(row, -1, 0, size), kv_piece(row, -1, 0, size), kv_rr + d, "sp_1", y_right
        )
        links.arrived(kv_piece(row, 1), kv_l + d, "sp_1")
        links.start(
            kv_piece(row, 1, size, size), kv_piece(row, 1, size, size), kv_ll + d, "sp_1", y_left
        )

    for i, d in enumerate(order):
        row = at("sp_0", nz, -d)
        if d:
            links.arrived(kv_ref.at[row, :, here], zk + d, "sp_0")
        links.start(kv_piece(row, 0), kv_piece(row, 0), kv_r + d, "sp_1", y_right)
        links.start(kv_piece(row, 0), kv_piece(row, 0), kv_l + d, "sp_1", y_left)
        if i >= 2:
            forward(order[i - 2])
    for d in order[-2:]:
        forward(d)
    for d in order:
        row = at("sp_0", nz, -d)
        if d:
            links.arrived(query_ref.at[row], zq + d, "sp_0")
        links.arrived(kv_piece(row, 2, 0, size), kv_rr + d, "sp_1")
        links.arrived(kv_piece(row, 2, size, size), kv_ll + d, "sp_1")
    for d in range(1, nx):
        links.arrived(shift_ref.at[at("fs", nx, -d)], shifts + d, "fs")
    links.drain()


def project_and_share(hidden, gates, shift, sb_weights, delta_weights):
    nz, ny, nx = (lax.axis_size(a) for a in ("sp_0", "sp_1", "fs"))
    tokens, part = hidden.shape
    rows, lanes = sb_weights[0].shape[0], sb_weights[0].shape[1] // nx
    size = lanes // 2
    vmem = pl.BlockSpec(memory_space=pltpu.VMEM)
    anywhere = pl.BlockSpec(memory_space=pl.ANY)
    copies = 96
    return pl.pallas_call(
        project_kernel,
        out_shape=(
            jax.ShapeDtypeStruct((nz, size, tokens), jnp.bfloat16),
            jax.ShapeDtypeStruct((nz, 2 * size, ny * tokens), jnp.bfloat16),
            jax.ShapeDtypeStruct((nx, tokens, 3 * lanes), jnp.bfloat16),
            jax.ShapeDtypeStruct((nx, 8, tokens), jnp.float32),
            jax.ShapeDtypeStruct((nx, 1, tokens), jnp.float32),
        ),
        in_specs=[vmem] * 3 + [anywhere] * 6,
        out_specs=(vmem,) * 5,
        scratch_shapes=[
            pltpu.VMEM((nx, 2, tokens, part), jnp.bfloat16),
            pltpu.VMEM((nx, rows, 3 * lanes), jnp.bfloat16),
            pltpu.VMEM((nx, rows, 4 * lanes), jnp.bfloat16),
            pltpu.VMEM((nz, 3 * size, tokens), jnp.bfloat16),
            pltpu.SemaphoreType.DMA((copies,)),
            pltpu.SemaphoreType.DMA((copies,)),
            pltpu.SemaphoreType.DMA((10,)),
        ],
        compiler_params=pltpu.CompilerParams(collective_id=0, has_side_effects=True),
        name="project",
        cost_estimate=pl.CostEstimate(
            flops=60_000_000_000, bytes_accessed=10_000_000, transcendentals=0
        ),
    )(hidden, gates, shift, *sb_weights, *delta_weights)


def mix_kernel(
    offset_ref, bias_ref, scale_ref, query_ref, kv_ref, delta_ref, pre_ref, shift_ref, gain_ref,
    sb_out_ref, delta_out_ref,
    result_ref,
    later_ref, rows_ref, acc_ref, beyond_ref, done_ref, sb_in, delta_in, delta_done,
    through, local_out, transfer, stage1, stage2, leaving, incoming,
    sb_out_w, delta_out_w, given, taken, send, recv, local,
):
    z, y, x, t = (lax.axis_index(a) for a in ("sp_0", "sp_1", "fs", "tp"))
    nz, ny, nx = (lax.axis_size(a) for a in ("sp_0", "sp_1", "fs"))
    me = {"sp_0": z, "sp_1": y, "fs": x, "tp": t}
    links = Links(send, recv, me)
    tile, size = query_ref.shape[2], query_ref.shape[1]
    groups = kv_ref.shape[2] // tile
    key = delta_ref.shape[2] // 3

    def at(axis, count, by):
        return lax.rem(me[axis] + by + count, count)

    loads = [
        pltpu.make_async_copy(sb_out_ref, sb_out_w, local.at[0]),
        pltpu.make_async_copy(delta_out_ref, delta_out_w, local.at[1]),
    ]
    for made in loads:
        made.start()
    barrier = pltpu.get_barrier_semaphore()
    peers = [
        {"sp_0": at("sp_0", nz, dz), "fs": at("fs", nx, dx)}
        for dz in range(nz)
        for dx in range(nx)
        if dz or dx
    ]
    peers += [{"sp_1": at("sp_1", ny, d)} for d in range(1, ny)] + [{"tp": 1 - t}]
    for peer in peers:
        pl.semaphore_signal(barrier, inc=1, device_id=peer, device_id_type=pl.DeviceIdType.MESH)
    pl.semaphore_wait(barrier, len(peers))

    row_at = lax.broadcasted_iota(jnp.int32, (tile, tile), 0)
    col_at = lax.broadcasted_iota(jnp.int32, (tile, tile), 1)
    later_ref[...] = jnp.where(row_at > col_at, 1.0, 0.0).astype(jnp.bfloat16)
    offset = offset_ref[2 * x + lax.rem(z, 2)]

    def low(a):
        return a.astype(jnp.bfloat16)

    def mul(a, b, contract=((1,), (0,))):
        return lax.dot_general(
            low(a), low(b), (contract, ((), ())), preferred_element_type=jnp.float32
        )

    same = row_at // BLOCK == col_at // BLOCK
    inclusive = same & (col_at <= row_at)
    strictly = same & (col_at < row_at)
    decay_pre = jnp.concatenate([pre_ref[s, 0:1] for s in range(nx)], axis=0)
    write_pre = jnp.concatenate([pre_ref[s, 1:2] for s in range(nx)], axis=0)
    shift = jnp.concatenate([shift_ref[s] for s in range(nx)], axis=0)
    softplus = jnp.maximum(decay_pre, 0.0) + jnp.log1p(jnp.exp(-jnp.abs(decay_pre)))
    rate = jnp.exp(jnp.full(decay_pre.shape, scale_ref[x], jnp.float32))
    log_decay = shift - rate * softplus
    strength = jax.nn.sigmoid(write_pre + bias_ref[x])
    up_to = jnp.where(same & (row_at <= col_at), 1.0, 0.0)
    both = jnp.concatenate([log_decay, strength], axis=0)
    summed = jnp.dot(
        both, up_to, preferred_element_type=jnp.float32, precision=lax.Precision.HIGHEST
    )
    sums_col = summed.T
    both_col = both.T
    blocks = tile // BLOCK

    def local_part(s):
        cum_row = summed[s : s + 1]
        cum = sums_col[:, s : s + 1]
        beta = both_col[:, nx + s : nx + s + 1]
        act = jax.nn.silu(delta_ref[s].astype(jnp.float32))
        q, k, v = act[:, 0:key], act[:, key : 2 * key], act[:, 2 * key : 3 * key]
        q = unit_rows(q) * key ** (-0.5)
        k = unit_rows(k)
        spread = cum - cum_row
        decay = jnp.where(inclusive, jnp.exp(jnp.where(inclusive, spread, 0.0)), 0.0)
        k_beta = k * beta
        lower = jnp.where(strictly, mul(k_beta, k, ((1,), (1,))) * decay, 0.0)
        inside = mul(q, k, ((1,), (1,))) * decay
        powered = lower
        inverse = jnp.where(row_at == col_at, 1.0, 0.0) - lower
        for _ in range(max(1, (BLOCK - 1).bit_length()) - 1):
            powered = mul(powered, powered)
            inverse = inverse + mul(inverse, powered)
        growth = jnp.exp(cum)
        updates = mul(inverse, jnp.concatenate([v * beta, k_beta * growth], axis=1))
        within = mul(inside, updates)
        reach = q * growth - within[:, key:]
        last = [cum[(b + 1) * BLOCK - 1 : (b + 1) * BLOCK] for b in range(blocks)]
        carried = None
        eye = jnp.where(
            lax.broadcasted_iota(jnp.int32, (key, key), 0)
            == lax.broadcasted_iota(jnp.int32, (key, key), 1),
            1.0,
            0.0,
        )
        zero = jnp.zeros((key, key), jnp.float32)
        for b in range(blocks):
            rows = slice(b * BLOCK, (b + 1) * BLOCK)
            damped = k[rows] * jnp.exp(last[b] - cum[rows])
            step = mul(damped, updates[rows], ((0,), (0,)))
            keep = jnp.exp(last[b])
            start = jnp.concatenate([zero, eye], axis=1) if carried is None else carried
            out = mul(reach[rows], start)
            local_out[s, rows] = within[rows, 0:key] + out[:, 0:key]
            through[s, rows] = low(out[:, key:])
            carried = (
                start * keep
                - mul(step[:, key:], start)
                + jnp.concatenate([step[:, 0:key], zero], axis=1)
            )
        transfer[s] = low(carried)

    for s in range(nx):
        local_part(s)

    one = links.number(ny)
    for d in (2, 1, 3):
        to = at("sp_1", ny, d)
        links.start(transfer.at[to], stage1.at[y], one + d, "sp_1", to)
    mine = pltpu.make_async_copy(transfer.at[y], stage1.at[y], local.at[2])
    mine.start()
    two, three = links.number(nz), links.number(ny)
    keep_own = pltpu.make_async_copy(leaving.at[y], incoming.at[y], local.at[3])

    def over_group():
        mine.wait()
        for d in range(1, ny):
            links.arrived(stage1.at[at("sp_1", ny, -d)], one + d, "sp_1")
        joined = stage1[0].astype(jnp.float32)
        for k in range(1, ny):
            own = stage1[k]
            new = mul(own[:, key:], joined)
            joined = jnp.concatenate(
                [new[:, 0:key] + own[:, 0:key].astype(jnp.float32), new[:, key:]], axis=1
            )
        stage2[z] = low(joined)

    def share_group():
        for d in (4, 3, 5, 2, 6, 1, 7):
            links.start(stage2.at[z], stage2.at[z], two + d, "sp_0", at("sp_0", nz, d), lambda: stage2.at[0])

    def over_line():
        for d in range(1, nz):
            links.arrived(stage2.at[at("sp_0", nz, -d)], two + d, "sp_0")
        state = jnp.zeros((key, key), jnp.float32)
        for k in range(nz - 1):
            own = stage2[k]
            new = mul(own[:, key:], state) + own[:, 0:key].astype(jnp.float32)
            state = jnp.where(k < z, new, state)
        for k in range(ny):
            leaving[k] = low(state)
            if k < ny - 1:
                own = stage1[k]
                state = mul(own[:, key:], state) + own[:, 0:key].astype(jnp.float32)

    def share_states():
        for d in (2, 1, 3):
            to = at("sp_1", ny, d)
            links.start(leaving.at[to], incoming.at[y], three + d, "sp_1", to, lambda: leaving.at[0])
        keep_own.start()

    def delta_end():
        keep_own.wait()
        for d in range(1, ny):
            links.arrived(incoming.at[at("sp_1", ny, -d)], three + d, "sp_1")
        for s in range(nx):
            rows = mul(through[s], incoming[s]) + local_out[s]
            normed = (
                rows
                * lax.rsqrt(jnp.mean(rows * rows, axis=-1, keepdims=True) + NORM_EPS)
                * gain_ref[...]
            )
            delta_done[s] = low(normed)

    four = links.number(nx)
    keep_delta = pltpu.make_async_copy(delta_done.at[x], delta_in.at[x], local.at[4])

    def share_delta():
        for d in (2, 1, 3):
            to = at("fs", nx, d)
            links.start(delta_done.at[to], delta_in.at[x], four + d, "fs", to, lambda: delta_done.at[0])
        keep_delta.start()

    def key_row(row, count, diagonal):
        queries = rows_ref[...]
        beyond = None if diagonal else beyond_ref[...]
        weights = []
        for k in range(count - 1, -1, -1):
            scores = (
                jnp.dot(
                    queries,
                    kv_ref[row, 0:size, k * tile : (k + 1) * tile],
                    preferred_element_type=jnp.float32,
                )
                + offset
            )
            above = jnp.maximum(scores, 0.0)
            below = scores - above
            small = jnp.exp(below - above)
            log_term = jnp.where(small < 2.0**-12, small, jnp.log(1.0 + small))
            passed = above + log_term
            exponent = below - log_term
            if diagonal and k == count - 1:
                visible = col_at < row_at
                passed = jnp.where(visible, passed, 0.0)
                exponent = jnp.where(visible, exponent, -jnp.inf)
            after = jnp.dot(low(passed), later_ref[...], preferred_element_type=jnp.float32)
            exponent = exponent - after
            if beyond is not None:
                exponent = exponent - beyond
            total = after[:, :1] + passed[:, :1]
            beyond = total if beyond is None else beyond + total
            weights.append(low(jnp.exp(exponent)))
        partial = lax.dot_general(
            jnp.concatenate(weights[::-1], axis=1),
            kv_ref[row, size : 2 * size, 0 : count * tile],
            (((1,), (1,)), ((), ())),
            preferred_element_type=jnp.float32,
        )
        beyond_ref[...] = beyond
        if diagonal:
            acc_ref[...] = partial
        else:
            acc_ref[...] += partial

    five = links.number(2 * nx)
    sends = links.sent
    links.sent += nz
    home = z // 2
    slot = 2 * x + lax.rem(z, 2)

    def sb_copy(row):
        return pltpu.make_async_remote_copy(
            src_ref=done_ref.at[row],
            dst_ref=sb_in.at[slot],
            send_sem=send.at[sends + row],
            recv_sem=recv.at[five + slot],
            device_id={"fs": home, "sp_0": row},
            device_id_type=pl.DeviceIdType.MESH,
        )

    keep_sb = pltpu.make_async_copy(done_ref.at[z], sb_in.at[slot], local.at[5])

    def send_back(row):
        stays = (row == z) & (home == x)

        @pl.when(stays)
        def _():
            keep_sb.start()

        @pl.when(jnp.logical_not(stays))
        def _():
            sb_copy(row).start()

    def per_query(row, unused):
        rows_ref[...] = low((query_ref[row].astype(jnp.float32) * size ** (-0.5)).T)
        pl.when(row == 3)(over_group)
        pl.when(row == 6)(over_line)
        pl.when(row == 7)(delta_end)
        for k in range(groups):

            @pl.when(y == k)
            def _():
                key_row(row, k + 1, True)

        pl.when(row == 3)(share_group)
        pl.when(row == 6)(share_states)
        pl.when(row == 7)(share_delta)

        @pl.when(row > 0)
        def _():
            send_back(row - 1)

        def earlier(step, carried):
            key_row(row - 1 - step, groups, False)
            return carried

        lax.fori_loop(0, row, earlier, 0)
        done_ref[row] = low(acc_ref[...].T)
        return unused

    lax.fori_loop(0, nz, per_query, 0)
    for made in loads:
        made.wait()
    send_back(nz - 1)
    keep_delta.wait()
    for d in range(1, nx):
        links.arrived(delta_in.at[at("fs", nx, -d)], four + d, "fs")

    rows = tile // 2
    mine_rows = pl.ds(pl.multiple_of(t * rows, rows), rows)
    other_rows = pl.ds(pl.multiple_of((1 - t) * rows, rows), rows)
    delta_mixed = [delta_in[k] for k in range(nx)]
    columns = result_ref.shape[1]
    span = columns // 4
    for k in range(nx):
        for h in range(2):
            here = (z == 2 * x + h) & (x == k)

            @pl.when(here)
            def _():
                keep_sb.wait()

            @pl.when(jnp.logical_not(here))
            def _():
                links.arrived(sb_in.at[2 * k + h], five + 2 * k + h, "fs")

    sb_rows = sb_in[...].reshape(nz * size, tile).astype(jnp.float32).T
    rows_ref2 = low(jnp.concatenate([sb_rows] + [d.astype(jnp.float32) for d in delta_mixed], axis=1))
    taken[...] = rows_ref2
    six = links.number(4)

    def projected(part, cols):
        return low(
            jnp.dot(
                taken[part, 0 : nz * size], sb_out_w[:, cols], preferred_element_type=jnp.float32
            )
            + jnp.dot(
                taken[part, nz * size :], delta_out_w[:, cols], preferred_element_type=jnp.float32
            )
        )

    outs = [slice(c * span, (c + 1) * span) for c in range(4)]
    for c in range(4):
        given[0, :, outs[c]] = projected(other_rows, outs[c])
        if c:
            links.start(
                given.at[0, :, outs[c - 1]], given.at[1, :, outs[c - 1]], six + c - 1, "tp", 1 - t
            )
    own = projected(mine_rows, outs[0])
    links.start(given.at[0, :, outs[3]], given.at[1, :, outs[3]], six + 3, "tp", 1 - t)
    for c in range(4):
        links.arrived(given.at[1, :, outs[c]], six + c, "tp")
        total = own.astype(jnp.float32) + given[1, :, outs[c]].astype(jnp.float32)
        result_ref[:, outs[c]] = low(total)
        if c < 3:
            own = projected(mine_rows, outs[c + 1])
    for row in range(nz):

        @pl.when(jnp.logical_not((row == z) & (home == x)))
        def _():
            sb_copy(row).wait_send()

    links.drain()


def mix(offset, bias, scale, queries, keys_values, delta_proj, pre, shift, gain, sb_out, delta_out):
    nz, ny, nx = (lax.axis_size(a) for a in ("sp_0", "sp_1", "fs"))
    size, tile = queries.shape[1:]
    key = delta_proj.shape[2] // 3
    columns = sb_out.shape[1]
    half = tile // 2
    smem = pl.BlockSpec(memory_space=pltpu.SMEM)
    vmem = pl.BlockSpec(memory_space=pltpu.VMEM)
    anywhere = pl.BlockSpec(memory_space=pl.ANY)
    copies = 64
    bf16, f32 = jnp.bfloat16, jnp.float32
    return pl.pallas_call(
        mix_kernel,
        out_shape=jax.ShapeDtypeStruct((half, columns), bf16),
        in_specs=[smem] * 3 + [vmem] * 6 + [anywhere] * 2,
        out_specs=vmem,
        scratch_shapes=[
            pltpu.VMEM((tile, tile), bf16),
            pltpu.VMEM((tile, size), bf16),
            pltpu.VMEM((tile, size), f32),
            pltpu.VMEM((tile, 1), f32),
            pltpu.VMEM((nz, size, tile), bf16),
            pltpu.VMEM((2 * nx, size, tile), bf16),
            pltpu.VMEM((nx, tile, key), bf16),
            pltpu.VMEM((nx, tile, key), bf16),
            pltpu.VMEM((nx, tile, key), bf16),
            pltpu.VMEM((nx, tile, key), f32),
            pltpu.VMEM((nx, key, 2 * key), bf16),
            pltpu.VMEM((ny, key, 2 * key), bf16),
            pltpu.VMEM((nz, key, 2 * key), bf16),
            pltpu.VMEM((ny, key, key), bf16),
            pltpu.VMEM((nx, key, key), bf16),
            pltpu.VMEM(sb_out.shape, bf16),
            pltpu.VMEM(delta_out.shape, bf16),
            pltpu.VMEM((2, half, columns), bf16),
            pltpu.VMEM((tile, nz * size + nx * key), bf16),
            pltpu.SemaphoreType.DMA((copies,)),
            pltpu.SemaphoreType.DMA((copies,)),
            pltpu.SemaphoreType.DMA((6,)),
        ],
        compiler_params=pltpu.CompilerParams(collective_id=1, has_side_effects=True),
        name="mix",
        cost_estimate=pl.CostEstimate(
            flops=60_000_000_000, bytes_accessed=10_000_000, transcendentals=30_000_000
        ),
    )(offset, bias, scale, queries, keys_values, delta_proj, pre, shift, gain, sb_out, delta_out)


def on_device(
    hidden_in,
    sb_query_w,
    sb_key_w,
    sb_value_w,
    sb_offset,
    delta_query_w,
    delta_key_w,
    delta_value_w,
    decay_w,
    write_w,
    write_bias,
    decay_log_scale,
    decay_shift,
    head_gain,
    sb_out_w,
    delta_out_w,
):
    tokens, part = hidden_in.shape[1], hidden_in.shape[2]
    fs_count = lax.axis_size("fs")
    mine = lax.axis_index("fs")
    gates_w = jnp.concatenate(
        [lax.dynamic_slice_in_dim(w, mine, 1, 1) for w in (decay_w, write_w)], axis=1
    )
    lanes = sb_query_w.shape[1] // fs_count
    gates_w = jnp.pad(gates_w, ((0, 0), (0, lanes - 2))).reshape(fs_count, -1, lanes)
    unit_queries, keys_values, delta_proj, pre, shift = project_and_share(
        hidden_in.reshape(tokens, part),
        gates_w,
        decay_shift.reshape(fs_count, 1, tokens),
        (sb_query_w, sb_key_w, sb_value_w),
        (delta_query_w, delta_key_w, delta_value_w),
    )
    result = mix(
        sb_offset,
        write_bias,
        decay_log_scale,
        unit_queries,
        keys_values,
        delta_proj,
        pre,
        shift,
        head_gain.reshape(1, -1),
        sb_out_w,
        delta_out_w,
    )
    return result.reshape(1, *result.shape)


def solution(mesh):
    finer = Mesh(
        mesh.devices.reshape(8, 4, mesh.shape["fs"], mesh.shape["tp"]), ("sp_0", "sp_1", "fs", "tp")
    )
    return jax.shard_map(
        on_device,
        mesh=finer,
        in_specs=(
            P("fs", SP, "tp"),
            P("fs", "tp"),
            P("fs", "tp"),
            P("fs", "tp"),
            P("tp"),
            P("fs", "tp"),
            P("fs", "tp"),
            P("fs", "tp"),
            P(None, "tp"),
            P(None, "tp"),
            P("tp"),
            P("tp"),
            P("fs", "tp", SP),
            P(),
            P("tp", None),
            P("tp", None),
        ),
        out_specs=P("fs", SP_TP, None),
        check_vma=False,
    )
```

time: 283 us -> 159 us (0.56)
  the two profiles are of different devices: /device:TPU:1 before, /device:TPU:249 now
where the time goes in v3:
time: 159 us; the launch traced here: 158 us
  Pallas kernels  153 us (96%)
  local copies, waits for them, and re-layouts  5.14 us (3%)
    pallas_call x1, Pallas kernels, project_and_share(): pl.pallas_call(project_kernel, out_shape=(jax.ShapeDtypeStruct((nz, size,...  80.1 us
    pallas_call x1, Pallas kernels, mix(): pl.pallas_call(mix_kernel, out_shape=jax.ShapeDtypeStruct((half, columns)...  73.1 us

profile of v3, /device:TPU:249, one launch (start us, length us, event | category | flops | bytes accessed | tf_op | source)
XLA Modules:
  0.0 158.4 jit_solution(7193820001656351637)
XLA Ops:
  0.0 1.3 reshape.17.shift_in
  1.3 0.8 constant_dynamic-slice_fusion
  2.1 0.3 copy.18
  2.4 0.9 pad.4.clone
  3.3 80.1 %project.1 = (bf16[8,64,256]{2,1,0:T(8,128)(2,1)}, bf16[8,128,1024]{2,1,0:T(8,128)(2,1)}, bf16[4,256,384]{2,1,0:T(8,128)(2,1)}, f32[4,8,256]{2,1,0:T(8,128)}, f32[4,1,256]{2,1,0:T(1,128)}) custom-call(bf16[256,1024]{1,0:T(8,128)(2,1)} %bitcast.6, bf16[4,512,128]{2,1,0:T(8,128)(2,1)} %bitcast.5, f32[4,1,256]{2,1,0:T(1,128)} %reshape.17.shift_in, ...), custom_call_target="tpu_custom_call" | custom-call | flops 60000002048 | bytes 10000000 | tf_op jit(solution)/shard_map/project/pallas_call | solution.py:281
  83.4 73.1 %mix.1 = bf16[128,2048]{1,0:T(8,128)(2,1)} custom-call(f32[8]{0:T(128)} %offset_ref.1, f32[4]{0:T(128)} %bias_ref.1, f32[4]{0:T(128)} %scale_ref.1, bf16[8,64,256]{2,1,0:T(8,128)(2,1)} %get-tuple-element.10.query_ref, bf16[8,128,1024]{2,1,0:T(8,128)(2,1)} %get-tuple-element.11.kv_ref, bf16[4,256,384]{2,1,0:T(8,128)(2,1)} %get-tuple-element.12.delta_ref, ...), custom_call_target="tpu_custom_call" | custom-call | flops 60000002048 | bytes 10000000 | tf_op jit(solution)/shard_map/mix/pallas_call | solution.py:670
  156.5 1.9 %copy.20 = bf16[1,128,2048]{2,1,0:T(8,128)(2,1)} copy(bf16[1,128,2048]{2,1,0:T(8,128)(2,1)} %bitcast.4) | data formatting | bytes 1048576
  (1 shorter events, 0.0 us)

commit v4 on v3

--- a/solution.py
+++ b/solution.py
@@ -55,261 +55,11 @@
         self.open = []
 
 
-def greet(peers):
-    barrier = pltpu.get_barrier_semaphore()
-    for axis, to in peers:
-        pl.semaphore_signal(
-            barrier, inc=1, device_id={axis: to}, device_id_type=pl.DeviceIdType.MESH
-        )
-    pl.semaphore_wait(barrier, len(peers))
-
-
-def project_kernel(
-    hidden_ref, gates_ref, shift_in, q0, k0, v0, q1, k1, v1,
-    query_ref, kv_ref, delta_ref, pre_ref, shift_ref,
-    acts, sb_w, delta_w, units, send, recv, local,
-):
-    z, y, x, t = (lax.axis_index(a) for a in ("sp_0", "sp_1", "fs", "tp"))
-    nz, ny, nx = (lax.axis_size(a) for a in ("sp_0", "sp_1", "fs"))
-    me = {"sp_0": z, "sp_1": y, "fs": x, "tp": t}
-    links = Links(send, recv, me)
-    tokens = hidden_ref.shape[0]
-    half = tokens // 2
-    lanes = q0.shape[1] // nx
-    z_rows, y_rows = q0.shape[0] // nz, q0.shape[0] // ny
-
-    def at(axis, size, by):
-        return lax.rem(me[axis] + by + size, size)
-
-    greet(
-        [("fs", at("fs", nx, d)) for d in range(1, nx)]
-        + [("sp_0", at("sp_0", nz, d)) for d in range(1, nz)]
-        + [("sp_1", at("sp_1", ny, d)) for d in (1, -1)]
-        + [("tp", 1 - t)]
-    )
-    sets = ((q0, k0, v0), sb_w, z * z_rows, z_rows), ((q1, k1, v1), delta_w, y * y_rows, y_rows)
-    width = 3 * lanes
-    first = {}
-    for d in (2, 1, 3):
-        to = at("fs", nx, d)
-        for s, (mats, held, row, size) in enumerate(sets):
-            first[d, s] = links.number()
-            for m, w in enumerate(mats):
-                links.start(
-                    w.at[pl.ds(row, size), pl.ds(to * lanes, lanes)],
-                    held.at[x, pl.ds(row, size), m * lanes : (m + 1) * lanes],
-                    first[d, s], "fs", to,
-                )
-    own = []
-    for s, (mats, held, row, size) in enumerate(sets):
-        for m, w in enumerate(mats):
-            own.append(
-                pltpu.make_async_copy(
-                    w.at[pl.ds(row, size), pl.ds(x * lanes, lanes)],
-                    held.at[x, pl.ds(row, size), m * lanes : (m + 1) * lanes],
-                    local.at[3 * s + m],
-                )
-            )
-            own[-1].start()
-    shifts = links.number(nx)
-    for d in range(1, nx):
-        links.start(shift_in.at[at("fs", nx, d)], shift_ref.at[x], shifts + d, "fs", at("fs", nx, d))
-    own.append(pltpu.make_async_copy(shift_in.at[x], shift_ref.at[x], local.at[9]))
-    own[-1].start()
-    right, left, other = at("fs", nx, 1), at("fs", nx, -1), 1 - t
-    act = links.number(8)
-    links.start(hidden_ref, acts.at[x, t], act, "fs", right)
-    links.start(hidden_ref, acts.at[x, t], act + 1, "fs", left)
-    links.start(hidden_ref, acts.at[x, t], act + 4, "tp", other)
-    keep = pltpu.make_async_copy(hidden_ref, acts.at[x, t], local.at[6])
-    keep.start()
-    for made in own:
-        made.wait()
-    for d in (1, 3, 2):
-        source = at("fs", nx, -d)
-        for s, (mats, held, row, size) in enumerate(sets):
-            links.arrived(held.at[source, pl.ds(row, size), 0:width], first[d, s], "fs")
-
-    def sb_piece(by, low=0, count=nx):
-        return sb_w.at[low : low + count, pl.ds(at("sp_0", nz, by) * z_rows, z_rows), :]
-
-    def delta_piece(by, low=0, count=nx):
-        rows = pl.ds(at("sp_1", ny, by) * y_rows, y_rows)
-        return delta_w.at[low : low + count, rows, 0:width]
-
-    z_right, z_left = at("sp_0", nz, 1), at("sp_0", nz, -1)
-    y_right, y_left = at("sp_1", ny, 1), at("sp_1", ny, -1)
-    steps = nz // 2
-    zr, zl = links.number(steps), links.number(steps)
-    yr, yl = links.number(2), links.number(2)
-    links.start(sb_piece(0), sb_piece(0), zr, "sp_0", z_right)
-    links.start(sb_piece(0), sb_piece(0), zl, "sp_0", z_left)
-    links.start(delta_piece(0), delta_piece(0), yr, "sp_1", y_right)
-    links.start(delta_piece(0), delta_piece(0), yl, "sp_1", y_left)
-
-    def z_step(s):
-        if s < steps:
-            low, count = (0, nx) if s < steps - 1 else (0, nx // 2)
-            links.arrived(sb_piece(-s), zr + s - 1, "sp_0")
-            links.start(sb_piece(-s, low, count), sb_piece(-s, low, count), zr + s, "sp_0", z_right)
-            low, count = (0, nx) if s < steps - 1 else (nx // 2, nx // 2)
-            links.arrived(sb_piece(s), zl + s - 1, "sp_0")
-            links.start(sb_piece(s, low, count), sb_piece(s, low, count), zl + s, "sp_0", z_left)
-        else:
-            links.arrived(sb_piece(steps, 0, nx // 2), zr + s - 1, "sp_0")
-            links.arrived(sb_piece(steps, nx // 2, nx // 2), zl + s - 1, "sp_0")
-
-    z_step(1)
-    links.arrived(delta_piece(-1), yr, "sp_1")
-    links.start(delta_piece(-1, 0, 2), delta_piece(-1, 0, 2), yr + 1, "sp_1", y_right)
-    links.arrived(delta_piece(1), yl, "sp_1")
-    links.start(delta_piece(1, 2, 2), delta_piece(1, 2, 2), yl + 1, "sp_1", y_left)
-    z_step(2)
-    before, after, far = at("fs", nx, -1), at("fs", nx, 1), at("fs", nx, 2)
-    links.arrived(acts.at[before, t], act, "fs")
-    links.start(acts.at[before, t, 0:half], acts.at[before, t, 0:half], act + 2, "fs", right)
-    links.start(acts.at[before, t], acts.at[before, t], act + 5, "tp", other)
-    links.arrived(acts.at[after, t], act + 1, "fs")
-    links.start(
-        acts.at[after, t, half:tokens], acts.at[after, t, half:tokens], act + 3, "fs", left
-    )
-    links.start(acts.at[after, t], acts.at[after, t], act + 6, "tp", other)
-    z_step(3)
-    delta_w[:, :, width : width + lanes] = gates_ref[...]
-    z_step(4)
-    links.arrived(delta_piece(2, 0, 2), yr + 1, "sp_1")
-    links.arrived(delta_piece(2, 2, 2), yl + 1, "sp_1")
-    links.arrived(acts.at[far, t, 0:half], act + 2, "fs")
-    links.arrived(acts.at[far, t, half:tokens], act + 3, "fs")
-    links.start(acts.at[far, t], acts.at[far, t], act + 7, "tp", other)
-    keep.wait()
-    for k, c in enumerate((x, before, after, far)):
-        links.arrived(acts.at[c, other], act + 4 + k, "tp")
-
-    size = lanes // 2
-    zq, zk = links.number(nz), links.number(nz)
-
-    def product(c, held, cols):
-        return sum(
-            jnp.dot(
-                acts[c, p],
-                held[2 * p : 2 * p + 2, :, cols].reshape(acts.shape[3], -1),
-                preferred_element_type=jnp.float32,
-            )
-            for p in range(2)
-        )
-
-    def sb_sequence(c, carried):
-        for m in range(3):
-            block = product(c, sb_w, slice(m * lanes, (m + 1) * lanes)).T.astype(jnp.bfloat16)
-            units[2 * c, m * size : (m + 1) * size, :] = block[0:size]
-            units[2 * c + 1, m * size : (m + 1) * size, :] = block[size:lanes]
-        return carried
-
-    lax.fori_loop(0, nx, sb_sequence, 0)
-
-    def delta_sequence(c, carried):
-        out = product(c, delta_w, slice(0, width + lanes))
-        delta_ref[c] = out[:, 0:width].astype(jnp.bfloat16)
-        pre_ref[c] = out[:, width : width + lanes].T[0:8]
-        return carried
-
-    delta_sequence(0, 0)
-
-    here = pl.ds(pl.multiple_of(y * tokens, tokens), tokens)
-    for d in (4, 3, 5, 2, 6, 1, 7):
-        to = at("sp_0", nz, d)
-        links.start(units.at[to, 0:size], query_ref.at[z], zq + d, "sp_0", to)
-        links.start(units.at[to, size : 3 * size], kv_ref.at[z, :, here], zk + d, "sp_0", to)
-    mine = (
-        pltpu.make_async_copy(units.at[z, 0:size], query_ref.at[z], local.at[7]),
-        pltpu.make_async_copy(units.at[z, size : 3 * size], kv_ref.at[z, :, here], local.at[8]),
-    )
-    for made in mine:
-        made.start()
-    lax.fori_loop(1, nx, delta_sequence, 0)
-    for made in mine:
-        made.wait()
-    kv_r, kv_l = links.number(nz), links.number(nz)
-    kv_rr, kv_ll = links.number(nz), links.number(nz)
-    order = (0, 1, 7, 2, 6, 3, 5, 4)
-
-    def kv_piece(row, by, low=0, count=2 * size):
-        cols = pl.ds(pl.multiple_of(at("sp_1", ny, by) * tokens, tokens), tokens)
-        return kv_ref.at[row, low : low + count, cols]
-
-    def forward(d):
-        row = at("sp_0", nz, -d)
-        links.arrived(kv_piece(row, -1), kv_r + d, "sp_1")
-        links.start(
-            kv_piece(row, -1, 0, size), kv_piece(row, -1, 0, size), kv_rr + d, "sp_1", y_right
-        )
-        links.arrived(kv_piece(row, 1), kv_l + d, "sp_1")
-        links.start(
-            kv_piece(row, 1, size, size), kv_piece(row, 1, size, size), kv_ll + d, "sp_1", y_left
-        )
-
-    for i, d in enumerate(order):
-        row = at("sp_0", nz, -d)
-        if d:
-            links.arrived(kv_ref.at[row, :, here], zk + d, "sp_0")
-        links.start(kv_piece(row, 0), kv_piece(row, 0), kv_r + d, "sp_1", y_right)
-        links.start(kv_piece(row, 0), kv_piece(row, 0), kv_l + d, "sp_1", y_left)
-        if i >= 2:
-            forward(order[i - 2])
-    for d in order[-2:]:
-        forward(d)
-    for d in order:
-        row = at("sp_0", nz, -d)
-        if d:
-            links.arrived(query_ref.at[row], zq + d, "sp_0")
-        links.arrived(kv_piece(row, 2, 0, size), kv_rr + d, "sp_1")
-        links.arrived(kv_piece(row, 2, size, size), kv_ll + d, "sp_1")
-    for d in range(1, nx):
-        links.arrived(shift_ref.at[at("fs", nx, -d)], shifts + d, "fs")
-    links.drain()
-
-
-def project_and_share(hidden, gates, shift, sb_weights, delta_weights):
-    nz, ny, nx = (lax.axis_size(a) for a in ("sp_0", "sp_1", "fs"))
-    tokens, part = hidden.shape
-    rows, lanes = sb_weights[0].shape[0], sb_weights[0].shape[1] // nx
-    size = lanes // 2
-    vmem = pl.BlockSpec(memory_space=pltpu.VMEM)
-    anywhere = pl.BlockSpec(memory_space=pl.ANY)
-    copies = 96
-    return pl.pallas_call(
-        project_kernel,
-        out_shape=(
-            jax.ShapeDtypeStruct((nz, size, tokens), jnp.bfloat16),
-            jax.ShapeDtypeStruct((nz, 2 * size, ny * tokens), jnp.bfloat16),
-            jax.ShapeDtypeStruct((nx, tokens, 3 * lanes), jnp.bfloat16),
-            jax.ShapeDtypeStruct((nx, 8, tokens), jnp.float32),
-            jax.ShapeDtypeStruct((nx, 1, tokens), jnp.float32),
-        ),
-        in_specs=[vmem] * 3 + [anywhere] * 6,
-        out_specs=(vmem,) * 5,
-        scratch_shapes=[
-            pltpu.VMEM((nx, 2, tokens, part), jnp.bfloat16),
-            pltpu.VMEM((nx, rows, 3 * lanes), jnp.bfloat16),
-            pltpu.VMEM((nx, rows, 4 * lanes), jnp.bfloat16),
-            pltpu.VMEM((nz, 3 * size, tokens), jnp.bfloat16),
-            pltpu.SemaphoreType.DMA((copies,)),
-            pltpu.SemaphoreType.DMA((copies,)),
-            pltpu.SemaphoreType.DMA((10,)),
-        ],
-        compiler_params=pltpu.CompilerParams(collective_id=0, has_side_effects=True),
-        name="project",
-        cost_estimate=pl.CostEstimate(
-            flops=60_000_000_000, bytes_accessed=10_000_000, transcendentals=0
-        ),
-    )(hidden, gates, shift, *sb_weights, *delta_weights)
-
-
-def mix_kernel(
-    offset_ref, bias_ref, scale_ref, query_ref, kv_ref, delta_ref, pre_ref, shift_ref, gain_ref,
-    sb_out_ref, delta_out_ref,
+def layer_kernel(
+    offset_ref, bias_ref, scale_ref, hidden_ref, decay_ref, write_ref, shift_in, gain_ref,
+    q0, k0, v0, q1, k1, v1, sb_out_ref, delta_out_ref,
     result_ref,
+    acts, sb_w, delta_w, units, query_ref, kv_ref, delta_ref, pre_ref, shift_out, shift_ref,
     later_ref, rows_ref, acc_ref, beyond_ref, done_ref, sb_in, delta_in, delta_done,
     through, local_out, transfer, stage1, stage2, leaving, incoming,
     sb_out_w, delta_out_w, given, taken, send, recv, local,
@@ -319,18 +69,19 @@
     me = {"sp_0": z, "sp_1": y, "fs": x, "tp": t}
     links = Links(send, recv, me)
     tile, size = query_ref.shape[2], query_ref.shape[1]
+    tokens, half = tile, tile // 2
     groups = kv_ref.shape[2] // tile
     key = delta_ref.shape[2] // 3
+    lanes = q0.shape[1] // nx
+    width = 3 * lanes
+    z_rows, y_rows = q0.shape[0] // nz, q0.shape[0] // ny
 
     def at(axis, count, by):
         return lax.rem(me[axis] + by + count, count)
 
-    loads = [
-        pltpu.make_async_copy(sb_out_ref, sb_out_w, local.at[0]),
-        pltpu.make_async_copy(delta_out_ref, delta_out_w, local.at[1]),
-    ]
-    for made in loads:
-        made.start()
+    def low(a):
+        return a.astype(jnp.bfloat16)
+
     barrier = pltpu.get_barrier_semaphore()
     peers = [
         {"sp_0": at("sp_0", nz, dz), "fs": at("fs", nx, dx)}
@@ -343,13 +94,240 @@
         pl.semaphore_signal(barrier, inc=1, device_id=peer, device_id_type=pl.DeviceIdType.MESH)
     pl.semaphore_wait(barrier, len(peers))
 
+    sets = (
+        ((q0, k0), sb_w, 0, z * z_rows, z_rows),
+        ((v0,), sb_w, 2, y * y_rows, y_rows),
+        ((q1, k1, v1), delta_w, 0, y * y_rows, y_rows),
+    )
+    first = {}
+    own = []
+
+    def pass_on(s, d):
+        mats, held, place, row, count = sets[s]
+        to = at("fs", nx, d)
+        first[s, d] = links.number()
+        for m, w in enumerate(mats):
+            src = w.at[pl.ds(row, count), pl.ds(pl.multiple_of(to * lanes, lanes), lanes)]
+            cols = slice((place + m) * lanes, (place + m + 1) * lanes)
+            dst = held.at[x, pl.ds(row, count), cols]
+            if d:
+                links.start(src, dst, first[s, d], "fs", to)
+            else:
+                own.append(pltpu.make_async_copy(src, dst, local.at[6 + len(own)]))
+                own[-1].start()
+
+    for d in (2, 1, 3, 0):
+        pass_on(0, d)
+        pass_on(1, d)
+    for d in (2, 1, 3, 0):
+        pass_on(2, d)
+    right, left, other = at("fs", nx, 1), at("fs", nx, -1), 1 - t
+    act = links.number(8)
+    links.start(hidden_ref, acts.at[x, t], act, "fs", right)
+    links.start(hidden_ref, acts.at[x, t], act + 1, "fs", left)
+    links.start(hidden_ref, acts.at[x, t], act + 4, "tp", other)
+    keep = pltpu.make_async_copy(hidden_ref, acts.at[x, t], local.at[12])
+    keep.start()
+    loads = [
+        pltpu.make_async_copy(sb_out_ref, sb_out_w, local.at[0]),
+        pltpu.make_async_copy(delta_out_ref, delta_out_w, local.at[1]),
+    ]
+    for s in range(nx):
+        shift_out[s] = shift_in[s : s + 1]
+    gates = jnp.concatenate(
+        [
+            decay_ref[...].astype(jnp.float32),
+            write_ref[...].astype(jnp.float32),
+            jnp.zeros((lanes - 2 * nx, decay_ref.shape[1]), jnp.float32),
+        ],
+        axis=0,
+    )
+    delta_w[:, :, width : width + lanes] = low(gates.T).reshape(nx, -1, lanes)
     row_at = lax.broadcasted_iota(jnp.int32, (tile, tile), 0)
     col_at = lax.broadcasted_iota(jnp.int32, (tile, tile), 1)
     later_ref[...] = jnp.where(row_at > col_at, 1.0, 0.0).astype(jnp.bfloat16)
     offset = offset_ref[2 * x + lax.rem(z, 2)]
 
-    def low(a):
-        return a.astype(jnp.bfloat16)
+    z_right, z_left = at("sp_0", nz, 1), at("sp_0", nz, -1)
+    y_right, y_left = at("sp_1", ny, 1), at("sp_1", ny, -1)
+    steps = nz // 2
+    zr, zl = links.number(steps), links.number(steps)
+    vr, vl, dr, dl = (links.number(2) for _ in range(4))
+
+    def sb_piece(by, lo=0, count=nx):
+        rows = pl.ds(at("sp_0", nz, by) * z_rows, z_rows)
+        return sb_w.at[lo : lo + count, rows, 0 : 2 * lanes]
+
+    def v_piece(by, lo=0, count=nx):
+        rows = pl.ds(at("sp_1", ny, by) * y_rows, y_rows)
+        return sb_w.at[lo : lo + count, rows, 2 * lanes : width]
+
+    def delta_piece(by, lo=0, count=nx):
+        rows = pl.ds(at("sp_1", ny, by) * y_rows, y_rows)
+        return delta_w.at[lo : lo + count, rows, 0:width]
+
+    def come(s, rows):
+        mats, held, place, row, count = sets[s]
+        for d in (1, 3, 2):
+            links.arrived(
+                held.at[
+                    at("fs", nx, -d), pl.ds(row, count),
+                    place * lanes : (place + len(mats)) * lanes,
+                ],
+                first[s, d], "fs",
+            )
+
+    def y_start(piece, r, l):
+        links.start(piece(0), piece(0), r, "sp_1", y_right)
+        links.start(piece(0), piece(0), l, "sp_1", y_left)
+
+    def y_step(piece, r, l):
+        links.arrived(piece(-1), r, "sp_1")
+        links.start(piece(-1, 0, 2), piece(-1, 0, 2), r + 1, "sp_1", y_right)
+        links.arrived(piece(1), l, "sp_1")
+        links.start(piece(1, 2, 2), piece(1, 2, 2), l + 1, "sp_1", y_left)
+
+    def y_end(piece, r, l):
+        links.arrived(piece(2, 0, 2), r + 1, "sp_1")
+        links.arrived(piece(2, 2, 2), l + 1, "sp_1")
+
+    def z_step(s):
+        if s < steps:
+            lo, count = (0, nx) if s < steps - 1 else (0, nx // 2)
+            links.arrived(sb_piece(-s), zr + s - 1, "sp_0")
+            links.start(sb_piece(-s, lo, count), sb_piece(-s, lo, count), zr + s, "sp_0", z_right)
+            lo, count = (0, nx) if s < steps - 1 else (nx // 2, nx // 2)
+            links.arrived(sb_piece(s), zl + s - 1, "sp_0")
+            links.start(sb_piece(s, lo, count), sb_piece(s, lo, count), zl + s, "sp_0", z_left)
+        else:
+            links.arrived(sb_piece(steps, 0, nx // 2), zr + s - 1, "sp_0")
+            links.arrived(sb_piece(steps, nx // 2, nx // 2), zl + s - 1, "sp_0")
+
+    for made in own:
+        made.wait()
+    come(0, z_rows)
+    links.start(sb_piece(0), sb_piece(0), zr, "sp_0", z_right)
+    links.start(sb_piece(0), sb_piece(0), zl, "sp_0", z_left)
+    come(1, y_rows)
+    y_start(v_piece, vr, vl)
+    shifts = links.number(nx)
+    for d in range(1, nx):
+        to = at("fs", nx, d)
+        links.start(shift_out.at[to], shift_ref.at[x], shifts + d, "fs", to)
+    keep_shift = pltpu.make_async_copy(shift_out.at[x], shift_ref.at[x], local.at[13])
+    keep_shift.start()
+    come(2, y_rows)
+    y_start(delta_piece, dr, dl)
+    z_step(1)
+    y_step(v_piece, vr, vl)
+    z_step(2)
+    before, after, far = at("fs", nx, -1), at("fs", nx, 1), at("fs", nx, 2)
+    links.arrived(acts.at[before, t], act, "fs")
+    links.start(acts.at[before, t, 0:half], acts.at[before, t, 0:half], act + 2, "fs", right)
+    links.start(acts.at[before, t], acts.at[before, t], act + 5, "tp", other)
+    links.arrived(acts.at[after, t], act + 1, "fs")
+    links.start(
+        acts.at[after, t, half:tokens], acts.at[after, t, half:tokens], act + 3, "fs", left
+    )
+    links.start(acts.at[after, t], acts.at[after, t], act + 6, "tp", other)
+    for made in loads:
+        made.start()
+    z_step(3)
+    y_step(delta_piece, dr, dl)
+    y_end(v_piece, vr, vl)
+    z_step(4)
+    keep.wait()
+
+    def product(c, held):
+        return sum(
+            jnp.dot(
+                acts[c, p],
+                held[2 * p : 2 * p + 2].reshape(acts.shape[3], -1),
+                preferred_element_type=jnp.float32,
+            )
+            for p in range(2)
+        )
+
+    def sb_sequence(c):
+        out = product(c, sb_w)
+        for m in range(3):
+            block = low(out[:, m * lanes : (m + 1) * lanes].T)
+            units[2 * c, m * size : (m + 1) * size, :] = block[0:size]
+            units[2 * c + 1, m * size : (m + 1) * size, :] = block[size:lanes]
+
+    def delta_sequence(c):
+        out = product(c, delta_w)
+        delta_ref[c] = low(out[:, 0:width])
+        pre_ref[c] = out[:, width : width + lanes].T[0:8]
+
+    def near(i, carried):
+        c = lax.rem(x + i + nx - 1, nx)
+        sb_sequence(c)
+        return carried
+
+    for k, c in enumerate((x, before, after)):
+        links.arrived(acts.at[c, other], act + 4 + k, "tp")
+    lax.fori_loop(0, 3, near, 0)
+    links.arrived(acts.at[far, t, 0:half], act + 2, "fs")
+    links.arrived(acts.at[far, t, half:tokens], act + 3, "fs")
+    links.start(acts.at[far, t], acts.at[far, t], act + 7, "tp", other)
+    y_end(delta_piece, dr, dl)
+    links.arrived(acts.at[far, other], act + 7, "tp")
+    lax.fori_loop(3, 4, near, 0)
+    delta_sequence(x)
+
+    here = pl.ds(pl.multiple_of(y * tokens, tokens), tokens)
+    zq, zk = links.number(nz), links.number(nz)
+    order = (4, 3, 5, 2, 6, 1, 7)
+    mine_units = (
+        pltpu.make_async_copy(units.at[z, 0:size], query_ref.at[z], local.at[14]),
+        pltpu.make_async_copy(units.at[z, size : 3 * size], kv_ref.at[z, :, here], local.at[15]),
+    )
+    for d in order:
+        to = at("sp_0", nz, d)
+        links.start(units.at[to, size : 3 * size], kv_ref.at[z, :, here], zk + d, "sp_0", to)
+    for made in mine_units:
+        made.start()
+    for d in order:
+        to = at("sp_0", nz, d)
+        links.start(units.at[to, 0:size], query_ref.at[z], zq + d, "sp_0", to)
+
+    kv_r, kv_l = links.number(nz), links.number(nz)
+    kv_rr, kv_ll = links.number(nz), links.number(nz)
+
+    def kv_piece(row, by, lo=0, count=2 * size):
+        cols = pl.ds(pl.multiple_of(at("sp_1", ny, by) * tokens, tokens), tokens)
+        return kv_ref.at[row, lo : lo + count, cols]
+
+    def give(d):
+        row = at("sp_0", nz, -d)
+        if d:
+            links.arrived(kv_ref.at[row, :, here], zk + d, "sp_0")
+        links.start(kv_piece(row, 0), kv_piece(row, 0), kv_r + d, "sp_1", y_right)
+        links.start(kv_piece(row, 0), kv_piece(row, 0), kv_l + d, "sp_1", y_left)
+
+    def forward(d):
+        row = at("sp_0", nz, -d)
+        links.arrived(kv_piece(row, -1), kv_r + d, "sp_1")
+        links.start(
+            kv_piece(row, -1, 0, size), kv_piece(row, -1, 0, size), kv_rr + d, "sp_1", y_right
+        )
+        links.arrived(kv_piece(row, 1), kv_l + d, "sp_1")
+        links.start(
+            kv_piece(row, 1, size, size), kv_piece(row, 1, size, size), kv_ll + d, "sp_1", y_left
+        )
+
+    def delta_next(i, carried):
+        delta_sequence(lax.rem(x + i, nx))
+        return carried
+
+    for made in mine_units:
+        made.wait()
+    give(0)
+    lax.fori_loop(1, nx, delta_next, 0)
+    keep_shift.wait()
+    for d in range(1, nx):
+        links.arrived(shift_ref.at[at("fs", nx, -d)], shifts + d, "fs")
 
     def mul(a, b, contract=((1,), (0,))):
         return lax.dot_general(
@@ -359,8 +337,8 @@
     same = row_at // BLOCK == col_at // BLOCK
     inclusive = same & (col_at <= row_at)
     strictly = same & (col_at < row_at)
-    decay_pre = jnp.concatenate([pre_ref[s, 0:1] for s in range(nx)], axis=0)
-    write_pre = jnp.concatenate([pre_ref[s, 1:2] for s in range(nx)], axis=0)
+    decay_pre = jnp.concatenate([pre_ref[s, pl.ds(x, 1)] for s in range(nx)], axis=0)
+    write_pre = jnp.concatenate([pre_ref[s, pl.ds(nx + x, 1)] for s in range(nx)], axis=0)
     shift = jnp.concatenate([shift_ref[s] for s in range(nx)], axis=0)
     softplus = jnp.maximum(decay_pre, 0.0) + jnp.log1p(jnp.exp(-jnp.abs(decay_pre)))
     rate = jnp.exp(jnp.full(decay_pre.shape, scale_ref[x], jnp.float32))
@@ -422,8 +400,25 @@
             )
         transfer[s] = low(carried)
 
-    for s in range(nx):
-        local_part(s)
+    give(4)
+    local_part(0)
+    give(3)
+    give(5)
+    forward(0)
+    local_part(1)
+    give(2)
+    give(6)
+    forward(4)
+    forward(3)
+    local_part(2)
+    give(1)
+    give(7)
+    forward(5)
+    forward(2)
+    local_part(3)
+    forward(6)
+    forward(1)
+    forward(7)
 
     one = links.number(ny)
     for d in (2, 1, 3):
@@ -431,6 +426,12 @@
         links.start(transfer.at[to], stage1.at[y], one + d, "sp_1", to)
     mine = pltpu.make_async_copy(transfer.at[y], stage1.at[y], local.at[2])
     mine.start()
+    for d in (0,) + order:
+        row = at("sp_0", nz, -d)
+        if d:
+            links.arrived(query_ref.at[row], zq + d, "sp_0")
+        links.arrived(kv_piece(row, 2, 0, size), kv_rr + d, "sp_1")
+        links.arrived(kv_piece(row, 2, size, size), kv_ll + d, "sp_1")
     two, three = links.number(nz), links.number(ny)
     keep_own = pltpu.make_async_copy(leaving.at[y], incoming.at[y], local.at[3])
 
@@ -656,23 +657,34 @@
     links.drain()
 
 
-def mix(offset, bias, scale, queries, keys_values, delta_proj, pre, shift, gain, sb_out, delta_out):
+def layer(offset, bias, scale, hidden, decay, write, shift, gain, sb_w, delta_w, sb_out, delta_out):
     nz, ny, nx = (lax.axis_size(a) for a in ("sp_0", "sp_1", "fs"))
-    size, tile = queries.shape[1:]
-    key = delta_proj.shape[2] // 3
+    tile, part = hidden.shape
+    rows, lanes = sb_w[0].shape[0], sb_w[0].shape[1] // nx
+    size, key = lanes // 2, lanes
     columns = sb_out.shape[1]
     half = tile // 2
     smem = pl.BlockSpec(memory_space=pltpu.SMEM)
     vmem = pl.BlockSpec(memory_space=pltpu.VMEM)
     anywhere = pl.BlockSpec(memory_space=pl.ANY)
-    copies = 64
+    copies = 160
     bf16, f32 = jnp.bfloat16, jnp.float32
     return pl.pallas_call(
-        mix_kernel,
+        layer_kernel,
         out_shape=jax.ShapeDtypeStruct((half, columns), bf16),
-        in_specs=[smem] * 3 + [vmem] * 6 + [anywhere] * 2,
+        in_specs=[smem] * 3 + [vmem] * 5 + [anywhere] * 8,
         out_specs=vmem,
         scratch_shapes=[
+            pltpu.VMEM((nx, 2, tile, part), bf16),
+            pltpu.VMEM((nx, rows, 3 * lanes), bf16),
+            pltpu.VMEM((nx, rows, 4 * lanes), bf16),
+            pltpu.VMEM((nz, 3 * size, tile), bf16),
+            pltpu.VMEM((nz, size, tile), bf16),
+            pltpu.VMEM((nz, 2 * size, ny * tile), bf16),
+            pltpu.VMEM((nx, tile, 3 * key), bf16),
+            pltpu.VMEM((nx, 8, tile), f32),
+            pltpu.VMEM((nx, 1, tile), f32),
+            pltpu.VMEM((nx, 1, tile), f32),
             pltpu.VMEM((tile, tile), bf16),
             pltpu.VMEM((tile, size), bf16),
             pltpu.VMEM((tile, size), f32),
@@ -694,14 +706,11 @@
             pltpu.VMEM((tile, nz * size + nx * key), bf16),
             pltpu.SemaphoreType.DMA((copies,)),
             pltpu.SemaphoreType.DMA((copies,)),
-            pltpu.SemaphoreType.DMA((6,)),
+            pltpu.SemaphoreType.DMA((16,)),
         ],
-        compiler_params=pltpu.CompilerParams(collective_id=1, has_side_effects=True),
-        name="mix",
-        cost_estimate=pl.CostEstimate(
-            flops=60_000_000_000, bytes_accessed=10_000_000, transcendentals=30_000_000
-        ),
-    )(offset, bias, scale, queries, keys_values, delta_proj, pre, shift, gain, sb_out, delta_out)
+        compiler_params=pltpu.CompilerParams(collective_id=0, has_side_effects=True),
+        name="layer",
+    )(offset, bias, scale, hidden, decay, write, shift, gain, *sb_w, *delta_w, sb_out, delta_out)
 
 
 def on_device(
@@ -723,30 +732,17 @@
     delta_out_w,
 ):
     tokens, part = hidden_in.shape[1], hidden_in.shape[2]
-    fs_count = lax.axis_size("fs")
-    mine = lax.axis_index("fs")
-    gates_w = jnp.concatenate(
-        [lax.dynamic_slice_in_dim(w, mine, 1, 1) for w in (decay_w, write_w)], axis=1
-    )
-    lanes = sb_query_w.shape[1] // fs_count
-    gates_w = jnp.pad(gates_w, ((0, 0), (0, lanes - 2))).reshape(fs_count, -1, lanes)
-    unit_queries, keys_values, delta_proj, pre, shift = project_and_share(
-        hidden_in.reshape(tokens, part),
-        gates_w,
-        decay_shift.reshape(fs_count, 1, tokens),
-        (sb_query_w, sb_key_w, sb_value_w),
-        (delta_query_w, delta_key_w, delta_value_w),
-    )
-    result = mix(
+    result = layer(
         sb_offset,
         write_bias,
         decay_log_scale,
-        unit_queries,
-        keys_values,
-        delta_proj,
-        pre,
-        shift,
+        hidden_in.reshape(tokens, part),
+        decay_w.T,
+        write_w.T,
+        decay_shift.reshape(-1, tokens),
         head_gain.reshape(1, -1),
+        (sb_query_w, sb_key_w, sb_value_w),
+        (delta_query_w, delta_key_w, delta_value_w),
         sb_out_w,
         delta_out_w,
     )

time: 159 us -> 123 us (0.77)
  Pallas kernels: 153 us -> 121 us
  local copies, waits for them, and re-layouts: 5.14 us -> 1.88 us
    pallas_call x2 -> x1, Pallas kernels: 153 us -> 121 us  [layer(): pl.pallas_call(layer_kernel, out_shape=jax.ShapeDtypeStruct((half, column...]
where the time goes in v4:
time: 123 us
  Pallas kernels  121 us (98%)
  local copies, waits for them, and re-layouts  1.88 us (2%)
    pallas_call x1, Pallas kernels, layer(): pl.pallas_call(layer_kernel, out_shape=jax.ShapeDtypeStruct((half, column...  121 us

profile of v4, /device:TPU:249, one launch (start us, length us, event | category | flops | bytes accessed | tf_op | source)
XLA Modules:
  0.0 122.7 jit_solution(10456767199466923107)
XLA Ops:
  0.0 120.8 %layer.1 = bf16[128,2048]{1,0:T(8,128)(2,1)} custom-call(f32[8]{0:T(128)} %offset_ref.1, f32[4]{0:T(128)} %bias_ref.1, f32[4]{0:T(128)} %scale_ref.1, bf16[256,1024]{1,0:T(8,128)(2,1)} %bitcast.7, bf16[4,2048]{1,0:T(4,128)(2,1)} %bitcast.8, bf16[4,2048]{1,0:T(4,128)(2,1)} %bitcast.9, f32[4,256]{1,0:T(4,128)} %bitcast.10, f32[1,128]{1,0:T(1,128)} %bitcast.11, ...), custom_call_target="tpu_custom_call" | custom-call | tf_op jit(solution)/shard_map/layer/pallas_call | solution.py:672
  120.8 1.9 %copy.18 = bf16[1,128,2048]{2,1,0:T(8,128)(2,1)} copy(bf16[1,128,2048]{2,1,0:T(8,128)(2,1)} %bitcast.6) | data formatting | bytes 1048576

commit v5 on v4

--- a/solution.py
+++ b/solution.py
@@ -74,6 +74,7 @@
     key = delta_ref.shape[2] // 3
     lanes = q0.shape[1] // nx
     width = 3 * lanes
+    extra = kv_ref.shape[1] - 2 * size
     z_rows, y_rows = q0.shape[0] // nz, q0.shape[0] // ny
 
     def at(axis, count, by):
@@ -146,7 +147,19 @@
     row_at = lax.broadcasted_iota(jnp.int32, (tile, tile), 0)
     col_at = lax.broadcasted_iota(jnp.int32, (tile, tile), 1)
     later_ref[...] = jnp.where(row_at > col_at, 1.0, 0.0).astype(jnp.bfloat16)
-    offset = offset_ref[2 * x + lax.rem(z, 2)]
+    offset = jnp.full((tile, extra), offset_ref[2 * x + lax.rem(z, 2)], jnp.float32)
+    parts = []
+    for _ in range(3):
+        parts.append(low(offset).astype(jnp.float32))
+        offset = offset - parts[-1]
+    part_at = lax.broadcasted_iota(jnp.int32, (tile, extra), 1)
+    offset_part = jnp.zeros((tile, extra), jnp.float32)
+    for k in range(3):
+        offset_part = jnp.where(part_at == k, parts[k], offset_part)
+    for row in range(nz):
+        kv_ref[row, 2 * size : 2 * size + extra, :] = jnp.ones(
+            (extra, kv_ref.shape[2]), jnp.bfloat16
+        )
 
     z_right, z_left = at("sp_0", nz, 1), at("sp_0", nz, -1)
     y_right, y_left = at("sp_1", ny, 1), at("sp_1", ny, -1)
@@ -250,10 +263,11 @@
 
     def sb_sequence(c):
         out = product(c, sb_w)
-        for m in range(3):
+        for m, place in enumerate((0, 2, 1)):
             block = low(out[:, m * lanes : (m + 1) * lanes].T)
-            units[2 * c, m * size : (m + 1) * size, :] = block[0:size]
-            units[2 * c + 1, m * size : (m + 1) * size, :] = block[size:lanes]
+            rows = slice(place * size, (place + 1) * size)
+            units[2 * c, rows, :] = block[0:size]
+            units[2 * c + 1, rows, :] = block[size:lanes]
 
     def delta_sequence(c):
         out = product(c, delta_w)
@@ -281,11 +295,11 @@
     order = (4, 3, 5, 2, 6, 1, 7)
     mine_units = (
         pltpu.make_async_copy(units.at[z, 0:size], query_ref.at[z], local.at[14]),
-        pltpu.make_async_copy(units.at[z, size : 3 * size], kv_ref.at[z, :, here], local.at[15]),
+        pltpu.make_async_copy(units.at[z, size : 3 * size], kv_ref.at[z, 0 : 2 * size, here], local.at[15]),
     )
     for d in order:
         to = at("sp_0", nz, d)
-        links.start(units.at[to, size : 3 * size], kv_ref.at[z, :, here], zk + d, "sp_0", to)
+        links.start(units.at[to, size : 3 * size], kv_ref.at[z, 0 : 2 * size, here], zk + d, "sp_0", to)
     for made in mine_units:
         made.start()
     for d in order:
@@ -302,7 +316,7 @@
     def give(d):
         row = at("sp_0", nz, -d)
         if d:
-            links.arrived(kv_ref.at[row, :, here], zk + d, "sp_0")
+            links.arrived(kv_ref.at[row, 0 : 2 * size, here], zk + d, "sp_0")
         links.start(kv_piece(row, 0), kv_piece(row, 0), kv_r + d, "sp_1", y_right)
         links.start(kv_piece(row, 0), kv_piece(row, 0), kv_l + d, "sp_1", y_left)
 
@@ -499,13 +513,10 @@
         beyond = None if diagonal else beyond_ref[...]
         weights = []
         for k in range(count - 1, -1, -1):
-            scores = (
-                jnp.dot(
-                    queries,
-                    kv_ref[row, 0:size, k * tile : (k + 1) * tile],
-                    preferred_element_type=jnp.float32,
-                )
-                + offset
+            scores = jnp.dot(
+                queries,
+                kv_ref[row, size : 2 * size + extra, k * tile : (k + 1) * tile],
+                preferred_element_type=jnp.float32,
             )
             above = jnp.maximum(scores, 0.0)
             below = scores - above
@@ -525,8 +536,8 @@
             beyond = total if beyond is None else beyond + total
             weights.append(low(jnp.exp(exponent)))
         partial = lax.dot_general(
+            kv_ref[row, 0:size, 0 : count * tile],
             jnp.concatenate(weights[::-1], axis=1),
-            kv_ref[row, size : 2 * size, 0 : count * tile],
             (((1,), (1,)), ((), ())),
             preferred_element_type=jnp.float32,
         )
@@ -566,7 +577,8 @@
             sb_copy(row).start()
 
     def per_query(row, unused):
-        rows_ref[...] = low((query_ref[row].astype(jnp.float32) * size ** (-0.5)).T)
+        scaled = (query_ref[row].astype(jnp.float32) * size ** (-0.5)).T
+        rows_ref[...] = low(jnp.concatenate([scaled, offset_part], axis=1))
         pl.when(row == 3)(over_group)
         pl.when(row == 6)(over_line)
         pl.when(row == 7)(delta_end)
@@ -589,7 +601,7 @@
             return carried
 
         lax.fori_loop(0, row, earlier, 0)
-        done_ref[row] = low(acc_ref[...].T)
+        done_ref[row] = low(acc_ref[...])
         return unused
 
     lax.fori_loop(0, nz, per_query, 0)
@@ -680,14 +692,14 @@
             pltpu.VMEM((nx, rows, 4 * lanes), bf16),
             pltpu.VMEM((nz, 3 * size, tile), bf16),
             pltpu.VMEM((nz, size, tile), bf16),
-            pltpu.VMEM((nz, 2 * size, ny * tile), bf16),
+            pltpu.VMEM((nz, 2 * size + 16, ny * tile), bf16),
             pltpu.VMEM((nx, tile, 3 * key), bf16),
             pltpu.VMEM((nx, 8, tile), f32),
             pltpu.VMEM((nx, 1, tile), f32),
             pltpu.VMEM((nx, 1, tile), f32),
             pltpu.VMEM((tile, tile), bf16),
-            pltpu.VMEM((tile, size), bf16),
-            pltpu.VMEM((tile, size), f32),
+            pltpu.VMEM((tile, size + 16), bf16),
+            pltpu.VMEM((size, tile), f32),
             pltpu.VMEM((tile, 1), f32),
             pltpu.VMEM((nz, size, tile), bf16),
             pltpu.VMEM((2 * nx, size, tile), bf16),

time: 123 us -> 119 us (0.967)
  Pallas kernels: 121 us -> 117 us
    pallas_call x1, Pallas kernels: 121 us -> 117 us  [layer(): pl.pallas_call(layer_kernel, out_shape=jax.ShapeDtypeStruct((half, column...]
where the time goes in v5:
time: 119 us
  Pallas kernels  117 us (98%)
  local copies, waits for them, and re-layouts  1.88 us (2%)
    pallas_call x1, Pallas kernels, layer(): pl.pallas_call(layer_kernel, out_shape=jax.ShapeDtypeStruct((half, column...  117 us

profile of v5, /device:TPU:249, one launch (start us, length us, event | category | flops | bytes accessed | tf_op | source)
XLA Modules:
  0.0 118.6 jit_solution(11053226223949850816)
XLA Ops:
  0.0 116.7 %layer.1 = bf16[128,2048]{1,0:T(8,128)(2,1)} custom-call(f32[8]{0:T(128)} %offset_ref.1, f32[4]{0:T(128)} %bias_ref.1, f32[4]{0:T(128)} %scale_ref.1, bf16[256,1024]{1,0:T(8,128)(2,1)} %bitcast.7, bf16[4,2048]{1,0:T(4,128)(2,1)} %bitcast.8, bf16[4,2048]{1,0:T(4,128)(2,1)} %bitcast.9, f32[4,256]{1,0:T(4,128)} %bitcast.10, f32[1,128]{1,0:T(1,128)} %bitcast.11, ...), custom_call_target="tpu_custom_call" | custom-call | tf_op jit(solution)/shard_map/layer/pallas_call | solution.py:684
  116.7 1.9 %copy.18 = bf16[1,128,2048]{2,1,0:T(8,128)(2,1)} copy(bf16[1,128,2048]{2,1,0:T(8,128)(2,1)} %bitcast.6) | data formatting | bytes 1048576
